TPU v7x, 512 devices: a whole 4x8x8 slice. The times are simulated.
512 devices in a mesh: dp: 4 (over x), kv: 64 (over z, y), tp: 2 (over core).
Axes of the slice: x: 4, y: 8, z: 8, core: 2. Of those that a mesh axis runs over, the one named last changes fastest.
Arguments:
- tokens: bfloat16 [256, 4096], P('dp', ('kv', 'tp')), parts along dimension 0, may hold values from -16 to 16
- mix_gain: float32 [4096], replicated, may hold values from 0.1 to 1.9
- w_query: bfloat16 [4096, 2048], P('kv', 'tp'), may hold values from -0.09375 to 0.09375
- w_key: bfloat16 [4096, 2048], P('kv', 'tp'), may hold values from -0.09375 to 0.09375
- w_value: bfloat16 [4096, 4096], P('kv', 'tp'), may hold values from -0.09375 to 0.09375
- w_igate: bfloat16 [4096, 16], replicated, may hold values from -0.09375 to 0.09375
- w_fgate: bfloat16 [4096, 16], replicated, may hold values from -0.09375 to 0.09375
- igate_bias: float32 [16], replicated, may hold values from -3 to 1
- fgate_bias: float32 [16], replicated, may hold values from -2 to 5
- memory: float32 [256, 16, 256, 128], P(('dp', 'kv'), 'tp'), parts along dimension 0, may hold values from -6 to 6
- normalizer: float32 [256, 16, 128], P(('dp', 'kv'), 'tp'), parts along dimension 0, may hold values from -6 to 6
- stabilizer: float32 [256, 16], P(('dp', 'kv'), 'tp'), parts along dimension 0, may hold values from -3 to 3
- w_output: bfloat16 [4096, 4096], P('tp', 'kv'), may hold values from -0.09375 to 0.09375
- mlp_gain: float32 [4096], replicated, may hold values from 0.1 to 1.9
- w_up: bfloat16 [4096, 16384], P(None, ('kv', 'tp')), may hold values from -0.09375 to 0.09375
- w_down: bfloat16 [16384, 4096], P(('kv', 'tp')), may hold values from -0.1875 to 0.1875
Outputs:
- new_tokens: bfloat16 [256, 4096], P('dp', ('kv', 'tp')), parts along dimension 0
- new_memory: float32 [256, 16, 256, 128], P(('dp', 'kv'), 'tp'), parts along dimension 0
- new_normalizer: float32 [256, 16, 128], P(('dp', 'kv'), 'tp'), parts along dimension 0
- new_stabilizer: float32 [256, 16], P(('dp', 'kv'), 'tp'), parts along dimension 0
There are 4 independent parts, one for each index of `dp`. A program takes and returns all parts, laid end to end along the dimension named above; an argument that names none is the same for every part. Nothing has to cross between parts.
All inputs are finite; a program needn't handle non-finite values.
Results may differ from a plain program's by a relative error of at most 0.019.
Values may be sent and summed in bfloat16 or wider, within the bound.
No kernel may reach another device: no remote copies, remote signals or barrier semaphores. Data moves between devices by JAX's collectives and lax.ppermute only.
A program may use at most 64 MiB of HBM per device.

v0:
```python
import jax
import jax.numpy as jnp
from jax import lax
from jax.sharding import PartitionSpec as P

DV = 256
DQK = 128


norm_eps = 1e-06


def cut_along(shard, dim, length):
    before, after = (shard.shape[:dim], shard.shape[dim + 1 :])
    return jnp.moveaxis(shard.reshape(*before, length, -1, *after), dim, 0)


def summed_on_arrival(shard, axis, dim):
    length = lax.axis_size(axis)
    tiles = lax.all_to_all(cut_along(shard, dim, length), axis, 0, 0, tiled=True)
    return jnp.sum(tiles.astype(jnp.float32), axis=0)


def from_everyone(shard, axis):
    length = lax.axis_size(axis)
    return lax.all_to_all(
        jnp.broadcast_to(shard[None], (length, *shard.shape)), axis, 0, 0, tiled=True
    )


def joined_along(tiles, dim):
    dims = list(tiles.shape[1:])
    dims[dim] *= tiles.shape[0]
    return jnp.moveaxis(tiles, 0, dim).reshape(dims)


def collect(shard, axis, dim):
    tiles = from_everyone(shard, axis)
    return joined_along(tiles, dim)


def of_everyone(shard, axis):
    return from_everyone(shard, axis).astype(jnp.float32).sum(axis=0)


def rms_normed(rows, gain):
    wide_rows = rows.astype(jnp.float32)
    scale = lax.rsqrt(jnp.mean(wide_rows * wide_rows, axis=-1, keepdims=True) + norm_eps)
    return (wide_rows * scale * gain).astype(jnp.bfloat16)


def on_device(
    tokens,
    mix_gain,
    w_query,
    w_key,
    w_value,
    w_igate,
    w_fgate,
    igate_bias,
    fgate_bias,
    memory,
    normalizer,
    stabilizer,
    w_output,
    mlp_gain,
    w_up,
    w_down,
):
    kv_count = lax.axis_size("kv")
    tp_count = lax.axis_size("tp")
    kv_index = lax.axis_index("kv")
    tp_index = lax.axis_index("tp")
    own_rows = memory.shape[0]
    head_count = memory.shape[1]
    whole_rows = lax.all_gather(tokens, ("kv", "tp"), axis=1, tiled=True)
    wide_rows = whole_rows.astype(jnp.float32)
    normed = rms_normed(whole_rows, mix_gain)
    row_span = w_query.shape[0]
    own_cols = lax.dynamic_slice_in_dim(normed, kv_index * row_span, row_span, 1)
    joined = summed_on_arrival(
        jnp.concatenate(
            [
                jnp.dot(own_cols, w_query, preferred_element_type=jnp.float32),
                jnp.dot(own_cols, w_key, preferred_element_type=jnp.float32),
                jnp.dot(own_cols, w_value, preferred_element_type=jnp.float32),
            ],
            axis=1,
        ).astype(jnp.bfloat16),
        "kv",
        0,
    )
    query_cols = w_query.shape[1]
    queries = joined[:, :query_cols].reshape(own_rows, head_count, DQK) * DQK ** (-0.5)
    key_rows = joined[:, query_cols : 2 * query_cols].reshape(own_rows, head_count, DQK)
    values = joined[:, 2 * query_cols :].reshape(own_rows, head_count, DV)
    own_normed = lax.dynamic_slice_in_dim(normed, kv_index * own_rows, own_rows, 0)
    igate_cols = lax.dynamic_slice_in_dim(w_igate, tp_index * head_count, head_count, 1)
    fgate_cols = lax.dynamic_slice_in_dim(w_fgate, tp_index * head_count, head_count, 1)
    ibias_own = lax.dynamic_slice_in_dim(igate_bias, tp_index * head_count, head_count, 0)
    fbias_own = lax.dynamic_slice_in_dim(fgate_bias, tp_index * head_count, head_count, 0)
    input_gate = jnp.dot(own_normed, igate_cols, preferred_element_type=jnp.float32) + ibias_own
    log_forget = jax.nn.log_sigmoid(
        jnp.dot(own_normed, fgate_cols, preferred_element_type=jnp.float32) + fbias_own
    )
    carried = log_forget + stabilizer
    new_stabilizer = jnp.maximum(carried, input_gate)
    keep_weight = jnp.exp(carried - new_stabilizer)
    fresh_weight = jnp.exp(input_gate - new_stabilizer)
    recall = jnp.einsum("bhvd,bhd->bhv", memory, queries, precision=lax.Precision.HIGHEST)
    match_score = jnp.sum(queries * key_rows, axis=-1)
    numerator = keep_weight[..., None] * recall + (fresh_weight * match_score)[..., None] * values
    denominator = keep_weight * jnp.sum(normalizer * queries, axis=-1) + fresh_weight * match_score
    floor_value = jnp.maximum(jnp.abs(denominator), jnp.exp(-new_stabilizer))
    cell_out = (
        (numerator / floor_value[..., None]).astype(jnp.bfloat16).reshape(own_rows, head_count * DV)
    )
    new_memory = (
        keep_weight[..., None, None] * memory
        + fresh_weight[..., None, None] * values[..., :, None] * key_rows[..., None, :]
    )
    new_normalizer = keep_weight[..., None] * normalizer + fresh_weight[..., None] * key_rows
    partial_value = jnp.dot(
        collect(cell_out, "kv", 0), w_output, preferred_element_type=jnp.float32
    )
    block_cols = partial_value.shape[1]
    pair_total = of_everyone(partial_value.astype(jnp.bfloat16), "tp").astype(jnp.float32)
    local_rows = lax.dynamic_slice_in_dim(wide_rows, kv_index * block_cols, block_cols, 1)
    middle_block = (local_rows + pair_total).astype(jnp.bfloat16)
    middle = collect(middle_block, "kv", 1)
    mixer_in = rms_normed(middle, mlp_gain)
    up_rows = jnp.dot(mixer_in, w_up, preferred_element_type=jnp.float32)
    activation = jnp.square(jax.nn.relu(up_rows)).astype(jnp.bfloat16)
    thin_cols = tokens.shape[1]
    hidden_rows = w_down.shape[0]
    reordered = jnp.transpose(
        w_down.reshape(hidden_rows, kv_count, tp_count, thin_cols), (0, 2, 1, 3)
    ).reshape(hidden_rows, tp_count * kv_count * thin_cols)
    chip_sums = summed_on_arrival(
        lax.dot_general(
            reordered, activation, (((0,), (1,)), ((), ())), preferred_element_type=jnp.float32
        ).astype(jnp.bfloat16),
        "tp",
        0,
    )
    down_cols = summed_on_arrival(chip_sums.astype(jnp.bfloat16), "kv", 0)
    middle_own = lax.dynamic_slice_in_dim(
        middle, (kv_index * tp_count + tp_index) * thin_cols, thin_cols, 1
    )
    new_tokens = (middle_own.astype(jnp.float32) + down_cols.T).astype(jnp.bfloat16)
    return (new_tokens, new_memory, new_normalizer, new_stabilizer)


def solution(mesh):
    in_specs = (
        P("dp", ("kv", "tp")),
        P(),
        P("kv", "tp"),
        P("kv", "tp"),
        P("kv", "tp"),
        P(),
        P(),
        P(),
        P(),
        P(("dp", "kv"), "tp", None, None),
        P(("dp", "kv"), "tp", None),
        P(("dp", "kv"), "tp"),
        P("tp", "kv"),
        P(),
        P(None, ("kv", "tp")),
        P(("kv", "tp"), None),
    )
    out_specs = (
        P("dp", ("kv", "tp")),
        P(("dp", "kv"), "tp", None, None),
        P(("dp", "kv"), "tp", None),
        P(("dp", "kv"), "tp"),
    )
    return jax.shard_map(
        on_device, mesh=mesh, in_specs=in_specs, out_specs=out_specs, check_vma=False
    )
```

profile of v0, /device:TPU:1, one launch (start us, length us, event | category | flops | bytes accessed | tf_op | source)
XLA Modules:
  0.0 189.8 jit_solution(15945729594412308125)
XLA Ops:
  0.6 59.5 %all_gather.3 = bf16[64,4096]{0,1:T(8,128)(2,1)S(1)} all-gather(bf16[64,32]{0,1:T(8,128)(2,1)} %param.16), channel_id=1, replica_groups=mesh['dp'=4,'kv'=64,'tp'=2] {'kv','tp'}, dimensions={1}, use_global_device_ids=true | all-gather | bytes 528384 | tf_op jit(solution)/shard_map/all_gather | solution.py:76
  63.9 1.2 reshape.279
  65.1 7.1 %all-to-all-start = ((bf16[64,2,2048]{2,1,0:T(2,128)(2,1)}), bf16[64,2,2048]{2,1,0:T(2,128)(2,1)S(1)}, u32[]{:S(2)}, u32[]{:S(2)}) async-start(bf16[64,2,2048]{2,1,0:T(2,128)(2,1)} %reshape.279), calls=%async_computation | async-start | bytes 1048576 | tf_op jit(solution)/shard_map/all_to_all | solution.py:20
  74.3 15.7 %all-to-all-done = bf16[64,2,2048]{2,1,0:T(2,128)(2,1)S(1)} async-done(((bf16[64,2,2048]{2,1,0:T(2,128)(2,1)}), bf16[64,2,2048]{2,1,0:T(2,128)(2,1)S(1)}, u32[]{:S(2)}, u32[]{:S(2)}) %all-to-all-start) | async-done | bytes 524320 | tf_op jit(solution)/shard_map/all_to_all | solution.py:20
  90.0 1.8 reshape.280
  91.8 2.4 %convert_reduce_fusion.1 = f32[4096]{0:T(1024)S(1)} fusion(bf16[64,1,4096]{2,1,0:T(2,128)(2,1)} %reshape.280), kind=kLoop, calls=%fused_computation.25 | loop fusion | flops 520192 | bytes 540672 | tf_op jit(solution)/shard_map/reduce_sum | solution.py:21
  96.4 2.2 %reduce.10 = bf16[64,2048]{1,0:T(8,128)(2,1)S(1)} reduce(bf16[64,1,2048]{2,1,0:T(2,128)(2,1)S(1)} %broadcast_in_dim.9, bf16[]{:T(256)} %broadcast.126), dimensions={1}, to_apply=%broadcast_in_dim.9.reduce_sub_computation | reduce | bytes 524290 | tf_op jit(solution)/shard_map/broadcast_in_dim | solution.py:27
  99.5 6.6 %all-to-all-start.1 = ((bf16[64,2,1024]{2,1,0:T(2,128)(2,1)}), bf16[64,2,1024]{2,1,0:T(2,128)(2,1)S(1)}, u32[]{:S(2)}, u32[]{:S(2)}) async-start(bf16[64,2,1024]{2,1,0:T(2,128)(2,1)} %reshape.281), calls=%async_computation.1 | async-start | bytes 524288 | tf_op jit(solution)/shard_map/all_to_all | solution.py:26
  107.1 11.3 %all-to-all-done.1 = bf16[64,2,1024]{2,1,0:T(2,128)(2,1)S(1)} async-done(((bf16[64,2,1024]{2,1,0:T(2,128)(2,1)}), bf16[64,2,1024]{2,1,0:T(2,128)(2,1)S(1)}, u32[]{:S(2)}, u32[]{:S(2)}) %all-to-all-start.1) | async-done | bytes 262176 | tf_op jit(solution)/shard_map/all_to_all | solution.py:26
  119.0 6.8 %all_to_all.30 = bf16[2,2,2048]{2,1,0:T(2,128)(2,1)S(1)} all-to-all(bf16[2,2,2048]{2,1,0:T(2,128)(2,1)S(1)} %reshape.283), channel_id=1, replica_groups=mesh['dp'=4,'kv'=64,'tp'=2] {'tp'}, dimensions={0} | all-to-all | bytes 32768 | tf_op jit(solution)/shard_map/all_to_all | solution.py:26
  127.2 1.6 reshape.285
  128.7 5.5 %all-to-all-start.3 = ((bf16[64,2,2048]{2,1,0:T(2,128)(2,1)}), bf16[64,2,2048]{2,1,0:T(2,128)(2,1)}, u32[]{:S(2)}, u32[]{:S(2)}) async-start(bf16[64,2,2048]{2,1,0:T(2,128)(2,1)} %reshape.285), calls=%async_computation.3 | async-start | bytes 1048576 | tf_op jit(solution)/shard_map/all_to_all | solution.py:26
  134.2 1.6 copy.44
  135.8 1.1 copy.45
  136.9 15.1 %all-to-all-done.3 = bf16[64,2,2048]{2,1,0:T(2,128)(2,1)} async-done(((bf16[64,2,2048]{2,1,0:T(2,128)(2,1)}), bf16[64,2,2048]{2,1,0:T(2,128)(2,1)}, u32[]{:S(2)}, u32[]{:S(2)}) %all-to-all-start.3) | async-done | bytes 524320 | tf_op jit(solution)/shard_map/all_to_all | solution.py:26
  152.0 2.3 %reshape.286 = bf16[64,64,64]{2,1,0:T(8,128)(2,1)S(1)} reshape(bf16[64,2,2048]{2,1,0:T(2,128)(2,1)} %all-to-all-done.3) | data formatting | bytes 1048576
  154.9 3.5 %convolution_convert_fusion = bf16[64,4096]{1,0:T(8,128)(2,1)} fusion(bf16[128,4096]{0,1:T(8,128)(2,1)} %bitcast.116, bf16[4096,128]{1,0:T(8,128)(2,1)S(1)} %copy-done, bf16[64,4096]{0,1:T(8,128)(2,1)S(1)} %bitcast.113, f32[4096]{0:T(1024)S(1)} %copy-done.7, f32[64]{0:T(128)S(1)} %add_rsqrt_fusion), kind=kOutput, calls=%fused_computation | convolution fusion | flops 135553024 | bytes 3162368 | tf_op jit(solution)/shard_map/dot_general | solution.py:140
  158.4 1.1 copy.63
  159.5 6.0 %all_to_all.31 = bf16[2,2048,64]{1,2,0:T(8,128)(2,1)} all-to-all(bf16[2,2048,64]{1,2,0:T(8,128)(2,1)S(1)} %bitcast.118), channel_id=1, replica_groups=mesh['dp'=4,'kv'=64,'tp'=2] {'tp'}, dimensions={0} | all-to-all | bytes 1048576 | tf_op jit(solution)/shard_map/all_to_all | solution.py:20
  165.5 1.1 reduce_sum.90
  167.6 2.1 %reshape.287 = bf16[64,2,1024]{2,1,0:T(2,128)(2,1)} reshape(bf16[64,32,64]{2,1,0:T(8,128)(2,1)} %bitcast.117) | data formatting | bytes 524288
  169.7 5.9 %all-to-all-start.5 = ((bf16[64,2,1024]{2,1,0:T(2,128)(2,1)}), bf16[64,2,1024]{2,1,0:T(2,128)(2,1)S(1)}, u32[]{:S(2)}, u32[]{:S(2)}) async-start(bf16[64,2,1024]{2,1,0:T(2,128)(2,1)} %reshape.287), calls=%async_computation.5 | async-start | bytes 524288 | tf_op jit(solution)/shard_map/all_to_all | solution.py:20
  175.6 1.3 multiply_add_fusion
  177.0 11.8 %all-to-all-done.5 = bf16[64,2,1024]{2,1,0:T(2,128)(2,1)S(1)} async-done(((bf16[64,2,1024]{2,1,0:T(2,128)(2,1)}), bf16[64,2,1024]{2,1,0:T(2,128)(2,1)S(1)}, u32[]{:S(2)}, u32[]{:S(2)}) %all-to-all-start.5) | async-done | bytes 262176 | tf_op jit(solution)/shard_map/all_to_all | solution.py:20
  (72 shorter events, 14.3 us)
Async XLA Ops:
  0.6 154.3 %copy-start = (bf16[4096,128]{1,0:T(8,128)(2,1)S(1)}, bf16[4096,128]{1,0:T(8,128)(2,1)}, u32[]{:S(2)}) copy-start(bf16[4096,128]{1,0:T(8,128)(2,1)} %param.30) | copy-start | bytes 3145732
  60.2 0.7 copy-start.6
  60.5 1.0 copy-start.3
  60.5 1.2 copy-start.4
  60.8 1.3 copy-start.5
  61.1 0.9 copy-start.2
  63.8 8.4 %copy-start.11 = (bf16[4096,16]{0,1:T(8,128)(2,1)S(1)}, bf16[4096,16]{0,1:T(8,128)(2,1)}, u32[]{:S(2)}) copy-start(bf16[4096,16]{0,1:T(8,128)(2,1)} %param.21) | copy-start | bytes 393220
  63.8 8.4 %copy-start.13 = (f32[16]{0:T(128)S(1)}, f32[16]{0:T(128)}, u32[]{:S(2)}) copy-start(f32[16]{0:T(128)} %param.23) | copy-start | bytes 196
  63.9 9.4 %copy-start.12 = (bf16[4096,16]{0,1:T(8,128)(2,1)S(1)}, bf16[4096,16]{0,1:T(8,128)(2,1)}, u32[]{:S(2)}) copy-start(bf16[4096,16]{0,1:T(8,128)(2,1)} %param.22) | copy-start | bytes 393220
  63.9 9.4 %copy-start.14 = (f32[1,8]{1,0:T(1,128)S(1)}, f32[1,8]{1,0:T(1,128)}, u32[]{:S(2)}) copy-start(f32[1,8]{1,0:T(1,128)} %param.27) | copy-start | bytes 100
  63.9 9.4 %copy-start.15 = (f32[16]{0:T(128)S(1)}, f32[16]{0:T(128)}, u32[]{:S(2)}) copy-start(f32[16]{0:T(128)} %param.24) | copy-start | bytes 196
  65.1 25.0 %all-to-all-start = ((bf16[64,2,2048]{2,1,0:T(2,128)(2,1)}), bf16[64,2,2048]{2,1,0:T(2,128)(2,1)S(1)}, u32[]{:S(2)}, u32[]{:S(2)}) async-start(bf16[64,2,2048]{2,1,0:T(2,128)(2,1)} %reshape.279), calls=%async_computation | async-start | bytes 1048576 | tf_op jit(solution)/shard_map/all_to_all | solution.py:20
  74.3 21.7 %copy-start.9 = (f32[1,8]{1,0:T(1,128)}, f32[1,8]{1,0:T(1,128)S(1)}, u32[]{:S(2)}) copy-start(f32[1,8]{1,0:T(1,128)S(1)} %get-tuple-element.7) | copy-start | bytes 100
  74.3 19.9 %copy-start.1 = (f32[1,8,256,128]{3,2,1,0:T(8,128)S(1)}, f32[1,8,256,128]{3,2,1,0:T(8,128)}, u32[]{:S(2)}) copy-start(f32[1,8,256,128]{3,2,1,0:T(8,128)} %param.25) | copy-start | bytes 3145732
  91.8 3.4 %copy-start.8 = (f32[1,8,128]{2,1,0:T(8,128)S(1)}, f32[1,8,128]{2,1,0:T(8,128)}, u32[]{:S(2)}) copy-start(f32[1,8,128]{2,1,0:T(8,128)} %param.26) | copy-start | bytes 12292
  99.5 18.9 %all-to-all-start.1 = ((bf16[64,2,1024]{2,1,0:T(2,128)(2,1)}), bf16[64,2,1024]{2,1,0:T(2,128)(2,1)S(1)}, u32[]{:S(2)}, u32[]{:S(2)}) async-start(bf16[64,2,1024]{2,1,0:T(2,128)(2,1)} %reshape.281), calls=%async_computation.1 | async-start | bytes 524288 | tf_op jit(solution)/shard_map/all_to_all | solution.py:26
  106.1 12.5 %copy-start.10 = (bf16[2048,64]{0,1:T(8,128)(2,1)S(1)}, bf16[2048,64]{0,1:T(8,128)(2,1)}, u32[]{:S(2)}) copy-start(bf16[2048,64]{0,1:T(8,128)(2,1)} %param.28) | copy-start | bytes 786436
  128.7 23.3 %all-to-all-start.3 = ((bf16[64,2,2048]{2,1,0:T(2,128)(2,1)}), bf16[64,2,2048]{2,1,0:T(2,128)(2,1)}, u32[]{:S(2)}, u32[]{:S(2)}) async-start(bf16[64,2,2048]{2,1,0:T(2,128)(2,1)} %reshape.285), calls=%async_computation.3 | async-start | bytes 1048576 | tf_op jit(solution)/shard_map/all_to_all | solution.py:26
  136.9 18.0 %copy-start.7 = (f32[4096]{0:T(1024)S(1)}, f32[4096]{0:T(1024)}, u32[]{:S(2)}) copy-start(f32[4096]{0:T(1024)} %param.29) | copy-start | bytes 49156
  169.7 19.0 %all-to-all-start.5 = ((bf16[64,2,1024]{2,1,0:T(2,128)(2,1)}), bf16[64,2,1024]{2,1,0:T(2,128)(2,1)S(1)}, u32[]{:S(2)}, u32[]{:S(2)}) async-start(bf16[64,2,1024]{2,1,0:T(2,128)(2,1)} %reshape.287), calls=%async_computation.5 | async-start | bytes 524288 | tf_op jit(solution)/shard_map/all_to_all | solution.py:20
where the time goes:
time: 192 us; the launch traced here: 190 us
  blocking collectives  72.4 us (38%)
  waiting for transfers between devices  53.9 us (28%)
  starting transfers between devices  25.2 us (13%)
  local copies, waits for them, and re-layouts  17.3 us (9%)
  other arithmetic  12.6 us (7%)
  matrix products  7.47 us (4%)
    all_gather x1, blocking collectives, on_device(): whole_rows = lax.all_gather(tokens, ('kv', 'tp'), axis=1, tiled=True)  59.5 us
    all_to_all x2, waiting for transfers between devices, summed_on_arrival(): lax.all_to_all(cut_along(shard, dim, length), axis, 0, 0, tiled=True)  27.5 us
    all_to_all x2, waiting for transfers between devices, from_everyone(): lax.all_to_all(jnp.broadcast_to(shard[None], (length, *shard.shape)), axi...  26.4 us
    all_to_all x2, starting transfers between devices, summed_on_arrival(): lax.all_to_all(cut_along(shard, dim, length), axis, 0, 0, tiled=True)  13.1 us
    unnamed x45, local copies, waits for them, and re-layouts  12.9 us
    all_to_all x2, starting transfers between devices, from_everyone(): lax.all_to_all(jnp.broadcast_to(shard[None], (length, *shard.shape)), axi...  12.1 us
    all_to_all x1, blocking collectives, from_everyone(): lax.all_to_all(jnp.broadcast_to(shard[None], (length, *shard.shape)), axi...  6.81 us
    all_to_all x1, blocking collectives, summed_on_arrival(): lax.all_to_all(cut_along(shard, dim, length), axis, 0, 0, tiled=True)  6.01 us
  transfers between devices with their start and end apart: 4, of which 4 were waited for; matrix products, arithmetic and copies ran while one was open for 4% of the time, Pallas kernels for 0%

commit v1 on v0

v1 whole, which is shorter than its diff:
```python
import jax
import jax.numpy as jnp
from jax import lax
from jax.experimental import pallas as pl
from jax.experimental.pallas import tpu as pltpu
from jax.sharding import PartitionSpec as P

DV = 256
DQK = 128
LANES = 128
NORM_EPS = 1e-06
PITCH = 40

F32 = jnp.float32
BF16 = jnp.bfloat16

NT = (((1,), (1,)), ((), ()))

TN = (((0,), (0,)), ((), ()))


def split(wide):
    high = wide.astype(BF16)
    return high, (wide - high.astype(F32)).astype(BF16)


vmem = pl.BlockSpec(memory_space=pltpu.VMEM)
smem = pl.BlockSpec(memory_space=pltpu.SMEM)


def project_kernel(kv_pos, packed, gain, wq, wk, wv, wig, wfg, out, rows):
    n = packed.shape[1] // 2
    block = kv_pos[0] // 2
    odd = kv_pos[0] % 2
    wide = packed[...].astype(F32)
    x = jnp.concatenate([wide[:, :n].T, wide[:, n:].T], axis=1)
    twice = jnp.concatenate([x, x], axis=1)
    lane = lax.broadcasted_iota(jnp.int32, twice.shape, 1)
    mine = (lane // n) == odd
    scaled = jnp.where(mine, twice * gain[pl.ds(block, 1), :], 0.0)
    wide_lhs = scaled.astype(BF16)
    folded = scaled[:, :n] + scaled[:, n:]
    lhs = folded.astype(BF16)
    start = pl.multiple_of(block * LANES, LANES)
    ig = wig[:, pl.ds(start, LANES)]
    fg = wfg[:, pl.ds(start, LANES)]
    gates = jnp.concatenate([ig, fg, ig, fg, jnp.zeros((LANES - 4 * ig.shape[0], LANES), BF16)], axis=0)
    sums = lax.dot_general(wide_lhs, gates, NT, preferred_element_type=F32)
    squares = jnp.sum(x * x, axis=1, keepdims=True)
    sums = jnp.where(lane >= n, jnp.broadcast_to(squares, sums.shape), sums)
    low = ((lane >= n // 2) & (lane < n)) | (lane == n + 1)
    sums = jnp.where(low, sums - sums.astype(BF16).astype(F32), sums)
    for at in range(32, 40):
        rows[pl.ds(at, n, stride=PITCH), :] = sums

    def place(w, first, step):
        cols = w.shape[1]
        for c in range(0, cols, 256):
            part = jnp.dot(lhs, w[:, c : c + 256], preferred_element_type=F32)
            for half in range(2):
                tile = c // LANES + half
                at = first + (tile if step == 1 else (tile % 2) * 8 + tile // 2)
                rows[pl.ds(at, n, stride=PITCH), :] = part[:, half * LANES : (half + 1) * LANES]

    place(wq, 0, 1)
    place(wk, 8, 1)
    place(wv, 16, 2)
    for r in range(n):
        out[r] = rows[r * PITCH : r * PITCH + PITCH, :].astype(BF16)


def cell_kernel(tp_pos, arrived, memory, normalizer, stab, ibias, fbias, out, memory_out, norm_out, stab_out):
    tp = tp_pos[0]
    count = arrived.shape[0]

    def add(i, acc):
        for j in range(8):
            acc = acc + arrived[i * 8 + j].astype(F32)
        return acc

    acc = lax.fori_loop(0, count // 8, add, jnp.zeros((PITCH, LANES), F32))
    lane = lax.broadcasted_iota(jnp.int32, (8, LANES), 1)
    sub = lax.broadcasted_iota(jnp.int32, (8, LANES), 0)
    extra = jnp.broadcast_to(acc[32:33], (8, LANES))
    squares = jnp.sum(jnp.where((lane == 64) | (lane == 65), extra, 0.0), axis=1, keepdims=True)
    scale = lax.rsqrt(squares * (1.0 / 4096.0) + NORM_EPS)
    pad8 = jnp.zeros((1, LANES - 8), F32)
    pad16 = jnp.zeros((1, LANES - 32), F32)
    bias = jnp.concatenate([ibias[...], fbias[...], pad16], axis=1)
    gates = extra * scale + bias
    head = tp * 8 + sub
    igate = jnp.sum(jnp.where((lane == head) | (lane == head + 32), gates, 0.0), axis=1, keepdims=True)
    fgate = jnp.sum(jnp.where((lane == head + 16) | (lane == head + 48), gates, 0.0), axis=1, keepdims=True)
    old = jnp.sum(jnp.where(lane == sub, jnp.concatenate([stab[...], pad8], axis=1), 0.0), axis=1, keepdims=True)
    log_forget = jnp.minimum(fgate, 0.0) - jnp.log1p(jnp.exp(-jnp.abs(fgate)))
    carried = log_forget + old
    new = jnp.maximum(carried, igate)
    keep = jnp.exp(carried - new)
    fresh = jnp.exp(igate - new)
    stab_out[...] = jnp.sum(jnp.where(lane == sub, new, 0.0), axis=0, keepdims=True)[:, :8]
    q = acc[0:8] * (scale * DQK ** (-0.5))
    k = acc[8:16] * scale
    v = jnp.concatenate([acc[16:24], acc[24:32]], axis=1) * scale
    q_both = jnp.concatenate(split(q), axis=0)
    sub2 = lax.broadcasted_iota(jnp.int32, (8, DV), 0)
    recall = jnp.zeros((8, DV), F32)
    for h in range(8):
        part = lax.dot_general(q_both, memory[h].astype(BF16), NT, preferred_element_type=F32)
        recall = jnp.where(sub2 == h, part[:8] + part[8:], recall)
    match = jnp.sum(q * k, axis=1, keepdims=True)
    old_norm = normalizer[...]
    denominator = keep * jnp.sum(old_norm * q, axis=1, keepdims=True) + fresh * match
    floor = jnp.maximum(jnp.abs(denominator), jnp.exp(-new))
    cell = (keep * recall + (fresh * match) * v) / floor
    tile = jnp.concatenate([cell[:, :LANES], cell[:, LANES:]], axis=0).astype(BF16)
    for r in range(count):
        out[r] = tile
    norm_out[...] = keep * old_norm + fresh * k
    value = fresh * v
    v_high, v_low = split(value)
    k_high, k_low = split(k)
    for h in range(8):
        row = slice(h, h + 1)
        left = jnp.concatenate([v_high[row], v_high[row], v_low[row]], axis=0)
        right = jnp.concatenate([k_high[row], k_low[row], k_high[row]], axis=0)
        outer = lax.dot_general(left, right, TN, preferred_element_type=F32)
        memory_out[h] = keep[row] * memory[h] + outer


def output_kernel(arrived, w, out, rows):
    count = arrived.shape[0]
    for r in range(count):
        rows[r * 16 : r * 16 + 16, :] = arrived[r].astype(F32)
    parts = []
    for tile in range(16):
        c = (tile % 2) * 8 + tile // 2
        parts.append(rows[pl.ds(c, count, stride=16), :].astype(BF16))
    acc = lax.dot_general(w[...], jnp.concatenate(parts, axis=1), NT, preferred_element_type=F32)
    half = acc.shape[0] // 2
    out[...] = jnp.concatenate([acc[:half], acc[half:]], axis=1)


def mixer_kernel(middle, w_up, w_down, out):
    n = middle.shape[1] // 2
    x = middle[...]
    wide = x.astype(F32)
    squares = jnp.sum(wide * wide, axis=0, keepdims=True)
    squares = squares[:, :n] + squares[:, n:]
    scale = lax.rsqrt(squares * (1.0 / 4096.0) + NORM_EPS)
    both = jnp.dot(w_up[...], x, preferred_element_type=F32)
    hidden = both.shape[0] // 2
    up = (both[:hidden, :n] + both[hidden:, n:]) * scale
    act = jnp.square(jnp.maximum(up, 0.0))
    zero = jnp.zeros_like(act)
    rhs = jnp.concatenate(
        [jnp.concatenate([act, zero], axis=1), jnp.concatenate([zero, act], axis=1)], axis=0
    ).astype(BF16)
    for i in range(0, w_down.shape[0], 256):
        out[i : i + 256, :] = jnp.dot(w_down[i : i + 256, :], rhs, preferred_element_type=F32).astype(BF16)


def call(kernel, shapes, *args, scalars=0, scratch=()):
    outs = [jax.ShapeDtypeStruct(s, d) for s, d in shapes]
    many = len(outs) > 1
    return pl.pallas_call(
        kernel,
        out_shape=outs if many else outs[0],
        in_specs=[smem] * scalars + [vmem] * (len(args) - scalars),
        out_specs=[vmem] * len(outs) if many else vmem,
        scratch_shapes=list(scratch),
        compiler_params=pltpu.CompilerParams(vmem_limit_bytes=16 * 1024 * 1024),
    )(*args)


def on_device(
    tokens,
    mix_gain,
    w_query,
    w_key,
    w_value,
    w_igate,
    w_fgate,
    igate_bias,
    fgate_bias,
    memory,
    normalizer,
    stabilizer,
    w_output,
    mlp_gain,
    w_up,
    w_down,
):
    kv = lax.axis_size("kv")
    kv_index = lax.axis_index("kv")
    tp_index = lax.axis_index("tp")
    rows, thin = tokens.shape
    kv_pos = kv_index.astype(jnp.int32).reshape(1)
    tp_pos = tp_index.astype(jnp.int32).reshape(1)
    thin_t = tokens.T
    side = lax.broadcasted_iota(jnp.int32, (thin, 2 * rows), 1) // rows
    padded = jnp.where(side == tp_index, jnp.concatenate([thin_t, thin_t], axis=1), jnp.zeros((), BF16))
    packed = lax.psum(padded, "tp")

    hidden = w_up.shape[1]
    up_t = (w_up.astype(F32) * mlp_gain[:, None]).astype(BF16)
    up_t = up_t.reshape(kv, 2, thin, hidden).transpose(1, 3, 0, 2).reshape(2 * hidden, kv * thin)
    down_t = w_down.reshape(hidden, kv, 2, thin).transpose(1, 3, 2, 0).reshape(kv * thin, 2 * hidden)

    sends = call(
        project_kernel,
        [((rows, PITCH, LANES), BF16)],
        kv_pos,
        packed,
        mix_gain.reshape(-1, LANES),
        w_query,
        w_key,
        w_value,
        w_igate.T,
        w_fgate.T,
        scalars=1,
        scratch=[pltpu.VMEM((rows * PITCH, LANES), F32)],
    )
    arrived = lax.all_to_all(sends, "kv", 0, 0, tiled=True)
    arrived, up_t, down_t = lax.optimization_barrier((arrived, up_t, down_t))
    cell, new_memory, new_normalizer, new_stabilizer = call(
        cell_kernel,
        [
            ((kv, 16, LANES), BF16),
            ((8, DV, DQK), F32),
            ((8, DQK), F32),
            ((1, 8), F32),
        ],
        tp_pos,
        arrived,
        memory[0],
        normalizer[0],
        stabilizer,
        igate_bias[None],
        fgate_bias[None],
        scalars=1,
    )
    cells = lax.all_to_all(cell, "kv", 0, 0, tiled=True)

    half = call(
        output_kernel,
        [((thin, 2 * rows), F32)],
        cells,
        w_output.T,
        scratch=[pltpu.VMEM((rows * 16, LANES), F32)],
    )
    middle = (packed.astype(F32) + lax.psum(half, "tp")).astype(BF16)
    middles = lax.all_to_all(
        jnp.broadcast_to(middle[None], (kv, thin, 2 * rows)), "kv", 0, 0, tiled=True
    )
    downs = call(
        mixer_kernel,
        [((kv * thin, 2 * rows), BF16)],
        middles.reshape(kv * thin, 2 * rows),
        up_t,
        down_t,
    )
    back = lax.all_to_all(downs.reshape(kv, thin, 2 * rows), "kv", 0, 0, tiled=True)
    total = lax.psum(jnp.sum(back.astype(F32), axis=0), "tp") + middle.astype(F32)
    own = jnp.where(tp_index == 0, total[:, :rows], total[:, rows:])
    new_tokens = own.astype(BF16).T
    return (new_tokens, new_memory[None], new_normalizer[None], new_stabilizer)


def solution(mesh):
    in_specs = (
        P("dp", ("kv", "tp")),
        P(),
        P("kv", "tp"),
        P("kv", "tp"),
        P("kv", "tp"),
        P(),
        P(),
        P(),
        P(),
        P(("dp", "kv"), "tp", None, None),
        P(("dp", "kv"), "tp", None),
        P(("dp", "kv"), "tp"),
        P("tp", "kv"),
        P(),
        P(None, ("kv", "tp")),
        P(("kv", "tp"), None),
    )
    out_specs = (
        P("dp", ("kv", "tp")),
        P(("dp", "kv"), "tp", None, None),
        P(("dp", "kv"), "tp", None),
        P(("dp", "kv"), "tp"),
    )
    return jax.shard_map(
        on_device, mesh=mesh, in_specs=in_specs, out_specs=out_specs, check_vma=False
    )
```

time: 192 us -> 133 us (0.69)
  blocking collectives: 72.4 us -> 41.8 us
  other arithmetic: 12.6 us -> 2.37 us
  matrix products: 7.47 us -> 0 us
  waiting for transfers between devices: 53.9 us -> 47.1 us
  Pallas kernels: 0 us -> 5.42 us
  local copies, waits for them, and re-layouts: 17.3 us -> 13 us
  starting transfers between devices: 25.2 us -> 22 us
    all_gather x1 -> x0, blocking collectives: 59.5 us -> none  [on_device(): whole_rows = lax.all_gather(tokens, ('kv', 'tp'), axis=1, tiled=True)]
    psum x0 -> x3, blocking collectives: none -> 22.5 us  [the longest x1 8.97 us: on_device(): packed = lax.psum(padded, 'tp')]
    dot_general x8 -> x0, matrix products: 7.47 us -> none  [the longest x1 3.5 us: on_device(): lax.dot_general(reordered, activation, (((0,), (1,)), ((), ())), preferre...]
    unnamed x45 -> x33, local copies, waits for them, and re-layouts: 12.9 us -> 6.11 us
    all_to_all x4 -> x3, waiting for transfers between devices: 53.9 us -> 47.1 us  [the longest x1 16.8 us: on_device(): lax.all_to_all(downs.reshape(kv, thin, 2 * rows), 'kv', 0, 0, tiled=True)]
    all_to_all x2 -> x1, blocking collectives: 12.8 us -> 19.4 us  [on_device(): cells = lax.all_to_all(cell, 'kv', 0, 0, tiled=True)]
    pallas_call x0 -> x4, Pallas kernels: none -> 5.42 us  [call(): pl.pallas_call(kernel, out_shape=outs if many else outs[0], in_specs=[sme...]
    reduce_sum x7 -> x1, other arithmetic: 5.26 us -> 0.1 us  [on_device(): jnp.sum(back.astype(F32), axis=0)]
  transfers between devices with their start and end apart: 4 -> 3, of which waited for: 4 -> 3; matrix products, arithmetic and copies ran while one was open for 4% -> 6% of each run, Pallas kernels for 0% -> 0%
where the time goes in v1:
time: 133 us
  waiting for transfers between devices  47.1 us (35%)
  blocking collectives  41.8 us (31%)
  starting transfers between devices  22 us (17%)
  local copies, waits for them, and re-layouts  13 us (10%)
  Pallas kernels  5.42 us (4%)
  other arithmetic  2.37 us (2%)
    all_to_all x1, blocking collectives, on_device(): cells = lax.all_to_all(cell, 'kv', 0, 0, tiled=True)  19.4 us
    all_to_all x1, waiting for transfers between devices, on_device(): lax.all_to_all(downs.reshape(kv, thin, 2 * rows), 'kv', 0, 0, tiled=True)  16.8 us
    all_to_all x1, waiting for transfers between devices, on_device(): lax.all_to_all(jnp.broadcast_to(middle[None], (kv, thin, 2 * rows)), 'kv'...  16.5 us
    all_to_all x1, waiting for transfers between devices, on_device(): arrived = lax.all_to_all(sends, 'kv', 0, 0, tiled=True)  13.8 us
    all_to_all x1, starting transfers between devices, on_device(): arrived = lax.all_to_all(sends, 'kv', 0, 0, tiled=True)  11 us
    psum x1, blocking collectives, on_device(): packed = lax.psum(padded, 'tp')  8.97 us
    psum x1, blocking collectives, on_device(): lax.psum(jnp.sum(back.astype(F32), axis=0), 'tp') + middle.astype(F32)  7.04 us
    psum x1, blocking collectives, on_device(): middle = (packed.astype(F32) + lax.psum(half, 'tp')).astype(BF16)  6.47 us
  transfers between devices with their start and end apart: 3, of which 3 were waited for; matrix products, arithmetic and copies ran while one was open for 6% of the time, Pallas kernels for 0%

profile of v1, /device:TPU:1, one launch (start us, length us, event | category | flops | bytes accessed | tf_op | source)
XLA Modules:
  0.0 132.6 jit_solution(16699266617694609410)
XLA Ops:
  0.7 0.9 fusion.1
  1.5 9.0 %psum.21.packed = bf16[32,128]{1,0:T(8,128)(2,1)S(1)} all-reduce(bf16[32,128]{1,0:T(8,128)(2,1)S(1)} %fusion.1), channel_id=1, replica_groups=mesh['dp'=4,'kv'=64,'tp'=2] {'tp'}, use_global_device_ids=true, to_apply=%region_0.1 | all-reduce | flops 4096 | bytes 16384 | tf_op jit(solution)/shard_map/psum | solution.py:202
  10.5 0.9 copy-done.2
  11.4 0.9 copy-done.3
  12.3 0.9 copy-done.4
  13.3 0.9 copy-done.5
  14.2 0.9 copy-done.6
  15.8 1.6 %shard_map.183 = bf16[64,40,128]{2,1,0:T(8,128)(2,1)} custom-call(s32[1]{0:T(128)} %bitcast.2.kv_pos, bf16[32,128]{1,0:T(8,128)(2,1)S(1)} %psum.21.packed, f32[32,128]{1,0:T(8,128)S(1)} %bitcast.37, bf16[64,1024]{1,0:T(8,128)(2,1)S(1)} %copy-done.3, bf16[64,1024]{1,0:T(8,128)(2,1)S(1)} %copy-done.4, bf16[64,2048]{1,0:T(8,128)(2,1)S(1)} %copy-done.2, ...), custom_call_target="tpu_custom_call" | custom-call | tf_op jit(solution)/shard_map/pallas_call | solution.py:165
  17.4 11.0 %all-to-all-start = ((bf16[64,40,128]{2,1,0:T(8,128)(2,1)}), bf16[64,40,128]{2,1,0:T(8,128)(2,1)S(1)}, u32[]{:S(2)}, u32[]{:S(2)}) async-start(bf16[64,40,128]{2,1,0:T(8,128)(2,1)} %shard_map.183), calls=%async_computation | async-start | bytes 1310720 | tf_op jit(solution)/shard_map/all_to_all | solution.py:223
  29.1 2.1 %copy.22 = bf16[64,2,32,128]{3,1,2,0:T(2,128)(2,1)} copy(bf16[64,2,32,128]{3,2,1,0:T(8,128)(2,1)S(1)} %bitcast.41) | data formatting | bytes 2097152 | tf_op jit(solution)/shard_map/reshape | solution.py:206
  31.9 1.1 copy.24
  33.1 1.4 %copy_bitcast_fusion = (bf16[2048,256]{1,0:T(8,128)(2,1)S(1)}, bf16[256,2048]{0,1:T(8,128)(2,1)}) fusion(bf16[256,8,2,128]{3,2,1,0:T(2,128)(2,1)S(1)} %bitcast.44, bf16[256,8,2,128]{3,2,1,0:T(2,128)(2,1)S(1)} %bitcast.43), kind=kLoop, calls=%fused_computation.1 | loop fusion | bytes 4194304 | tf_op jit(solution)/shard_map/reshape | solution.py:207
  34.5 13.8 %all-to-all-done.arrived = bf16[64,40,128]{2,1,0:T(8,128)(2,1)S(1)} async-done(((bf16[64,40,128]{2,1,0:T(8,128)(2,1)}), bf16[64,40,128]{2,1,0:T(8,128)(2,1)S(1)}, u32[]{:S(2)}, u32[]{:S(2)}) %all-to-all-start) | async-done | bytes 655392 | tf_op jit(solution)/shard_map/all_to_all | solution.py:223
  48.4 1.6 %shard_map.184 = (bf16[64,16,128]{2,1,0:T(8,128)(2,1)S(1)}, f32[8,256,128]{2,1,0:T(8,128)}, f32[8,128]{1,0:T(8,128)}, f32[1,8]{1,0:T(1,128)}) custom-call(s32[1]{0:T(128)} %bitcast.1.tp_pos, bf16[64,40,128]{2,1,0:T(8,128)(2,1)S(1)} %all-to-all-done.arrived, f32[8,256,128]{2,1,0:T(8,128)S(1)} %bitcast.33, f32[8,128]{1,0:T(8,128)S(1)} %bitcast.38, ...), custom_call_target="tpu_custom_call" | custom-call | tf_op jit(solution)/shard_map/pallas_call | solution.py:165
  50.0 19.4 %all_to_all.20.arrived = bf16[64,16,128]{2,1,0:T(8,128)(2,1)S(1)} all-to-all(bf16[64,16,128]{2,1,0:T(8,128)(2,1)S(1)} %get-tuple-element.12), channel_id=1, replica_groups=mesh['dp'=4,'kv'=64,'tp'=2] {'kv'}, dimensions={0} | all-to-all | bytes 524288 | tf_op jit(solution)/shard_map/all_to_all | solution.py:242
  69.7 6.5 %psum.22 = f32[32,128]{1,0:T(8,128)S(1)} all-reduce(f32[32,128]{1,0:T(8,128)S(1)} %shard_map.185), channel_id=1, replica_groups=mesh['dp'=4,'kv'=64,'tp'=2] {'tp'}, use_global_device_ids=true, to_apply=%region_1.2 | all-reduce | flops 4096 | bytes 32768 | tf_op jit(solution)/shard_map/psum | solution.py:251
  76.2 0.9 broadcast_in_dim.26
  77.1 4.6 %all-to-all-start.2 = ((bf16[64,32,128]{2,1,0:T(8,128)(2,1)}), bf16[64,32,128]{2,1,0:T(8,128)(2,1)S(1)}, u32[]{:S(2)}, u32[]{:S(2)}) async-start(bf16[64,32,128]{2,1,0:T(8,128)(2,1)} %broadcast_in_dim.26), calls=%async_computation.2 | async-start | bytes 1048576 | tf_op jit(solution)/shard_map/all_to_all | solution.py:252
  81.7 1.5 %copy.25.w_up = bf16[256,2048]{1,0:T(8,128)(2,1)S(1)} copy(bf16[256,2048]{0,1:T(8,128)(2,1)} %get-tuple-element.13) | data formatting | bytes 2097152 | tf_op jit(solution)/shard_map/optimization_barrier | solution.py:224
  83.2 16.5 %all-to-all-done.2 = bf16[64,32,128]{2,1,0:T(8,128)(2,1)S(1)} async-done(((bf16[64,32,128]{2,1,0:T(8,128)(2,1)}), bf16[64,32,128]{2,1,0:T(8,128)(2,1)S(1)}, u32[]{:S(2)}, u32[]{:S(2)}) %all-to-all-start.2) | async-done | bytes 524320 | tf_op jit(solution)/shard_map/all_to_all | solution.py:252
  99.8 1.8 %shard_map.186 = bf16[2048,128]{1,0:T(8,128)(2,1)} custom-call(bf16[2048,128]{1,0:T(8,128)(2,1)S(1)} %bitcast.32, bf16[256,2048]{1,0:T(8,128)(2,1)S(1)} %copy.25.w_up, bf16[2048,256]{1,0:T(8,128)(2,1)S(1)} %get-tuple-element.14.w_down), custom_call_target="tpu_custom_call" | custom-call | tf_op jit(solution)/shard_map/pallas_call | solution.py:165
  101.5 6.4 %all-to-all-start.3 = ((bf16[64,32,128]{2,1,0:T(8,128)(2,1)}), bf16[64,32,128]{2,1,0:T(8,128)(2,1)S(1)}, u32[]{:S(2)}, u32[]{:S(2)}) async-start(bf16[64,32,128]{2,1,0:T(8,128)(2,1)} %bitcast.16), calls=%async_computation.3 | async-start | bytes 1048576 | tf_op jit(solution)/shard_map/all_to_all | solution.py:262
  108.0 16.8 %all-to-all-done.3 = bf16[64,32,128]{2,1,0:T(8,128)(2,1)S(1)} async-done(((bf16[64,32,128]{2,1,0:T(8,128)(2,1)}), bf16[64,32,128]{2,1,0:T(8,128)(2,1)S(1)}, u32[]{:S(2)}, u32[]{:S(2)}) %all-to-all-start.3) | async-done | bytes 524320 | tf_op jit(solution)/shard_map/all_to_all | solution.py:262
  124.8 7.0 %psum.23 = f32[32,128]{1,0:T(8,128)S(1)} all-reduce(f32[32,128]{1,0:T(8,128)S(1)} %convert_reduce_fusion), channel_id=1, replica_groups=mesh['dp'=4,'kv'=64,'tp'=2] {'tp'}, use_global_device_ids=true, to_apply=%region_3.4 | all-reduce | flops 4096 | bytes 32768 | tf_op jit(solution)/shard_map/psum | solution.py:263
  (36 shorter events, 3.5 us)
Async XLA Ops:
  10.5 0.9 copy-start.2
  11.4 0.9 copy-start.3
  12.3 0.9 copy-start.4
  13.3 0.9 copy-start.5
  14.2 0.9 copy-start.6
  15.1 0.7 copy-start.7
  15.8 12.6 %copy-start.13 = (bf16[4096,128]{1,0:T(8,128)(2,1)S(1)}, bf16[4096,128]{1,0:T(8,128)(2,1)}, u32[]{:S(2)}) copy-start(bf16[4096,128]{1,0:T(8,128)(2,1)} %param.30) | copy-start | bytes 3145732
  15.8 12.6 %copy-start.15 = (f32[4096]{0:T(1024)S(1)}, f32[4096]{0:T(1024)}, u32[]{:S(2)}) copy-start(f32[4096]{0:T(1024)} %param.29) | copy-start | bytes 49156
  17.4 30.9 %all-to-all-start = ((bf16[64,40,128]{2,1,0:T(8,128)(2,1)}), bf16[64,40,128]{2,1,0:T(8,128)(2,1)S(1)}, u32[]{:S(2)}, u32[]{:S(2)}) async-start(bf16[64,40,128]{2,1,0:T(8,128)(2,1)} %shard_map.183), calls=%async_computation | async-start | bytes 1310720 | tf_op jit(solution)/shard_map/all_to_all | solution.py:223
  29.1 2.1 %copy-start.14 = (bf16[128,4096]{1,0:T(8,128)(2,1)S(1)}, bf16[128,4096]{1,0:T(8,128)(2,1)}, u32[]{:S(2)}) copy-start(bf16[128,4096]{1,0:T(8,128)(2,1)} %param.31) | copy-start | bytes 3145732
  31.9 1.2 copy-start.12
  33.1 15.2 %copy-start = (f32[1,8,256,128]{3,2,1,0:T(8,128)S(1)}, f32[1,8,256,128]{3,2,1,0:T(8,128)}, u32[]{:S(2)}) copy-start(f32[1,8,256,128]{3,2,1,0:T(8,128)} %param.25) | copy-start | bytes 3145732
  33.1 15.2 %copy-start.8 = (f32[1,8,128]{2,1,0:T(8,128)S(1)}, f32[1,8,128]{2,1,0:T(8,128)}, u32[]{:S(2)}) copy-start(f32[1,8,128]{2,1,0:T(8,128)} %param.26) | copy-start | bytes 12292
  33.1 15.2 %copy-start.9 = (f32[1,8]{1,0:T(1,128)S(1)}, f32[1,8]{1,0:T(1,128)}, u32[]{:S(2)}) copy-start(f32[1,8]{1,0:T(1,128)} %stab.1) | copy-start | bytes 100
  33.1 15.2 %copy-start.10 = (f32[16]{0:T(128)S(1)}, f32[16]{0:T(128)}, u32[]{:S(2)}) copy-start(f32[16]{0:T(128)} %param.23) | copy-start | bytes 196
  33.1 15.2 %copy-start.11 = (f32[16]{0:T(128)S(1)}, f32[16]{0:T(128)}, u32[]{:S(2)}) copy-start(f32[16]{0:T(128)} %param.24) | copy-start | bytes 196
  48.3 21.0 %copy-start.1 = (bf16[2048,64]{0,1:T(8,128)(2,1)S(1)}, bf16[2048,64]{0,1:T(8,128)(2,1)}, u32[]{:S(2)}) copy-start(bf16[2048,64]{0,1:T(8,128)(2,1)} %param.28) | copy-start | bytes 786436
  77.1 22.7 %all-to-all-start.2 = ((bf16[64,32,128]{2,1,0:T(8,128)(2,1)}), bf16[64,32,128]{2,1,0:T(8,128)(2,1)S(1)}, u32[]{:S(2)}, u32[]{:S(2)}) async-start(bf16[64,32,128]{2,1,0:T(8,128)(2,1)} %broadcast_in_dim.26), calls=%async_computation.2 | async-start | bytes 1048576 | tf_op jit(solution)/shard_map/all_to_all | solution.py:252
  101.5 23.2 %all-to-all-start.3 = ((bf16[64,32,128]{2,1,0:T(8,128)(2,1)}), bf16[64,32,128]{2,1,0:T(8,128)(2,1)S(1)}, u32[]{:S(2)}, u32[]{:S(2)}) async-start(bf16[64,32,128]{2,1,0:T(8,128)(2,1)} %bitcast.16), calls=%async_computation.3 | async-start | bytes 1048576 | tf_op jit(solution)/shard_map/all_to_all | solution.py:262

commit v2 on v1

--- a/solution.py
+++ b/solution.py
@@ -26,6 +26,25 @@
 
 vmem = pl.BlockSpec(memory_space=pltpu.VMEM)
 smem = pl.BlockSpec(memory_space=pltpu.SMEM)
+
+
+any_space = pl.BlockSpec(memory_space=pl.ANY)
+
+
+def fetch_kernel(kv_pos, tp_pos, tokens, gain, wq, wk, wv, wig, wfg, padded, *rest):
+    outs, sems = rest[:-1], rest[-1]
+    own, outs = outs[-1], outs[:-1]
+    start = pl.multiple_of(kv_pos[0] // 2 * LANES, LANES)
+    sources = (tokens, gain, wq, wk, wv, wig.at[:, pl.ds(start, LANES)], wfg.at[:, pl.ds(start, LANES)])
+    copies = [pltpu.make_async_copy(src, dst, sems.at[i]) for i, (src, dst) in enumerate(zip(sources, (own, *outs)))]
+    for copy in copies:
+        copy.start()
+    copies[0].wait()
+    x = own[...].astype(F32)
+    twice = jnp.concatenate([x, x], axis=1)
+    padded[...] = jnp.where(halves_of(twice) == tp_pos[0], twice, 0.0).astype(BF16)
+    for copy in copies[1:]:
+        copy.wait()
 
 
 def project_kernel(kv_pos, packed, gain, wq, wk, wv, wig, wfg, out, rows):
@@ -41,9 +60,8 @@
     wide_lhs = scaled.astype(BF16)
     folded = scaled[:, :n] + scaled[:, n:]
     lhs = folded.astype(BF16)
-    start = pl.multiple_of(block * LANES, LANES)
-    ig = wig[:, pl.ds(start, LANES)]
-    fg = wfg[:, pl.ds(start, LANES)]
+    ig = wig[...]
+    fg = wfg[...]
     gates = jnp.concatenate([ig, fg, ig, fg, jnp.zeros((LANES - 4 * ig.shape[0], LANES), BF16)], axis=0)
     sums = lax.dot_general(wide_lhs, gates, NT, preferred_element_type=F32)
     squares = jnp.sum(x * x, axis=1, keepdims=True)
@@ -69,8 +87,13 @@
         out[r] = rows[r * PITCH : r * PITCH + PITCH, :].astype(BF16)
 
 
-def cell_kernel(tp_pos, arrived, memory, normalizer, stab, ibias, fbias, out, memory_out, norm_out, stab_out):
+def cell_kernel(tp_pos, arrived, normalizer, small, memory_in, out, norm_out, stab_out, memory_out, memory, sems):
     tp = tp_pos[0]
+    heads = memory.shape[0]
+    loads = [pltpu.make_async_copy(memory_in.at[h], memory.at[h], sems.at[h]) for h in range(heads)]
+    stores = [pltpu.make_async_copy(memory.at[h], memory_out.at[h], sems.at[heads + h]) for h in range(heads)]
+    for load in loads:
+        load.start()
     count = arrived.shape[0]
 
     def add(i, acc):
@@ -84,14 +107,11 @@
     extra = jnp.broadcast_to(acc[32:33], (8, LANES))
     squares = jnp.sum(jnp.where((lane == 64) | (lane == 65), extra, 0.0), axis=1, keepdims=True)
     scale = lax.rsqrt(squares * (1.0 / 4096.0) + NORM_EPS)
-    pad8 = jnp.zeros((1, LANES - 8), F32)
-    pad16 = jnp.zeros((1, LANES - 32), F32)
-    bias = jnp.concatenate([ibias[...], fbias[...], pad16], axis=1)
-    gates = extra * scale + bias
+    gates = extra * scale + small[0:1, :]
     head = tp * 8 + sub
     igate = jnp.sum(jnp.where((lane == head) | (lane == head + 32), gates, 0.0), axis=1, keepdims=True)
     fgate = jnp.sum(jnp.where((lane == head + 16) | (lane == head + 48), gates, 0.0), axis=1, keepdims=True)
-    old = jnp.sum(jnp.where(lane == sub, jnp.concatenate([stab[...], pad8], axis=1), 0.0), axis=1, keepdims=True)
+    old = jnp.sum(jnp.where(lane == sub, small[1:2, :], 0.0), axis=1, keepdims=True)
     log_forget = jnp.minimum(fgate, 0.0) - jnp.log1p(jnp.exp(-jnp.abs(fgate)))
     carried = log_forget + old
     new = jnp.maximum(carried, igate)
@@ -104,7 +124,8 @@
     q_both = jnp.concatenate(split(q), axis=0)
     sub2 = lax.broadcasted_iota(jnp.int32, (8, DV), 0)
     recall = jnp.zeros((8, DV), F32)
-    for h in range(8):
+    for h in range(heads):
+        loads[h].wait()
         part = lax.dot_general(q_both, memory[h].astype(BF16), NT, preferred_element_type=F32)
         recall = jnp.where(sub2 == h, part[:8] + part[8:], recall)
     match = jnp.sum(q * k, axis=1, keepdims=True)
@@ -119,12 +140,15 @@
     value = fresh * v
     v_high, v_low = split(value)
     k_high, k_low = split(k)
-    for h in range(8):
+    for h in range(heads):
         row = slice(h, h + 1)
         left = jnp.concatenate([v_high[row], v_high[row], v_low[row]], axis=0)
         right = jnp.concatenate([k_high[row], k_low[row], k_high[row]], axis=0)
         outer = lax.dot_general(left, right, TN, preferred_element_type=F32)
-        memory_out[h] = keep[row] * memory[h] + outer
+        memory[h] = keep[row] * memory[h] + outer
+        stores[h].start()
+    for store in stores:
+        store.wait()
 
 
 def output_kernel(arrived, w, out, rows):
@@ -140,33 +164,118 @@
     out[...] = jnp.concatenate([acc[:half], acc[half:]], axis=1)
 
 
-def mixer_kernel(middle, w_up, w_down, out):
-    n = middle.shape[1] // 2
-    x = middle[...]
-    wide = x.astype(F32)
+def prepare_kernel(tp_pos, w_up, gain, w_down, stab, ibias, fbias, normalizer, w_out, keep, send, small, *rest):
+    outs, turned, sems = rest[:-2], rest[-2], rest[-1]
+    copies = [
+        pltpu.make_async_copy(src, dst, sems.at[i])
+        for i, (src, dst) in enumerate(zip((normalizer, w_out), outs))
+    ]
+    for copy in copies:
+        copy.start()
+    small[...] = jnp.zeros(small.shape, F32)
+    small[0:1, 0:16] = ibias[...]
+    small[0:1, 16:32] = fbias[...]
+    small[1:2, 0:8] = stab[...]
+    tp = tp_pos[0]
+    chips = w_up.shape[0]
+    for k in range(0, chips, 2):
+        turned[k : k + 2] = w_down[:, k * 64 : k * 64 + 128].T.reshape(2, 2, 2, 16, 128)
+    for side in range(2):
+        dst = (keep, send)[side]
+        half = (tp + side) % 2
+        for quarter in range(2):
+            lanes = slice(quarter * 128, quarter * 128 + 128)
+            factors = gain[pl.ds(half * 2 + quarter, 1), :]
+            for block in range(4):
+                part = w_up[block * 16 : block * 16 + 16, half, quarter].reshape(256, 128).T
+                part = part.astype(F32) * factors[:, block * 256 : block * 256 + 256]
+                dst[block * 256 + quarter * 128 : block * 256 + quarter * 128 + 128, :] = part.astype(BF16)
+            dst[1024:2048, lanes] = turned[:, half, quarter].reshape(1024, 128)
+    for copy in copies:
+        copy.wait()
+
+
+def middle_kernel(tp_pos, half_sum, packed, out, own):
+    tp = tp_pos[0]
+    whole = packed[...].astype(F32) + half_sum[...]
+    n = whole.shape[1] // 2
+    mine = jnp.where(tp == 0, whole[:, :n], whole[:, n:])
+    thin = mine.shape[0] // 2
+    tile = jnp.concatenate([mine[:thin], mine[thin:]], axis=1).astype(BF16)
+    own[...] = tile
+    for r in range(out.shape[0]):
+        out[r] = tile
+
+
+def halves_of(like):
+    return (lax.broadcasted_iota(jnp.int32, like.shape, 1) >= like.shape[1] // 2).astype(jnp.int32)
+
+
+def swapped(wide):
+    n = wide.shape[1] // 2
+    return jnp.concatenate([wide[:, n:], wide[:, :n]], axis=1)
+
+
+def up_kernel(tp_pos, middle, keep, other, out):
+    tp = tp_pos[0]
+    wide = middle[...].astype(F32)
     squares = jnp.sum(wide * wide, axis=0, keepdims=True)
-    squares = squares[:, :n] + squares[:, n:]
-    scale = lax.rsqrt(squares * (1.0 / 4096.0) + NORM_EPS)
-    both = jnp.dot(w_up[...], x, preferred_element_type=F32)
-    hidden = both.shape[0] // 2
-    up = (both[:hidden, :n] + both[hidden:, n:]) * scale
-    act = jnp.square(jnp.maximum(up, 0.0))
-    zero = jnp.zeros_like(act)
-    rhs = jnp.concatenate(
-        [jnp.concatenate([act, zero], axis=1), jnp.concatenate([zero, act], axis=1)], axis=0
-    ).astype(BF16)
-    for i in range(0, w_down.shape[0], 256):
-        out[i : i + 256, :] = jnp.dot(w_down[i : i + 256, :], rhs, preferred_element_type=F32).astype(BF16)
-
-
-def call(kernel, shapes, *args, scalars=0, scratch=()):
-    outs = [jax.ShapeDtypeStruct(s, d) for s, d in shapes]
+
+    def product(w):
+        acc = jnp.zeros((256, 128), F32)
+        for block in range(4):
+            rows = slice(block * 256, block * 256 + 256)
+            acc = acc + jnp.dot(w[rows, :], middle[rows, :], preferred_element_type=F32)
+        low = acc[:128] + swapped(acc[128:])
+        return jnp.where(halves_of(low) == 0, low, swapped(low))
+
+    own = product(keep)
+    out[:128] = jnp.where(halves_of(own) == tp, own, product(other))
+    out[128:] = jnp.broadcast_to(squares + swapped(squares), (8, 128))
+
+
+def down_kernel(tp_pos, near, far_sums, keep, other, out):
+    tp = tp_pos[0]
+    sums = near[...] + far_sums[...]
+    scale = lax.rsqrt(sums[128:129] * (1.0 / 4096.0) + NORM_EPS)
+    act = jnp.square(jnp.maximum(sums[:128] * scale, 0.0))
+    swap = swapped(act)
+    side = halves_of(act)
+
+    def spread(rows):
+        return jnp.concatenate([jnp.where(side == 0, rows, 0.0), jnp.where(side == 1, rows, 0.0)], axis=0).astype(BF16)
+
+    own = spread(jnp.where(side == tp, act, swap))
+    far = spread(jnp.where(side == tp, swap, act))
+    for i in range(0, 1024, 256):
+        rows = slice(1024 + i, 1280 + i)
+        part = jnp.dot(keep[rows, :], own, preferred_element_type=F32)
+        part = part + jnp.dot(other[rows, :], far, preferred_element_type=F32)
+        out[i : i + 256, :] = part.astype(BF16)
+
+
+def finish_kernel(back, own, out):
+    def add(i, acc):
+        for j in range(8):
+            acc = acc + back[i * 8 + j].astype(F32)
+        return acc
+
+    acc = lax.fori_loop(0, back.shape[0] // 8, add, own[...].astype(F32))
+    n = acc.shape[1] // 2
+    out[...] = jnp.concatenate([acc[:, :n], acc[:, n:]], axis=0).astype(BF16)
+
+
+def call(kernel, shapes, *args, scalars=0, far=0, fetched=0, away=(), scratch=()):
+    outs = [jax.ShapeDtypeStruct(s, d) if i in away else pltpu.VMEM(s, d) for i, (s, d) in enumerate(shapes)]
+    out_specs = [vmem] * (len(outs) - fetched) + [any_space] * fetched
     many = len(outs) > 1
+    near = len(args) - far
+    args = args[:near] + tuple(pltpu.with_memory_space_constraint(x, pltpu.HBM) for x in args[near:])
     return pl.pallas_call(
         kernel,
         out_shape=outs if many else outs[0],
-        in_specs=[smem] * scalars + [vmem] * (len(args) - scalars),
-        out_specs=[vmem] * len(outs) if many else vmem,
+        in_specs=[smem] * scalars + [vmem] * (near - scalars) + [any_space] * far,
+        out_specs=out_specs if many else out_specs[0],
         scratch_shapes=list(scratch),
         compiler_params=pltpu.CompilerParams(vmem_limit_bytes=16 * 1024 * 1024),
     )(*args)
@@ -196,48 +305,96 @@
     rows, thin = tokens.shape
     kv_pos = kv_index.astype(jnp.int32).reshape(1)
     tp_pos = tp_index.astype(jnp.int32).reshape(1)
-    thin_t = tokens.T
-    side = lax.broadcasted_iota(jnp.int32, (thin, 2 * rows), 1) // rows
-    padded = jnp.where(side == tp_index, jnp.concatenate([thin_t, thin_t], axis=1), jnp.zeros((), BF16))
-    packed = lax.psum(padded, "tp")
-
-    hidden = w_up.shape[1]
-    up_t = (w_up.astype(F32) * mlp_gain[:, None]).astype(BF16)
-    up_t = up_t.reshape(kv, 2, thin, hidden).transpose(1, 3, 0, 2).reshape(2 * hidden, kv * thin)
-    down_t = w_down.reshape(hidden, kv, 2, thin).transpose(1, 3, 2, 0).reshape(kv * thin, 2 * hidden)
-
-    sends = call(
-        project_kernel,
-        [((rows, PITCH, LANES), BF16)],
+    padded, gain_near, wq, wk, wv, ig, fg = call(
+        fetch_kernel,
+        [
+            ((thin, 2 * rows), BF16),
+            ((mix_gain.shape[0] // LANES, LANES), F32),
+            (w_query.shape, BF16),
+            (w_key.shape, BF16),
+            (w_value.shape, BF16),
+            ((w_igate.shape[1], LANES), BF16),
+            ((w_fgate.shape[1], LANES), BF16),
+        ],
         kv_pos,
-        packed,
+        tp_pos,
+        tokens.T,
         mix_gain.reshape(-1, LANES),
         w_query,
         w_key,
         w_value,
         w_igate.T,
         w_fgate.T,
+        scalars=2,
+        far=7,
+        fetched=6,
+        scratch=[pltpu.VMEM((thin, rows), BF16), pltpu.SemaphoreType.DMA((7,))],
+    )
+    packed = lax.psum(padded, "tp")
+
+    hidden = w_up.shape[1]
+    quarter = thin // 2
+    gains = mlp_gain.reshape(kv, 2, 2, quarter).transpose(1, 2, 0, 3).reshape(4, kv * quarter)
+    keep, send, small, state_norm, w_out = call(
+        prepare_kernel,
+        [
+            ((2048, 256), BF16),
+            ((2048, 256), BF16),
+            ((8, LANES), F32),
+            (normalizer.shape[1:], F32),
+            (w_output.shape[::-1], BF16),
+        ],
+        tp_pos,
+        w_up.reshape(kv, 2, 2, quarter, hidden),
+        gains,
+        w_down,
+        stabilizer,
+        igate_bias[None],
+        fgate_bias[None],
+        normalizer[0],
+        w_output.T,
         scalars=1,
+        far=2,
+        fetched=2,
+        scratch=[pltpu.VMEM((kv, 2, 2, quarter, hidden), BF16), pltpu.SemaphoreType.DMA((2,))],
+    )
+    other = lax.ppermute(send, "tp", [(0, 1), (1, 0)])
+
+    sends = call(
+        project_kernel,
+        [((rows, PITCH, LANES), BF16)],
+        kv_pos,
+        packed,
+        gain_near,
+        wq,
+        wk,
+        wv,
+        ig,
+        fg,
+        scalars=1,
+        away=(0,),
         scratch=[pltpu.VMEM((rows * PITCH, LANES), F32)],
     )
     arrived = lax.all_to_all(sends, "kv", 0, 0, tiled=True)
-    arrived, up_t, down_t = lax.optimization_barrier((arrived, up_t, down_t))
-    cell, new_memory, new_normalizer, new_stabilizer = call(
+    arrived, keep, other = lax.optimization_barrier((arrived, keep, other))
+    cell, new_normalizer, new_stabilizer, new_memory = call(
         cell_kernel,
         [
             ((kv, 16, LANES), BF16),
-            ((8, DV, DQK), F32),
             ((8, DQK), F32),
             ((1, 8), F32),
+            (memory.shape[1:], F32),
         ],
         tp_pos,
         arrived,
+        state_norm,
+        small,
         memory[0],
-        normalizer[0],
-        stabilizer,
-        igate_bias[None],
-        fgate_bias[None],
         scalars=1,
+        far=1,
+        fetched=1,
+        away=(1, 2, 3),
+        scratch=[pltpu.VMEM(memory.shape[1:], F32), pltpu.SemaphoreType.DMA((16,))],
     )
     cells = lax.all_to_all(cell, "kv", 0, 0, tiled=True)
 
@@ -245,24 +402,31 @@
         output_kernel,
         [((thin, 2 * rows), F32)],
         cells,
-        w_output.T,
+        w_out,
         scratch=[pltpu.VMEM((rows * 16, LANES), F32)],
     )
-    middle = (packed.astype(F32) + lax.psum(half, "tp")).astype(BF16)
-    middles = lax.all_to_all(
-        jnp.broadcast_to(middle[None], (kv, thin, 2 * rows)), "kv", 0, 0, tiled=True
-    )
+    middle, own = call(
+        middle_kernel,
+        [((kv, quarter, 2 * rows), BF16), ((quarter, 2 * rows), BF16)],
+        tp_pos,
+        lax.psum(half, "tp"),
+        packed,
+        scalars=1,
+    )
+    middles = lax.all_to_all(middle, "kv", 0, 0, tiled=True).reshape(kv * quarter, 2 * rows)
+    sums = call(up_kernel, [((136, 128), F32)], tp_pos, middles, keep, other, scalars=1)
     downs = call(
-        mixer_kernel,
-        [((kv * thin, 2 * rows), BF16)],
-        middles.reshape(kv * thin, 2 * rows),
-        up_t,
-        down_t,
-    )
-    back = lax.all_to_all(downs.reshape(kv, thin, 2 * rows), "kv", 0, 0, tiled=True)
-    total = lax.psum(jnp.sum(back.astype(F32), axis=0), "tp") + middle.astype(F32)
-    own = jnp.where(tp_index == 0, total[:, :rows], total[:, rows:])
-    new_tokens = own.astype(BF16).T
+        down_kernel,
+        [((kv * quarter, 2 * rows), BF16)],
+        tp_pos,
+        sums,
+        lax.ppermute(sums, "tp", [(0, 1), (1, 0)]),
+        keep,
+        other,
+        scalars=1,
+    )
+    back = lax.all_to_all(downs.reshape(kv, quarter, 2 * rows), "kv", 0, 0, tiled=True)
+    new_tokens = call(finish_kernel, [((thin, rows), BF16)], back, own, away=(0,)).T
     return (new_tokens, new_memory[None], new_normalizer[None], new_stabilizer)
 
 

time: 133 us -> 117 us (0.88)
  waiting for transfers between devices: 47.1 us -> 14.3 us
  blocking collectives: 41.8 us -> 69.4 us
  local copies, waits for them, and re-layouts: 13 us -> 2.23 us
  Pallas kernels: 5.42 us -> 10.8 us
  starting transfers between devices: 22 us -> 17.9 us
  other arithmetic: 2.37 us -> 0 us
    all_to_all x0 -> x2, blocking collectives: none -> 34.5 us  [the longest x1 17.3 us: on_device(): lax.all_to_all(middle, 'kv', 0, 0, tiled=True)]
    all_to_all x2 -> x0, waiting for transfers between devices: 33.3 us -> none  [the longest x1 16.8 us: on_device(): lax.all_to_all(downs.reshape(kv, thin, 2 * rows), 'kv', 0, 0, tiled=True)]
    all_to_all x2 -> x0, starting transfers between devices: 11 us -> none  [the longest x1 6.41 us: on_device(): lax.all_to_all(downs.reshape(kv, thin, 2 * rows), 'kv', 0, 0, tiled=True)]
    psum x2 -> x1, blocking collectives: 13.5 us -> 6.46 us  [on_device(): lax.psum(half, 'tp')]
    ppermute x0 -> x2, starting transfers between devices: none -> 6.79 us  [the longest x1 4.28 us: on_device(): lax.ppermute(sums, 'tp', [(0, 1), (1, 0)])]
    pallas_call x4 -> x9, Pallas kernels: 5.42 us -> 10.8 us  [call(): pl.pallas_call(kernel, out_shape=outs if many else outs[0], in_specs=[sme...]
    unnamed x33 -> x12, local copies, waits for them, and re-layouts: 6.11 us -> 1.88 us
    ppermute x0 -> x2, waiting for transfers between devices: none -> 3.15 us  [the longest x1 2.26 us: on_device(): other = lax.ppermute(send, 'tp', [(0, 1), (1, 0)])]
  transfers between devices with their start and end apart: 3 -> 3, of which waited for: 3 -> 3; matrix products, arithmetic and copies ran while one was open for 6% -> 0% of each run, Pallas kernels for 0% -> 1%
where the time goes in v2:
time: 117 us; the launch traced here: 115 us
  blocking collectives  69.4 us (59%)
  starting transfers between devices  17.9 us (15%)
  waiting for transfers between devices  14.3 us (12%)
  Pallas kernels  10.8 us (9%)
  local copies, waits for them, and re-layouts  2.23 us (2%)
    all_to_all x1, blocking collectives, on_device(): cells = lax.all_to_all(cell, 'kv', 0, 0, tiled=True)  19.4 us
    all_to_all x1, blocking collectives, on_device(): lax.all_to_all(middle, 'kv', 0, 0, tiled=True)  17.3 us
    all_to_all x1, blocking collectives, on_device(): lax.all_to_all(downs.reshape(kv, quarter, 2 * rows), 'kv', 0, 0, tiled=True)  17.2 us
    all_to_all x1, waiting for transfers between devices, on_device(): arrived = lax.all_to_all(sends, 'kv', 0, 0, tiled=True)  11.1 us
    all_to_all x1, starting transfers between devices, on_device(): arrived = lax.all_to_all(sends, 'kv', 0, 0, tiled=True)  11.1 us
    pallas_call x9, Pallas kernels, call(): pl.pallas_call(kernel, out_shape=outs if many else outs[0], in_specs=[sme...  10.8 us
    psum x1, blocking collectives, on_device(): packed = lax.psum(padded, 'tp')  9 us
    psum x1, blocking collectives, on_device(): lax.psum(half, 'tp')  6.46 us
  transfers between devices with their start and end apart: 3, of which 3 were waited for; matrix products, arithmetic and copies ran while one was open for 0% of the time, Pallas kernels for 1%

profile of v2, /device:TPU:1, one launch (start us, length us, event | category | flops | bytes accessed | tf_op | source)
XLA Modules:
  0.0 115.3 jit_solution(10083753320000563990)
XLA Ops:
  0.6 1.2 %shard_map.183 = (bf16[32,128]{1,0:T(8,128)(2,1)S(1)}, f32[32,128]{1,0:T(8,128)S(1)}, bf16[64,1024]{1,0:T(8,128)(2,1)S(1)}, bf16[64,1024]{1,0:T(8,128)(2,1)S(1)}...) custom-call(s32[1]{0:T(128)} %bitcast.1.kv_pos, s32[1]{0:T(128)} %bitcast.tp_pos, ...), custom_call_target="tpu_custom_call" | custom-call | tf_op jit(solution)/shard_map/pallas_call | solution.py:274
  1.8 9.0 %psum.14.packed = bf16[32,128]{1,0:T(8,128)(2,1)S(1)} all-reduce(bf16[32,128]{1,0:T(8,128)(2,1)S(1)} %get-tuple-element.25), channel_id=1, replica_groups=mesh['dp'=4,'kv'=64,'tp'=2] {'tp'}, use_global_device_ids=true, to_apply=%region_0.0 | all-reduce | flops 4096 | bytes 16384 | tf_op jit(solution)/shard_map/psum | solution.py:333
  10.8 1.6 %shard_map.184 = bf16[64,40,128]{2,1,0:T(8,128)(2,1)} custom-call(s32[1]{0:T(128)} %bitcast.1.kv_pos, bf16[32,128]{1,0:T(8,128)(2,1)S(1)} %psum.14.packed, f32[32,128]{1,0:T(8,128)S(1)} %get-tuple-element.26.gain, bf16[64,1024]{1,0:T(8,128)(2,1)S(1)} %get-tuple-element.27.wq, bf16[64,1024]{1,0:T(8,128)(2,1)S(1)} %get-tuple-element.28.wk, ...), custom_call_target="tpu_custom_call" | custom-call | tf_op jit(solution)/shard_map/pallas_call | solution.py:274
  12.4 11.1 %all-to-all-start = ((bf16[64,40,128]{2,1,0:T(8,128)(2,1)}), bf16[64,40,128]{2,1,0:T(8,128)(2,1)S(1)}, u32[]{:S(2)}, u32[]{:S(2)}) async-start(bf16[64,40,128]{2,1,0:T(8,128)(2,1)} %shard_map.184), calls=%async_computation | async-start | bytes 1310720 | tf_op jit(solution)/shard_map/all_to_all | solution.py:378
  23.6 0.2 reshape.36
  23.8 0.1 reshape.37.gain
  24.0 0.6 copy-done.2
  24.6 1.2 %copy-done.1 = bf16[128,4096]{1,0:T(8,128)(2,1)S(1)} copy-done((bf16[128,4096]{1,0:T(8,128)(2,1)S(1)}, bf16[128,4096]{1,0:T(8,128)(2,1)}, u32[]{:S(2)}) %copy-start.1) | copy-done | bytes 1048600
  25.8 1.7 %shard_map.185 = (bf16[2048,256]{1,0:T(8,128)(2,1)S(1)}, bf16[2048,256]{1,0:T(8,128)(2,1)S(1)}, f32[8,128]{1,0:T(8,128)S(1)}, f32[8,128]{1,0:T(8,128)S(1)}, bf16[64,2048]{1,0:T(8,128)(2,1)S(1)}) custom-call(s32[1]{0:T(128)} %bitcast.tp_pos, bf16[64,2,2,16,128]{4,3,2,1,0:T(8,128)(2,1)S(1)} %bitcast.20, f32[4,1024]{1,0:T(4,128)S(1)} %reshape.37.gain, ...), custom_call_target="tpu_custom_call" | custom-call | tf_op jit(solution)/shard_map/pallas_call | solution.py:274
  27.5 2.5 %collective-permute-start = (bf16[2048,256]{1,0:T(8,128)(2,1)S(1)}, bf16[2048,256]{1,0:T(8,128)(2,1)S(1)}, u32[]{:S(2)}, u32[]{:S(2)}) collective-permute-start(bf16[2048,256]{1,0:T(8,128)(2,1)S(1)} %get-tuple-element.33), channel_id=1, source_target_pairs={{0,1},{1,0},{2,3},{3,2},{4,5},{5,4},{6,7},{7,6},{8,9},{9,8},{10,11... | collective-permute-start | bytes 3145736 | tf_op jit(solution)/shard_map/ppermute | solution.py:361
  30.1 2.3 %collective-permute-done.other = bf16[2048,256]{1,0:T(8,128)(2,1)S(1)} collective-permute-done((bf16[2048,256]{1,0:T(8,128)(2,1)S(1)}, bf16[2048,256]{1,0:T(8,128)(2,1)S(1)}, u32[]{:S(2)}, u32[]{:S(2)}) %collective-permute-start) | collective-permute-done | bytes 1048608 | tf_op jit(solution)/shard_map/ppermute | solution.py:361
  32.3 11.1 %all-to-all-done.arrived = bf16[64,40,128]{2,1,0:T(8,128)(2,1)S(1)} async-done(((bf16[64,40,128]{2,1,0:T(8,128)(2,1)}), bf16[64,40,128]{2,1,0:T(8,128)(2,1)S(1)}, u32[]{:S(2)}, u32[]{:S(2)}) %all-to-all-start) | async-done | bytes 655392 | tf_op jit(solution)/shard_map/all_to_all | solution.py:378
  43.5 3.9 %shard_map.186 = (bf16[64,16,128]{2,1,0:T(8,128)(2,1)S(1)}, f32[8,128]{1,0:T(8,128)}, f32[1,8]{1,0:T(1,128)}, f32[8,256,128]{2,1,0:T(8,128)}) custom-call(s32[1]{0:T(128)} %bitcast.tp_pos, bf16[64,40,128]{2,1,0:T(8,128)(2,1)S(1)} %all-to-all-done.arrived, f32[8,128]{1,0:T(8,128)S(1)} %get-tuple-element.35.normalizer, f32[8,128]{1,0:T(8,128)S(1)} %get-tuple-element.36.small, ...), custom_call_target="tpu_custom_call" | custom-call | tf_op jit(solution)/shard_map/pallas_call | solution.py:274
  47.4 19.4 %all_to_all.20.arrived = bf16[64,16,128]{2,1,0:T(8,128)(2,1)S(1)} all-to-all(bf16[64,16,128]{2,1,0:T(8,128)(2,1)S(1)} %get-tuple-element.37), channel_id=1, replica_groups=mesh['dp'=4,'kv'=64,'tp'=2] {'kv'}, dimensions={0} | all-to-all | bytes 524288 | tf_op jit(solution)/shard_map/all_to_all | solution.py:399
  66.7 0.4 shard_map.187
  67.1 6.5 %psum.15.half_sum = f32[32,128]{1,0:T(8,128)S(1)} all-reduce(f32[32,128]{1,0:T(8,128)S(1)} %shard_map.187), channel_id=1, replica_groups=mesh['dp'=4,'kv'=64,'tp'=2] {'tp'}, use_global_device_ids=true, to_apply=%region_1.0 | all-reduce | flops 4096 | bytes 32768 | tf_op jit(solution)/shard_map/psum | solution.py:412
  73.6 0.2 shard_map.188
  73.7 17.3 %all_to_all.21 = bf16[64,16,128]{2,1,0:T(8,128)(2,1)S(1)} all-to-all(bf16[64,16,128]{2,1,0:T(8,128)(2,1)S(1)} %get-tuple-element.39), channel_id=1, replica_groups=mesh['dp'=4,'kv'=64,'tp'=2] {'kv'}, dimensions={0} | all-to-all | bytes 524288 | tf_op jit(solution)/shard_map/all_to_all | solution.py:416
  91.0 0.6 shard_map.189.near
  91.6 4.3 %collective-permute-start.1 = (f32[136,128]{1,0:T(8,128)S(1)}, f32[136,128]{1,0:T(8,128)S(1)}, u32[]{:S(2)}, u32[]{:S(2)}) collective-permute-start(f32[136,128]{1,0:T(8,128)S(1)} %shard_map.189.near), channel_id=1, source_target_pairs={{0,1},{1,0},{2,3},{3,2},{4,5},{5,4},{6,7},{7,6},{8,9},{9,8},{10,11... | collective-permute-start | bytes 208904 | tf_op jit(solution)/shard_map/ppermute | solution.py:423
  95.9 0.9 collective-permute-done.1.far_sums
  96.8 0.5 shard_map.190
  97.3 17.2 %all_to_all.22.back = bf16[64,16,128]{2,1,0:T(8,128)(2,1)S(1)} all-to-all(bf16[64,16,128]{2,1,0:T(8,128)(2,1)S(1)} %bitcast.21), channel_id=1, replica_groups=mesh['dp'=4,'kv'=64,'tp'=2] {'kv'}, dimensions={0} | all-to-all | bytes 524288 | tf_op jit(solution)/shard_map/all_to_all | solution.py:428
  114.5 0.8 shard_map.191
  (11 shorter events, 0.1 us)
Async XLA Ops:
  12.4 11.1 %copy-start.5 = (f32[4096]{0:T(1024)S(1)}, f32[4096]{0:T(1024)}, u32[]{:S(2)}) copy-start(f32[4096]{0:T(1024)} %param.29) | copy-start | bytes 49156
  12.4 11.5 %copy-start = (bf16[4096,128]{1,0:T(8,128)(2,1)S(1)}, bf16[4096,128]{1,0:T(8,128)(2,1)}, u32[]{:S(2)}) copy-start(bf16[4096,128]{1,0:T(8,128)(2,1)} %param.30) | copy-start | bytes 3145732
  12.4 31.0 %all-to-all-start = ((bf16[64,40,128]{2,1,0:T(8,128)(2,1)}), bf16[64,40,128]{2,1,0:T(8,128)(2,1)S(1)}, u32[]{:S(2)}, u32[]{:S(2)}) async-start(bf16[64,40,128]{2,1,0:T(8,128)(2,1)} %shard_map.184), calls=%async_computation | async-start | bytes 1310720 | tf_op jit(solution)/shard_map/all_to_all | solution.py:378
  23.9 0.7 copy-start.2
  23.9 0.7 copy-start.3
  23.9 0.7 copy-start.4
  24.6 1.2 %copy-start.1 = (bf16[128,4096]{1,0:T(8,128)(2,1)S(1)}, bf16[128,4096]{1,0:T(8,128)(2,1)}, u32[]{:S(2)}) copy-start(bf16[128,4096]{1,0:T(8,128)(2,1)} %w_down.1) | copy-start | bytes 3145732
  27.5 4.8 %collective-permute-start = (bf16[2048,256]{1,0:T(8,128)(2,1)S(1)}, bf16[2048,256]{1,0:T(8,128)(2,1)S(1)}, u32[]{:S(2)}, u32[]{:S(2)}) collective-permute-start(bf16[2048,256]{1,0:T(8,128)(2,1)S(1)} %get-tuple-element.33), channel_id=1, source_target_pairs={{0,1},{1,0},{2,3},{3,2},{4,5},{5,4},{6,7},{7,6},{8,9},{9,8},{10,11... | collective-permute-start | bytes 3145736 | tf_op jit(solution)/shard_map/ppermute | solution.py:361
  91.6 5.2 %collective-permute-start.1 = (f32[136,128]{1,0:T(8,128)S(1)}, f32[136,128]{1,0:T(8,128)S(1)}, u32[]{:S(2)}, u32[]{:S(2)}) collective-permute-start(f32[136,128]{1,0:T(8,128)S(1)} %shard_map.189.near), channel_id=1, source_target_pairs={{0,1},{1,0},{2,3},{3,2},{4,5},{5,4},{6,7},{7,6},{8,9},{9,8},{10,11... | collective-permute-start | bytes 208904 | tf_op jit(solution)/shard_map/ppermute | solution.py:423

commit v3 on v2

--- a/solution.py
+++ b/solution.py
@@ -5,6 +5,7 @@
 from jax.experimental.pallas import tpu as pltpu
 from jax.sharding import PartitionSpec as P
 
+
 DV = 256
 DQK = 128
 LANES = 128
@@ -33,21 +34,24 @@
 
 def fetch_kernel(kv_pos, tp_pos, tokens, gain, wq, wk, wv, wig, wfg, padded, *rest):
     outs, sems = rest[:-1], rest[-1]
-    own, outs = outs[-1], outs[:-1]
     start = pl.multiple_of(kv_pos[0] // 2 * LANES, LANES)
     sources = (tokens, gain, wq, wk, wv, wig.at[:, pl.ds(start, LANES)], wfg.at[:, pl.ds(start, LANES)])
-    copies = [pltpu.make_async_copy(src, dst, sems.at[i]) for i, (src, dst) in enumerate(zip(sources, (own, *outs)))]
+    copies = [pltpu.make_async_copy(src, dst, sems.at[i]) for i, (src, dst) in enumerate(zip(sources, outs))]
     for copy in copies:
         copy.start()
     copies[0].wait()
-    x = own[...].astype(F32)
+    x = outs[0][...].astype(F32)
     twice = jnp.concatenate([x, x], axis=1)
     padded[...] = jnp.where(halves_of(twice) == tp_pos[0], twice, 0.0).astype(BF16)
     for copy in copies[1:]:
         copy.wait()
 
 
-def project_kernel(kv_pos, packed, gain, wq, wk, wv, wig, wfg, out, rows):
+def project_kernel(kv_pos, packed, gain, wq, wk, wv, wig, wfg, *rest):
+    sources, out, held, rows, sems = rest[:5], rest[5], rest[6:11], rest[11], rest[12]
+    copies = [pltpu.make_async_copy(src, dst, sems.at[i]) for i, (src, dst) in enumerate(zip(sources, held))]
+    for copy in copies:
+        copy.start()
     n = packed.shape[1] // 2
     block = kv_pos[0] // 2
     odd = kv_pos[0] % 2
@@ -85,15 +89,19 @@
     place(wv, 16, 2)
     for r in range(n):
         out[r] = rows[r * PITCH : r * PITCH + PITCH, :].astype(BF16)
-
-
-def cell_kernel(tp_pos, arrived, normalizer, small, memory_in, out, norm_out, stab_out, memory_out, memory, sems):
+    for copy in copies:
+        copy.wait()
+
+
+def cell_kernel(tp_pos, arrived, memory, normalizer, stab, ibias, fbias, gain, *rest):
+    out, keys, vals, keeps, norm_out, stab_out, gain_out, sem = rest
+    copy = pltpu.make_async_copy(gain, gain_out, sem)
+    copy.start()
     tp = tp_pos[0]
     heads = memory.shape[0]
-    loads = [pltpu.make_async_copy(memory_in.at[h], memory.at[h], sems.at[h]) for h in range(heads)]
-    stores = [pltpu.make_async_copy(memory.at[h], memory_out.at[h], sems.at[heads + h]) for h in range(heads)]
-    for load in loads:
-        load.start()
+    pad = jnp.zeros((1, LANES - 32), F32)
+    bias = jnp.concatenate([ibias[...], fbias[...], pad], axis=1)
+    old_stab = jnp.concatenate([stab[...], jnp.zeros((1, LANES - 8), F32)], axis=1)
     count = arrived.shape[0]
 
     def add(i, acc):
@@ -107,11 +115,11 @@
     extra = jnp.broadcast_to(acc[32:33], (8, LANES))
     squares = jnp.sum(jnp.where((lane == 64) | (lane == 65), extra, 0.0), axis=1, keepdims=True)
     scale = lax.rsqrt(squares * (1.0 / 4096.0) + NORM_EPS)
-    gates = extra * scale + small[0:1, :]
+    gates = extra * scale + bias
     head = tp * 8 + sub
     igate = jnp.sum(jnp.where((lane == head) | (lane == head + 32), gates, 0.0), axis=1, keepdims=True)
     fgate = jnp.sum(jnp.where((lane == head + 16) | (lane == head + 48), gates, 0.0), axis=1, keepdims=True)
-    old = jnp.sum(jnp.where(lane == sub, small[1:2, :], 0.0), axis=1, keepdims=True)
+    old = jnp.sum(jnp.where(lane == sub, old_stab, 0.0), axis=1, keepdims=True)
     log_forget = jnp.minimum(fgate, 0.0) - jnp.log1p(jnp.exp(-jnp.abs(fgate)))
     carried = log_forget + old
     new = jnp.maximum(carried, igate)
@@ -125,7 +133,6 @@
     sub2 = lax.broadcasted_iota(jnp.int32, (8, DV), 0)
     recall = jnp.zeros((8, DV), F32)
     for h in range(heads):
-        loads[h].wait()
         part = lax.dot_general(q_both, memory[h].astype(BF16), NT, preferred_element_type=F32)
         recall = jnp.where(sub2 == h, part[:8] + part[8:], recall)
     match = jnp.sum(q * k, axis=1, keepdims=True)
@@ -137,21 +144,39 @@
     for r in range(count):
         out[r] = tile
     norm_out[...] = keep * old_norm + fresh * k
-    value = fresh * v
-    v_high, v_low = split(value)
-    k_high, k_low = split(k)
+    keys[...] = k
+    vals[...] = fresh * v
+    keeps[...] = jnp.broadcast_to(keep, keeps.shape)
+    copy.wait()
+
+
+def update_kernel(keys, vals, keeps, memory_in, memory_out, memory, sems):
+    heads = memory.shape[0]
+    loads = [pltpu.make_async_copy(memory_in.at[h], memory.at[h], sems.at[h]) for h in range(heads)]
+    stores = [pltpu.make_async_copy(memory.at[h], memory_out.at[h], sems.at[heads + h]) for h in range(heads)]
+    for load in loads:
+        load.start()
+    v_high, v_low = split(vals[...])
+    k_high, k_low = split(keys[...])
     for h in range(heads):
         row = slice(h, h + 1)
         left = jnp.concatenate([v_high[row], v_high[row], v_low[row]], axis=0)
         right = jnp.concatenate([k_high[row], k_low[row], k_high[row]], axis=0)
         outer = lax.dot_general(left, right, TN, preferred_element_type=F32)
-        memory[h] = keep[row] * memory[h] + outer
+        loads[h].wait()
+        memory[h] = keeps[row, :] * memory[h] + outer
         stores[h].start()
     for store in stores:
         store.wait()
 
 
-def output_kernel(arrived, w, out, rows):
+def folded(wide):
+    thin = wide.shape[0] // 2
+    return jnp.concatenate([wide[:thin], wide[thin:]], axis=1)
+
+
+def output_kernel(tp_pos, arrived, w, own, out, rows):
+    tp = tp_pos[0]
     count = arrived.shape[0]
     for r in range(count):
         rows[r * 16 : r * 16 + 16, :] = arrived[r].astype(F32)
@@ -161,21 +186,15 @@
         parts.append(rows[pl.ds(c, count, stride=16), :].astype(BF16))
     acc = lax.dot_general(w[...], jnp.concatenate(parts, axis=1), NT, preferred_element_type=F32)
     half = acc.shape[0] // 2
-    out[...] = jnp.concatenate([acc[:half], acc[half:]], axis=1)
-
-
-def prepare_kernel(tp_pos, w_up, gain, w_down, stab, ibias, fbias, normalizer, w_out, keep, send, small, *rest):
-    outs, turned, sems = rest[:-2], rest[-2], rest[-1]
-    copies = [
-        pltpu.make_async_copy(src, dst, sems.at[i])
-        for i, (src, dst) in enumerate(zip((normalizer, w_out), outs))
-    ]
-    for copy in copies:
-        copy.start()
-    small[...] = jnp.zeros(small.shape, F32)
-    small[0:1, 0:16] = ibias[...]
-    small[0:1, 16:32] = fbias[...]
-    small[1:2, 0:8] = stab[...]
+    first = folded(acc[:half])
+    second = folded(acc[half:])
+    own[...] = jnp.where(tp == 0, first, second).astype(BF16)
+    out[...] = jnp.concatenate([jnp.where(tp == 1, first, 0.0), jnp.where(tp == 0, second, 0.0)], axis=0).astype(BF16)
+
+
+def prepare_kernel(tp_pos, w_up, gain, w_down, w_out, keep, send, held, turned, sem):
+    copy = pltpu.make_async_copy(w_out, held, sem)
+    copy.start()
     tp = tp_pos[0]
     chips = w_up.shape[0]
     for k in range(0, chips, 2):
@@ -191,17 +210,14 @@
                 part = part.astype(F32) * factors[:, block * 256 : block * 256 + 256]
                 dst[block * 256 + quarter * 128 : block * 256 + quarter * 128 + 128, :] = part.astype(BF16)
             dst[1024:2048, lanes] = turned[:, half, quarter].reshape(1024, 128)
-    for copy in copies:
-        copy.wait()
-
-
-def middle_kernel(tp_pos, half_sum, packed, out, own):
+    copy.wait()
+
+
+def middle_kernel(tp_pos, half, both, tokens, out, own):
     tp = tp_pos[0]
-    whole = packed[...].astype(F32) + half_sum[...]
-    n = whole.shape[1] // 2
-    mine = jnp.where(tp == 0, whole[:, :n], whole[:, n:])
-    thin = mine.shape[0] // 2
-    tile = jnp.concatenate([mine[:thin], mine[thin:]], axis=1).astype(BF16)
+    thin = half.shape[0]
+    other = jnp.where(tp == 0, both[:thin].astype(F32), both[thin:].astype(F32))
+    tile = (folded(tokens[...].astype(F32)) + half[...].astype(F32) + other).astype(BF16)
     own[...] = tile
     for r in range(out.shape[0]):
         out[r] = tile
@@ -266,7 +282,7 @@
 
 
 def call(kernel, shapes, *args, scalars=0, far=0, fetched=0, away=(), scratch=()):
-    outs = [jax.ShapeDtypeStruct(s, d) if i in away else pltpu.VMEM(s, d) for i, (s, d) in enumerate(shapes)]
+    outs = [pltpu.HBM(s, d) if i in away else pltpu.VMEM(s, d) for i, (s, d) in enumerate(shapes)]
     out_specs = [vmem] * (len(outs) - fetched) + [any_space] * fetched
     many = len(outs) > 1
     near = len(args) - far
@@ -305,10 +321,11 @@
     rows, thin = tokens.shape
     kv_pos = kv_index.astype(jnp.int32).reshape(1)
     tp_pos = tp_index.astype(jnp.int32).reshape(1)
-    padded, gain_near, wq, wk, wv, ig, fg = call(
+    padded, own_tokens, gain_near, wq, wk, wv, ig, fg = call(
         fetch_kernel,
         [
             ((thin, 2 * rows), BF16),
+            ((thin, rows), BF16),
             ((mix_gain.shape[0] // LANES, LANES), F32),
             (w_query.shape, BF16),
             (w_key.shape, BF16),
@@ -328,41 +345,20 @@
         scalars=2,
         far=7,
         fetched=6,
-        scratch=[pltpu.VMEM((thin, rows), BF16), pltpu.SemaphoreType.DMA((7,))],
+        scratch=[pltpu.SemaphoreType.DMA((7,))],
     )
     packed = lax.psum(padded, "tp")
 
-    hidden = w_up.shape[1]
-    quarter = thin // 2
-    gains = mlp_gain.reshape(kv, 2, 2, quarter).transpose(1, 2, 0, 3).reshape(4, kv * quarter)
-    keep, send, small, state_norm, w_out = call(
-        prepare_kernel,
+    sends, state, state_norm, old_stab, ibias, fbias = call(
+        project_kernel,
         [
-            ((2048, 256), BF16),
-            ((2048, 256), BF16),
-            ((8, LANES), F32),
+            ((rows, PITCH, LANES), BF16),
+            (memory.shape[1:], F32),
             (normalizer.shape[1:], F32),
-            (w_output.shape[::-1], BF16),
+            (stabilizer.shape, F32),
+            ((1, igate_bias.shape[0]), F32),
+            ((1, fgate_bias.shape[0]), F32),
         ],
-        tp_pos,
-        w_up.reshape(kv, 2, 2, quarter, hidden),
-        gains,
-        w_down,
-        stabilizer,
-        igate_bias[None],
-        fgate_bias[None],
-        normalizer[0],
-        w_output.T,
-        scalars=1,
-        far=2,
-        fetched=2,
-        scratch=[pltpu.VMEM((kv, 2, 2, quarter, hidden), BF16), pltpu.SemaphoreType.DMA((2,))],
-    )
-    other = lax.ppermute(send, "tp", [(0, 1), (1, 0)])
-
-    sends = call(
-        project_kernel,
-        [((rows, PITCH, LANES), BF16)],
         kv_pos,
         packed,
         gain_near,
@@ -371,46 +367,92 @@
         wv,
         ig,
         fg,
+        memory[0],
+        normalizer[0],
+        stabilizer,
+        igate_bias[None],
+        fgate_bias[None],
         scalars=1,
-        away=(0,),
-        scratch=[pltpu.VMEM((rows * PITCH, LANES), F32)],
+        far=5,
+        fetched=5,
+        scratch=[pltpu.VMEM((rows * PITCH, LANES), F32), pltpu.SemaphoreType.DMA((5,))],
     )
     arrived = lax.all_to_all(sends, "kv", 0, 0, tiled=True)
-    arrived, keep, other = lax.optimization_barrier((arrived, keep, other))
-    cell, new_normalizer, new_stabilizer, new_memory = call(
+    cell, keys, vals, keeps, new_normalizer, new_stabilizer, late_gain = call(
         cell_kernel,
         [
             ((kv, 16, LANES), BF16),
             ((8, DQK), F32),
+            ((8, DV), F32),
+            ((8, LANES), F32),
+            ((8, DQK), F32),
             ((1, 8), F32),
-            (memory.shape[1:], F32),
+            ((mlp_gain.shape[0] // LANES, LANES), F32),
         ],
         tp_pos,
         arrived,
+        state,
         state_norm,
-        small,
-        memory[0],
+        old_stab,
+        ibias,
+        fbias,
+        mlp_gain.reshape(-1, LANES),
         scalars=1,
         far=1,
         fetched=1,
-        away=(1, 2, 3),
+        away=(0, 4, 5),
+        scratch=[pltpu.SemaphoreType.DMA],
+    )
+    cells = lax.all_to_all(cell, "kv", 0, 0, tiled=True)
+    new_memory = call(
+        update_kernel,
+        [(memory.shape[1:], F32)],
+        keys,
+        vals,
+        keeps,
+        memory[0],
+        far=1,
+        fetched=1,
+        away=(0,),
         scratch=[pltpu.VMEM(memory.shape[1:], F32), pltpu.SemaphoreType.DMA((16,))],
     )
-    cells = lax.all_to_all(cell, "kv", 0, 0, tiled=True)
-
-    half = call(
+
+    hidden = w_up.shape[1]
+    quarter = thin // 2
+    gains = late_gain.reshape(kv, 2, 2, quarter).transpose(1, 2, 0, 3).reshape(4, kv * quarter)
+    keep, send, w_out = call(
+        prepare_kernel,
+        [((2048, 256), BF16), ((2048, 256), BF16), (w_output.shape[::-1], BF16)],
+        tp_pos,
+        w_up.reshape(kv, 2, 2, quarter, hidden),
+        gains,
+        w_down,
+        w_output.T,
+        scalars=1,
+        far=1,
+        fetched=1,
+        away=(1,),
+        scratch=[pltpu.VMEM((kv, 2, 2, quarter, hidden), BF16), pltpu.SemaphoreType.DMA],
+    )
+    other = lax.ppermute(send, "tp", [(0, 1), (1, 0)])
+    cells, keep, other, new_memory = lax.optimization_barrier((cells, keep, other, new_memory))
+
+    half, crossing = call(
         output_kernel,
-        [((thin, 2 * rows), F32)],
+        [((quarter, 2 * rows), BF16), ((thin, 2 * rows), BF16)],
+        tp_pos,
         cells,
         w_out,
+        scalars=1,
         scratch=[pltpu.VMEM((rows * 16, LANES), F32)],
     )
     middle, own = call(
         middle_kernel,
         [((kv, quarter, 2 * rows), BF16), ((quarter, 2 * rows), BF16)],
         tp_pos,
-        lax.psum(half, "tp"),
-        packed,
+        half,
+        lax.psum(crossing, "tp"),
+        own_tokens,
         scalars=1,
     )
     middles = lax.all_to_all(middle, "kv", 0, 0, tiled=True).reshape(kv * quarter, 2 * rows)
@@ -455,6 +497,4 @@
         P(("dp", "kv"), "tp", None),
         P(("dp", "kv"), "tp"),
     )
-    return jax.shard_map(
-        on_device, mesh=mesh, in_specs=in_specs, out_specs=out_specs, check_vma=False
-    )
+    return jax.shard_map(on_device, mesh=mesh, in_specs=in_specs, out_specs=out_specs, check_vma=False)

time: 117 us -> 119 us (1.017)
  blocking collectives: 69.4 us -> 78.5 us
  starting transfers between devices: 17.9 us -> 14.7 us
  waiting for transfers between devices: 14.3 us -> 11.3 us
  local copies, waits for them, and re-layouts: 2.23 us -> 0.35 us
  Pallas kernels: 10.8 us -> 12 us
    all_to_all x1, blocking collectives: 19.4 us -> 30.7 us  [on_device(): arrived = lax.all_to_all(sends, 'kv', 0, 0, tiled=True)]
    all_to_all x1, starting transfers between devices: 11.1 us -> 6.12 us  [on_device(): cells = lax.all_to_all(cell, 'kv', 0, 0, tiled=True)]
    ppermute x1, waiting for transfers between devices: 2.26 us -> 0.01 us  [on_device(): other = lax.ppermute(send, 'tp', [(0, 1), (1, 0)])]
    psum x1, blocking collectives: 6.46 us -> 4.37 us  [on_device(): lax.psum(crossing, 'tp')]
    unnamed x12 -> x4, local copies, waits for them, and re-layouts: 1.88 us -> 0.01 us
    ppermute x1, starting transfers between devices: 2.52 us -> 4.14 us  [on_device(): other = lax.ppermute(send, 'tp', [(0, 1), (1, 0)])]
    pallas_call x9 -> x10, Pallas kernels: 10.8 us -> 12 us  [call(): pl.pallas_call(kernel, out_shape=outs if many else outs[0], in_specs=[sme...]
  transfers between devices with their start and end apart: 3 -> 3, of which waited for: 3 -> 2; matrix products, arithmetic and copies ran while one was open for 0% -> 0% of each run, Pallas kernels for 1% -> 3%
where the time goes in v3:
time: 119 us; the launch traced here: 118 us
  blocking collectives  78.5 us (66%)
  starting transfers between devices  14.7 us (12%)
  Pallas kernels  12 us (10%)
  waiting for transfers between devices  11.3 us (9%)
    all_to_all x1, blocking collectives, on_device(): arrived = lax.all_to_all(sends, 'kv', 0, 0, tiled=True)  30.7 us
    all_to_all x1, blocking collectives, on_device(): lax.all_to_all(downs.reshape(kv, quarter, 2 * rows), 'kv', 0, 0, tiled=True)  17.2 us
    all_to_all x1, blocking collectives, on_device(): lax.all_to_all(middle, 'kv', 0, 0, tiled=True)  17.2 us
    pallas_call x10, Pallas kernels, call(): pl.pallas_call(kernel, out_shape=outs if many else outs[0], in_specs=[sme...  12 us
    all_to_all x1, waiting for transfers between devices, on_device(): cells = lax.all_to_all(cell, 'kv', 0, 0, tiled=True)  10.4 us
    psum x1, blocking collectives, on_device(): packed = lax.psum(padded, 'tp')  9 us
    all_to_all x1, starting transfers between devices, on_device(): cells = lax.all_to_all(cell, 'kv', 0, 0, tiled=True)  6.12 us
    ppermute x1, starting transfers between devices, on_device(): lax.ppermute(sums, 'tp', [(0, 1), (1, 0)])  4.4 us
  transfers between devices with their start and end apart: 3, of which 2 were waited for; matrix products, arithmetic and copies ran while one was open for 0% of the time, Pallas kernels for 3%

profile of v3, /device:TPU:1, one launch (start us, length us, event | category | flops | bytes accessed | tf_op | source)
XLA Modules:
  0.0 117.5 jit_solution(11675442580924458003)
XLA Ops:
  0.6 1.2 %shard_map.183 = (bf16[32,128]{1,0:T(8,128)(2,1)S(1)}, bf16[32,64]{1,0:T(8,128)(2,1)S(1)}, f32[32,128]{1,0:T(8,128)S(1)}, bf16[64,1024]{1,0:T(8,128)(2,1)S(1)}, ...) custom-call(s32[1]{0:T(128)} %bitcast.1.kv_pos, ...), custom_call_target="tpu_custom_call" | custom-call | tf_op jit(solution)/shard_map/pallas_call | solution.py:290
  1.8 9.0 %psum.14.packed = bf16[32,128]{1,0:T(8,128)(2,1)S(1)} all-reduce(bf16[32,128]{1,0:T(8,128)(2,1)S(1)} %get-tuple-element.36), channel_id=1, replica_groups=mesh['dp'=4,'kv'=64,'tp'=2] {'tp'}, use_global_device_ids=true, to_apply=%region_0.0 | all-reduce | flops 4096 | bytes 16384 | tf_op jit(solution)/shard_map/psum | solution.py:350
  10.8 1.3 %shard_map.184 = (bf16[64,40,128]{2,1,0:T(8,128)(2,1)S(1)}, f32[8,256,128]{2,1,0:T(8,128)S(1)}, f32[8,128]{1,0:T(8,128)S(1)}, f32[1,8]{1,0:T(1,128)S(1)}, f32[1,16]{1,0:T(1,128)S(1)}, /*index=5*/f32[1,16]{1,0:T(1,128)S(1)}) custom-call(s32[1]{0:T(128)} %bitcast.1.kv_pos, bf16[32,128]{1,0:T(8,128)(2,1)S(1)} %psum.14.packed, ...), custom_call_target="tpu_custom_call" | custom-call | tf_op jit(solution)/shard_map/pallas_call | solution.py:290
  12.1 30.7 %all_to_all.20.arrived = bf16[64,40,128]{2,1,0:T(8,128)(2,1)S(1)} all-to-all(bf16[64,40,128]{2,1,0:T(8,128)(2,1)S(1)} %get-tuple-element.43), channel_id=1, replica_groups=mesh['dp'=4,'kv'=64,'tp'=2] {'kv'}, dimensions={0} | all-to-all | bytes 1310720 | tf_op jit(solution)/shard_map/all_to_all | solution.py:380
  42.8 1.6 %shard_map.185 = (bf16[64,16,128]{2,1,0:T(8,128)(2,1)}, f32[8,128]{1,0:T(8,128)S(1)}, f32[8,256]{1,0:T(8,128)S(1)}, f32[8,128]{1,0:T(8,128)S(1)}, f32[8,128]{1,0...) custom-call(s32[1]{0:T(128)} %bitcast.tp_pos, bf16[64,40,128]{2,1,0:T(8,128)(2,1)S(1)} %all_to_all.20.arrived, ...), custom_call_target="tpu_custom_call" | custom-call | tf_op jit(solution)/shard_map/pallas_call | solution.py:290
  44.4 0.2 reshape.40
  44.7 0.1 reshape.41.gain
  44.8 0.0 copy-done
  44.8 2.5 %shard_map.186 = (bf16[2048,256]{1,0:T(8,128)(2,1)S(1)}, bf16[2048,256]{1,0:T(8,128)(2,1)}, bf16[64,2048]{1,0:T(8,128)(2,1)S(1)}) custom-call(s32[1]{0:T(128)} %bitcast.tp_pos, bf16[64,2,2,16,128]{4,3,2,1,0:T(8,128)(2,1)S(1)} %bitcast.21, f32[4,1024]{1,0:T(4,128)S(1)} %reshape.41.gain, bf16[128,4096]{1,0:T(8,128)(2,1)S(1)} %copy-done.1, ...), custom_call_target="tpu_custom_call" | custom-call | tf_op jit(solution)/shard_map/pallas_call | solution.py:290
  47.2 4.1 %collective-permute-start = (bf16[2048,256]{1,0:T(8,128)(2,1)}, bf16[2048,256]{1,0:T(8,128)(2,1)S(1)}, u32[]{:S(2)}, u32[]{:S(2)}) collective-permute-start(bf16[2048,256]{1,0:T(8,128)(2,1)} %get-tuple-element.52), channel_id=1, source_target_pairs={{0,1},{1,0},{2,3},{3,2},{4,5},{5,4},{6,7},{7,6},{8,9},{9,8},{10,11... | collective-permute-start | bytes 3145736 | tf_op jit(solution)/shard_map/ppermute | solution.py:437
  51.4 6.1 %all-to-all-start.1 = ((bf16[64,16,128]{2,1,0:T(8,128)(2,1)}), bf16[64,16,128]{2,1,0:T(8,128)(2,1)S(1)}, u32[]{:S(2)}, u32[]{:S(2)}) async-start(bf16[64,16,128]{2,1,0:T(8,128)(2,1)} %get-tuple-element.49), calls=%async_computation.1 | async-start | bytes 524288 | tf_op jit(solution)/shard_map/all_to_all | solution.py:406
  57.5 3.2 %shard_map.187 = f32[8,256,128]{2,1,0:T(8,128)} custom-call(f32[8,128]{1,0:T(8,128)S(1)} %get-tuple-element.53.keys, f32[8,256]{1,0:T(8,128)S(1)} %get-tuple-element.54.vals, f32[8,128]{1,0:T(8,128)S(1)} %get-tuple-element.55.keeps, f32[8,256,128]{2,1,0:T(8,128)} %bitcast.25), custom_call_target="tpu_custom_call" | custom-call | tf_op jit(solution)/shard_map/pallas_call | solution.py:290
  60.7 10.4 %all-to-all-done.1.arrived = bf16[64,16,128]{2,1,0:T(8,128)(2,1)S(1)} async-done(((bf16[64,16,128]{2,1,0:T(8,128)(2,1)}), bf16[64,16,128]{2,1,0:T(8,128)(2,1)S(1)}, u32[]{:S(2)}, u32[]{:S(2)}) %all-to-all-start.1) | async-done | bytes 262176 | tf_op jit(solution)/shard_map/all_to_all | solution.py:406
  71.1 0.0 collective-permute-done.other
  71.1 0.4 shard_map.188
  71.5 4.4 %psum.15.both = bf16[32,128]{1,0:T(8,128)(2,1)S(1)} all-reduce(bf16[32,128]{1,0:T(8,128)(2,1)S(1)} %get-tuple-element.59), channel_id=1, replica_groups=mesh['dp'=4,'kv'=64,'tp'=2] {'tp'}, use_global_device_ids=true, to_apply=%region_1.0 | all-reduce | flops 4096 | bytes 16384 | tf_op jit(solution)/shard_map/psum | solution.py:454
  75.9 0.1 shard_map.189
  76.0 17.2 %all_to_all.21 = bf16[64,16,128]{2,1,0:T(8,128)(2,1)S(1)} all-to-all(bf16[64,16,128]{2,1,0:T(8,128)(2,1)S(1)} %get-tuple-element.61), channel_id=1, replica_groups=mesh['dp'=4,'kv'=64,'tp'=2] {'kv'}, dimensions={0} | all-to-all | bytes 524288 | tf_op jit(solution)/shard_map/all_to_all | solution.py:458
  93.2 0.6 shard_map.190.near
  93.7 4.4 %collective-permute-start.1 = (f32[136,128]{1,0:T(8,128)S(1)}, f32[136,128]{1,0:T(8,128)S(1)}, u32[]{:S(2)}, u32[]{:S(2)}) collective-permute-start(f32[136,128]{1,0:T(8,128)S(1)} %shard_map.190.near), channel_id=1, source_target_pairs={{0,1},{1,0},{2,3},{3,2},{4,5},{5,4},{6,7},{7,6},{8,9},{9,8},{10,11... | collective-permute-start | bytes 208904 | tf_op jit(solution)/shard_map/ppermute | solution.py:465
  98.1 0.9 collective-permute-done.1.far_sums
  99.0 0.5 shard_map.191
  99.5 17.2 %all_to_all.22.back = bf16[64,16,128]{2,1,0:T(8,128)(2,1)S(1)} all-to-all(bf16[64,16,128]{2,1,0:T(8,128)(2,1)S(1)} %bitcast.22), channel_id=1, replica_groups=mesh['dp'=4,'kv'=64,'tp'=2] {'kv'}, dimensions={0} | all-to-all | bytes 524288 | tf_op jit(solution)/shard_map/all_to_all | solution.py:470
  116.8 0.8 shard_map.192
  (4 shorter events, 0.0 us)
Async XLA Ops:
  42.8 2.0 %copy-start = (bf16[4096,128]{1,0:T(8,128)(2,1)S(1)}, bf16[4096,128]{1,0:T(8,128)(2,1)}, u32[]{:S(2)}) copy-start(bf16[4096,128]{1,0:T(8,128)(2,1)} %param.30) | copy-start | bytes 3145732
  42.8 2.0 %copy-start.1 = (bf16[128,4096]{1,0:T(8,128)(2,1)S(1)}, bf16[128,4096]{1,0:T(8,128)(2,1)}, u32[]{:S(2)}) copy-start(bf16[128,4096]{1,0:T(8,128)(2,1)} %w_down.1) | copy-start | bytes 3145732
  47.2 23.9 %collective-permute-start = (bf16[2048,256]{1,0:T(8,128)(2,1)}, bf16[2048,256]{1,0:T(8,128)(2,1)S(1)}, u32[]{:S(2)}, u32[]{:S(2)}) collective-permute-start(bf16[2048,256]{1,0:T(8,128)(2,1)} %get-tuple-element.52), channel_id=1, source_target_pairs={{0,1},{1,0},{2,3},{3,2},{4,5},{5,4},{6,7},{7,6},{8,9},{9,8},{10,11... | collective-permute-start | bytes 3145736 | tf_op jit(solution)/shard_map/ppermute | solution.py:437
  51.4 19.7 %all-to-all-start.1 = ((bf16[64,16,128]{2,1,0:T(8,128)(2,1)}), bf16[64,16,128]{2,1,0:T(8,128)(2,1)S(1)}, u32[]{:S(2)}, u32[]{:S(2)}) async-start(bf16[64,16,128]{2,1,0:T(8,128)(2,1)} %get-tuple-element.49), calls=%async_computation.1 | async-start | bytes 524288 | tf_op jit(solution)/shard_map/all_to_all | solution.py:406
  93.7 5.3 %collective-permute-start.1 = (f32[136,128]{1,0:T(8,128)S(1)}, f32[136,128]{1,0:T(8,128)S(1)}, u32[]{:S(2)}, u32[]{:S(2)}) collective-permute-start(f32[136,128]{1,0:T(8,128)S(1)} %shard_map.190.near), channel_id=1, source_target_pairs={{0,1},{1,0},{2,3},{3,2},{4,5},{5,4},{6,7},{7,6},{8,9},{9,8},{10,11... | collective-permute-start | bytes 208904 | tf_op jit(solution)/shard_map/ppermute | solution.py:465

commit v4 on v3

--- a/solution.py
+++ b/solution.py
@@ -48,7 +48,7 @@
 
 
 def project_kernel(kv_pos, packed, gain, wq, wk, wv, wig, wfg, *rest):
-    sources, out, held, rows, sems = rest[:5], rest[5], rest[6:11], rest[11], rest[12]
+    sources, out, held, rows, sems = rest[:4], rest[4], rest[5:9], rest[9], rest[10]
     copies = [pltpu.make_async_copy(src, dst, sems.at[i]) for i, (src, dst) in enumerate(zip(sources, held))]
     for copy in copies:
         copy.start()
@@ -93,12 +93,13 @@
         copy.wait()
 
 
-def cell_kernel(tp_pos, arrived, memory, normalizer, stab, ibias, fbias, gain, *rest):
-    out, keys, vals, keeps, norm_out, stab_out, gain_out, sem = rest
-    copy = pltpu.make_async_copy(gain, gain_out, sem)
-    copy.start()
+def cell_kernel(tp_pos, arrived, normalizer, stab, ibias, fbias, memory_in, *rest):
+    out, keys, vals, keeps, norm_out, stab_out, memory, sems = rest
     tp = tp_pos[0]
     heads = memory.shape[0]
+    loads = [pltpu.make_async_copy(memory_in.at[h], memory.at[h], sems.at[h]) for h in range(heads)]
+    for load in loads:
+        load.start()
     pad = jnp.zeros((1, LANES - 32), F32)
     bias = jnp.concatenate([ibias[...], fbias[...], pad], axis=1)
     old_stab = jnp.concatenate([stab[...], jnp.zeros((1, LANES - 8), F32)], axis=1)
@@ -133,6 +134,7 @@
     sub2 = lax.broadcasted_iota(jnp.int32, (8, DV), 0)
     recall = jnp.zeros((8, DV), F32)
     for h in range(heads):
+        loads[h].wait()
         part = lax.dot_general(q_both, memory[h].astype(BF16), NT, preferred_element_type=F32)
         recall = jnp.where(sub2 == h, part[:8] + part[8:], recall)
     match = jnp.sum(q * k, axis=1, keepdims=True)
@@ -147,7 +149,6 @@
     keys[...] = k
     vals[...] = fresh * v
     keeps[...] = jnp.broadcast_to(keep, keeps.shape)
-    copy.wait()
 
 
 def update_kernel(keys, vals, keeps, memory_in, memory_out, memory, sems):
@@ -349,11 +350,10 @@
     )
     packed = lax.psum(padded, "tp")
 
-    sends, state, state_norm, old_stab, ibias, fbias = call(
+    sends, state_norm, old_stab, ibias, fbias = call(
         project_kernel,
         [
             ((rows, PITCH, LANES), BF16),
-            (memory.shape[1:], F32),
             (normalizer.shape[1:], F32),
             (stabilizer.shape, F32),
             ((1, igate_bias.shape[0]), F32),
@@ -367,18 +367,37 @@
         wv,
         ig,
         fg,
-        memory[0],
         normalizer[0],
         stabilizer,
         igate_bias[None],
         fgate_bias[None],
         scalars=1,
-        far=5,
-        fetched=5,
-        scratch=[pltpu.VMEM((rows * PITCH, LANES), F32), pltpu.SemaphoreType.DMA((5,))],
+        far=4,
+        fetched=4,
+        away=(0,),
+        scratch=[pltpu.VMEM((rows * PITCH, LANES), F32), pltpu.SemaphoreType.DMA((4,))],
     )
     arrived = lax.all_to_all(sends, "kv", 0, 0, tiled=True)
-    cell, keys, vals, keeps, new_normalizer, new_stabilizer, late_gain = call(
+    hidden = w_up.shape[1]
+    quarter = thin // 2
+    gains = mlp_gain.reshape(kv, 2, 2, quarter).transpose(1, 2, 0, 3).reshape(4, kv * quarter)
+    keep, send, w_out = call(
+        prepare_kernel,
+        [((2048, 256), BF16), ((2048, 256), BF16), (w_output.shape[::-1], BF16)],
+        tp_pos,
+        w_up.reshape(kv, 2, 2, quarter, hidden),
+        gains,
+        w_down,
+        w_output.T,
+        scalars=1,
+        far=1,
+        fetched=1,
+        away=(1,),
+        scratch=[pltpu.VMEM((kv, 2, 2, quarter, hidden), BF16), pltpu.SemaphoreType.DMA],
+    )
+    other = lax.ppermute(send, "tp", [(0, 1), (1, 0)])
+    arrived, keep, other = lax.optimization_barrier((arrived, keep, other))
+    cell, keys, vals, keeps, new_normalizer, new_stabilizer = call(
         cell_kernel,
         [
             ((kv, 16, LANES), BF16),
@@ -387,21 +406,18 @@
             ((8, LANES), F32),
             ((8, DQK), F32),
             ((1, 8), F32),
-            ((mlp_gain.shape[0] // LANES, LANES), F32),
         ],
         tp_pos,
         arrived,
-        state,
         state_norm,
         old_stab,
         ibias,
         fbias,
-        mlp_gain.reshape(-1, LANES),
+        memory[0],
         scalars=1,
         far=1,
-        fetched=1,
         away=(0, 4, 5),
-        scratch=[pltpu.SemaphoreType.DMA],
+        scratch=[pltpu.VMEM(memory.shape[1:], F32), pltpu.SemaphoreType.DMA((8,))],
     )
     cells = lax.all_to_all(cell, "kv", 0, 0, tiled=True)
     new_memory = call(
@@ -417,25 +433,7 @@
         scratch=[pltpu.VMEM(memory.shape[1:], F32), pltpu.SemaphoreType.DMA((16,))],
     )
 
-    hidden = w_up.shape[1]
-    quarter = thin // 2
-    gains = late_gain.reshape(kv, 2, 2, quarter).transpose(1, 2, 0, 3).reshape(4, kv * quarter)
-    keep, send, w_out = call(
-        prepare_kernel,
-        [((2048, 256), BF16), ((2048, 256), BF16), (w_output.shape[::-1], BF16)],
-        tp_pos,
-        w_up.reshape(kv, 2, 2, quarter, hidden),
-        gains,
-        w_down,
-        w_output.T,
-        scalars=1,
-        far=1,
-        fetched=1,
-        away=(1,),
-        scratch=[pltpu.VMEM((kv, 2, 2, quarter, hidden), BF16), pltpu.SemaphoreType.DMA],
-    )
-    other = lax.ppermute(send, "tp", [(0, 1), (1, 0)])
-    cells, keep, other, new_memory = lax.optimization_barrier((cells, keep, other, new_memory))
+    cells, new_memory = lax.optimization_barrier((cells, new_memory))
 
     half, crossing = call(
         output_kernel,

time: 119 us -> 115 us (0.966)
  blocking collectives: 78.5 us -> 48.8 us
  waiting for transfers between devices: 11.3 us -> 23.6 us
  starting transfers between devices: 14.7 us -> 25.1 us
  Pallas kernels: 12 us -> 13.7 us
  local copies, waits for them, and re-layouts: 0.35 us -> 1.57 us
    all_to_all x1 -> x0, blocking collectives: 30.7 us -> none  [on_device(): arrived = lax.all_to_all(sends, 'kv', 0, 0, tiled=True)]
    all_to_all x0 -> x1, starting transfers between devices: none -> 11.1 us  [on_device(): arrived = lax.all_to_all(sends, 'kv', 0, 0, tiled=True)]
    all_to_all x0 -> x1, waiting for transfers between devices: none -> 10.9 us  [on_device(): arrived = lax.all_to_all(sends, 'kv', 0, 0, tiled=True)]
    ppermute x1, waiting for transfers between devices: 0.01 us -> 2.48 us  [on_device(): other = lax.ppermute(send, 'tp', [(0, 1), (1, 0)])]
    pallas_call x10, Pallas kernels: 12 us -> 13.7 us  [call(): pl.pallas_call(kernel, out_shape=outs if many else outs[0], in_specs=[sme...]
    ppermute x1, starting transfers between devices: 4.14 us -> 2.52 us  [on_device(): other = lax.ppermute(send, 'tp', [(0, 1), (1, 0)])]
    unnamed x4 -> x6, local copies, waits for them, and re-layouts: 0.01 us -> 1.23 us
  transfers between devices with their start and end apart: 3 -> 4, of which waited for: 2 -> 4; matrix products, arithmetic and copies ran while one was open for 0% -> 0% of each run, Pallas kernels for 3% -> 5%
where the time goes in v4:
time: 115 us; the launch traced here: 114 us
  blocking collectives  48.8 us (42%)
  starting transfers between devices  25.1 us (22%)
  waiting for transfers between devices  23.6 us (21%)
  Pallas kernels  13.7 us (12%)
  local copies, waits for them, and re-layouts  1.57 us (1%)
    all_to_all x1, blocking collectives, on_device(): lax.all_to_all(downs.reshape(kv, quarter, 2 * rows), 'kv', 0, 0, tiled=True)  17.2 us
    all_to_all x1, blocking collectives, on_device(): lax.all_to_all(middle, 'kv', 0, 0, tiled=True)  17.2 us
    pallas_call x10, Pallas kernels, call(): pl.pallas_call(kernel, out_shape=outs if many else outs[0], in_specs=[sme...  13.7 us
    all_to_all x1, starting transfers between devices, on_device(): arrived = lax.all_to_all(sends, 'kv', 0, 0, tiled=True)  11.1 us
    all_to_all x1, waiting for transfers between devices, on_device(): arrived = lax.all_to_all(sends, 'kv', 0, 0, tiled=True)  10.9 us
    all_to_all x1, waiting for transfers between devices, on_device(): cells = lax.all_to_all(cell, 'kv', 0, 0, tiled=True)  9.38 us
    psum x1, blocking collectives, on_device(): packed = lax.psum(padded, 'tp')  9 us
    all_to_all x1, starting transfers between devices, on_device(): cells = lax.all_to_all(cell, 'kv', 0, 0, tiled=True)  7.03 us
  transfers between devices with their start and end apart: 4, of which 4 were waited for; matrix products, arithmetic and copies ran while one was open for 0% of the time, Pallas kernels for 5%

profile of v4, /device:TPU:1, one launch (start us, length us, event | category | flops | bytes accessed | tf_op | source)
XLA Modules:
  0.0 113.5 jit_solution(10696317789284684963)
XLA Ops:
  0.6 1.2 %shard_map.183 = (bf16[32,128]{1,0:T(8,128)(2,1)S(1)}, bf16[32,64]{1,0:T(8,128)(2,1)S(1)}, f32[32,128]{1,0:T(8,128)S(1)}, bf16[64,1024]{1,0:T(8,128)(2,1)S(1)}, ...) custom-call(s32[1]{0:T(128)} %bitcast.1.kv_pos, ...), custom_call_target="tpu_custom_call" | custom-call | tf_op jit(solution)/shard_map/pallas_call | solution.py:291
  1.8 9.0 %psum.14.packed = bf16[32,128]{1,0:T(8,128)(2,1)S(1)} all-reduce(bf16[32,128]{1,0:T(8,128)(2,1)S(1)} %get-tuple-element.35), channel_id=1, replica_groups=mesh['dp'=4,'kv'=64,'tp'=2] {'tp'}, use_global_device_ids=true, to_apply=%region_0.0 | all-reduce | flops 4096 | bytes 16384 | tf_op jit(solution)/shard_map/psum | solution.py:351
  10.8 1.7 %shard_map.184 = (bf16[64,40,128]{2,1,0:T(8,128)(2,1)}, f32[8,128]{1,0:T(8,128)S(1)}, f32[1,8]{1,0:T(1,128)S(1)}, f32[1,16]{1,0:T(1,128)S(1)}, f32[1,16]{1,0:T(1,128)S(1)}) custom-call(s32[1]{0:T(128)} %bitcast.1.kv_pos, bf16[32,128]{1,0:T(8,128)(2,1)S(1)} %psum.14.packed, f32[32,128]{1,0:T(8,128)S(1)} %get-tuple-element.36.gain, ...), custom_call_target="tpu_custom_call" | custom-call | tf_op jit(solution)/shard_map/pallas_call | solution.py:291
  12.5 11.1 %all-to-all-start = ((bf16[64,40,128]{2,1,0:T(8,128)(2,1)}), bf16[64,40,128]{2,1,0:T(8,128)(2,1)S(1)}, u32[]{:S(2)}, u32[]{:S(2)}) async-start(bf16[64,40,128]{2,1,0:T(8,128)(2,1)} %get-tuple-element.42), calls=%async_computation | async-start | bytes 1310720 | tf_op jit(solution)/shard_map/all_to_all | solution.py:380
  23.6 0.2 reshape.36
  23.9 0.1 reshape.37.gain
  24.0 1.2 %copy-done.1 = bf16[128,4096]{1,0:T(8,128)(2,1)S(1)} copy-done((bf16[128,4096]{1,0:T(8,128)(2,1)S(1)}, bf16[128,4096]{1,0:T(8,128)(2,1)}, u32[]{:S(2)}) %copy-start.1) | copy-done | bytes 1048600
  25.2 2.4 %shard_map.185 = (bf16[2048,256]{1,0:T(8,128)(2,1)S(1)}, bf16[2048,256]{1,0:T(8,128)(2,1)}, bf16[64,2048]{1,0:T(8,128)(2,1)S(1)}) custom-call(s32[1]{0:T(128)} %bitcast.tp_pos, bf16[64,2,2,16,128]{4,3,2,1,0:T(8,128)(2,1)S(1)} %bitcast.20, f32[4,1024]{1,0:T(4,128)S(1)} %reshape.37.gain, bf16[128,4096]{1,0:T(8,128)(2,1)S(1)} %copy-done.1, ...), custom_call_target="tpu_custom_call" | custom-call | tf_op jit(solution)/shard_map/pallas_call | solution.py:291
  27.7 2.5 %collective-permute-start = (bf16[2048,256]{1,0:T(8,128)(2,1)}, bf16[2048,256]{1,0:T(8,128)(2,1)S(1)}, u32[]{:S(2)}, u32[]{:S(2)}) collective-permute-start(bf16[2048,256]{1,0:T(8,128)(2,1)} %get-tuple-element.44), channel_id=1, source_target_pairs={{0,1},{1,0},{2,3},{3,2},{4,5},{5,4},{6,7},{7,6},{8,9},{9,8},{10,11... | collective-permute-start | bytes 3145736 | tf_op jit(solution)/shard_map/ppermute | solution.py:398
  30.2 2.5 %collective-permute-done.other = bf16[2048,256]{1,0:T(8,128)(2,1)S(1)} collective-permute-done((bf16[2048,256]{1,0:T(8,128)(2,1)}, bf16[2048,256]{1,0:T(8,128)(2,1)S(1)}, u32[]{:S(2)}, u32[]{:S(2)}) %collective-permute-start) | collective-permute-done | bytes 1048608 | tf_op jit(solution)/shard_map/ppermute | solution.py:398
  32.7 10.9 %all-to-all-done.arrived = bf16[64,40,128]{2,1,0:T(8,128)(2,1)S(1)} async-done(((bf16[64,40,128]{2,1,0:T(8,128)(2,1)}), bf16[64,40,128]{2,1,0:T(8,128)(2,1)S(1)}, u32[]{:S(2)}, u32[]{:S(2)}) %all-to-all-start) | async-done | bytes 655392 | tf_op jit(solution)/shard_map/all_to_all | solution.py:380
  43.5 2.9 %shard_map.186 = (bf16[64,16,128]{2,1,0:T(8,128)(2,1)}, f32[8,128]{1,0:T(8,128)S(1)}, f32[8,256]{1,0:T(8,128)S(1)}, f32[8,128]{1,0:T(8,128)S(1)}, f32[8,128]{1,0:T(8,128)}, /*index=5*/f32[1,8]{1,0:T(1,128)}) custom-call(s32[1]{0:T(128)} %bitcast.tp_pos, bf16[64,40,128]{2,1,0:T(8,128)(2,1)S(1)} %all-to-all-done.arrived, ...), custom_call_target="tpu_custom_call" | custom-call | tf_op jit(solution)/shard_map/pallas_call | solution.py:291
  46.5 7.0 %all-to-all-start.1 = ((bf16[64,16,128]{2,1,0:T(8,128)(2,1)}), bf16[64,16,128]{2,1,0:T(8,128)(2,1)S(1)}, u32[]{:S(2)}, u32[]{:S(2)}) async-start(bf16[64,16,128]{2,1,0:T(8,128)(2,1)} %get-tuple-element.50), calls=%async_computation.1 | async-start | bytes 524288 | tf_op jit(solution)/shard_map/all_to_all | solution.py:422
  53.5 3.2 %shard_map.187 = f32[8,256,128]{2,1,0:T(8,128)} custom-call(f32[8,128]{1,0:T(8,128)S(1)} %get-tuple-element.51.keys, f32[8,256]{1,0:T(8,128)S(1)} %get-tuple-element.52.vals, f32[8,128]{1,0:T(8,128)S(1)} %get-tuple-element.53.keeps, f32[8,256,128]{2,1,0:T(8,128)} %bitcast.24), custom_call_target="tpu_custom_call" | custom-call | tf_op jit(solution)/shard_map/pallas_call | solution.py:291
  56.7 9.4 %all-to-all-done.1.arrived = bf16[64,16,128]{2,1,0:T(8,128)(2,1)S(1)} async-done(((bf16[64,16,128]{2,1,0:T(8,128)(2,1)}), bf16[64,16,128]{2,1,0:T(8,128)(2,1)S(1)}, u32[]{:S(2)}, u32[]{:S(2)}) %all-to-all-start.1) | async-done | bytes 262176 | tf_op jit(solution)/shard_map/all_to_all | solution.py:422
  66.1 0.4 shard_map.188
  66.4 5.4 %psum.15.both = bf16[32,128]{1,0:T(8,128)(2,1)S(1)} all-reduce(bf16[32,128]{1,0:T(8,128)(2,1)S(1)} %get-tuple-element.57), channel_id=1, replica_groups=mesh['dp'=4,'kv'=64,'tp'=2] {'tp'}, use_global_device_ids=true, to_apply=%region_1.0 | all-reduce | flops 4096 | bytes 16384 | tf_op jit(solution)/shard_map/psum | solution.py:452
  72.0 17.2 %all_to_all.20 = bf16[64,16,128]{2,1,0:T(8,128)(2,1)S(1)} all-to-all(bf16[64,16,128]{2,1,0:T(8,128)(2,1)S(1)} %get-tuple-element.59), channel_id=1, replica_groups=mesh['dp'=4,'kv'=64,'tp'=2] {'kv'}, dimensions={0} | all-to-all | bytes 524288 | tf_op jit(solution)/shard_map/all_to_all | solution.py:456
  89.1 0.6 shard_map.190.near
  89.7 4.4 %collective-permute-start.1 = (f32[136,128]{1,0:T(8,128)S(1)}, f32[136,128]{1,0:T(8,128)S(1)}, u32[]{:S(2)}, u32[]{:S(2)}) collective-permute-start(f32[136,128]{1,0:T(8,128)S(1)} %shard_map.190.near), channel_id=1, source_target_pairs={{0,1},{1,0},{2,3},{3,2},{4,5},{5,4},{6,7},{7,6},{8,9},{9,8},{10,11... | collective-permute-start | bytes 208904 | tf_op jit(solution)/shard_map/ppermute | solution.py:463
  94.1 0.9 collective-permute-done.1.far_sums
  95.0 0.5 shard_map.191
  95.5 17.2 %all_to_all.21.back = bf16[64,16,128]{2,1,0:T(8,128)(2,1)S(1)} all-to-all(bf16[64,16,128]{2,1,0:T(8,128)(2,1)S(1)} %bitcast.21), channel_id=1, replica_groups=mesh['dp'=4,'kv'=64,'tp'=2] {'kv'}, dimensions={0} | all-to-all | bytes 524288 | tf_op jit(solution)/shard_map/all_to_all | solution.py:468
  112.8 0.8 shard_map.192
  (7 shorter events, 0.1 us)
Async XLA Ops:
  12.5 11.5 %copy-start = (bf16[4096,128]{1,0:T(8,128)(2,1)S(1)}, bf16[4096,128]{1,0:T(8,128)(2,1)}, u32[]{:S(2)}) copy-start(bf16[4096,128]{1,0:T(8,128)(2,1)} %param.30) | copy-start | bytes 3145732
  12.5 11.1 %copy-start.2 = (f32[4096]{0:T(1024)S(1)}, f32[4096]{0:T(1024)}, u32[]{:S(2)}) copy-start(f32[4096]{0:T(1024)} %param.29) | copy-start | bytes 49156
  12.5 31.0 %all-to-all-start = ((bf16[64,40,128]{2,1,0:T(8,128)(2,1)}), bf16[64,40,128]{2,1,0:T(8,128)(2,1)S(1)}, u32[]{:S(2)}, u32[]{:S(2)}) async-start(bf16[64,40,128]{2,1,0:T(8,128)(2,1)} %get-tuple-element.42), calls=%async_computation | async-start | bytes 1310720 | tf_op jit(solution)/shard_map/all_to_all | solution.py:380
  24.0 1.2 %copy-start.1 = (bf16[128,4096]{1,0:T(8,128)(2,1)S(1)}, bf16[128,4096]{1,0:T(8,128)(2,1)}, u32[]{:S(2)}) copy-start(bf16[128,4096]{1,0:T(8,128)(2,1)} %w_down.1) | copy-start | bytes 3145732
  27.7 5.0 %collective-permute-start = (bf16[2048,256]{1,0:T(8,128)(2,1)}, bf16[2048,256]{1,0:T(8,128)(2,1)S(1)}, u32[]{:S(2)}, u32[]{:S(2)}) collective-permute-start(bf16[2048,256]{1,0:T(8,128)(2,1)} %get-tuple-element.44), channel_id=1, source_target_pairs={{0,1},{1,0},{2,3},{3,2},{4,5},{5,4},{6,7},{7,6},{8,9},{9,8},{10,11... | collective-permute-start | bytes 3145736 | tf_op jit(solution)/shard_map/ppermute | solution.py:398
  46.5 19.6 %all-to-all-start.1 = ((bf16[64,16,128]{2,1,0:T(8,128)(2,1)}), bf16[64,16,128]{2,1,0:T(8,128)(2,1)S(1)}, u32[]{:S(2)}, u32[]{:S(2)}) async-start(bf16[64,16,128]{2,1,0:T(8,128)(2,1)} %get-tuple-element.50), calls=%async_computation.1 | async-start | bytes 524288 | tf_op jit(solution)/shard_map/all_to_all | solution.py:422
  89.7 5.3 %collective-permute-start.1 = (f32[136,128]{1,0:T(8,128)S(1)}, f32[136,128]{1,0:T(8,128)S(1)}, u32[]{:S(2)}, u32[]{:S(2)}) collective-permute-start(f32[136,128]{1,0:T(8,128)S(1)} %shard_map.190.near), channel_id=1, source_target_pairs={{0,1},{1,0},{2,3},{3,2},{4,5},{5,4},{6,7},{7,6},{8,9},{9,8},{10,11... | collective-permute-start | bytes 208904 | tf_op jit(solution)/shard_map/ppermute | solution.py:463

commit v5 on v4

--- a/solution.py
+++ b/solution.py
@@ -10,7 +10,7 @@
 DQK = 128
 LANES = 128
 NORM_EPS = 1e-06
-PITCH = 40
+STACK = 34
 
 F32 = jnp.float32
 BF16 = jnp.bfloat16
@@ -58,6 +58,10 @@
     wide = packed[...].astype(F32)
     x = jnp.concatenate([wide[:, :n].T, wide[:, n:].T], axis=1)
     twice = jnp.concatenate([x, x], axis=1)
+
+    def put(at, tile):
+        rows[pl.ds(at // 2 * 2 * n + at % 2, n, stride=2), :] = tile
+
     lane = lax.broadcasted_iota(jnp.int32, twice.shape, 1)
     mine = (lane // n) == odd
     scaled = jnp.where(mine, twice * gain[pl.ds(block, 1), :], 0.0)
@@ -72,8 +76,8 @@
     sums = jnp.where(lane >= n, jnp.broadcast_to(squares, sums.shape), sums)
     low = ((lane >= n // 2) & (lane < n)) | (lane == n + 1)
     sums = jnp.where(low, sums - sums.astype(BF16).astype(F32), sums)
-    for at in range(32, 40):
-        rows[pl.ds(at, n, stride=PITCH), :] = sums
+    for at in range(32, STACK):
+        put(at, sums)
 
     def place(w, first, step):
         cols = w.shape[1]
@@ -82,24 +86,27 @@
             for half in range(2):
                 tile = c // LANES + half
                 at = first + (tile if step == 1 else (tile % 2) * 8 + tile // 2)
-                rows[pl.ds(at, n, stride=PITCH), :] = part[:, half * LANES : (half + 1) * LANES]
+                put(at, part[:, half * LANES : (half + 1) * LANES])
 
     place(wq, 0, 1)
     place(wk, 8, 1)
     place(wv, 16, 2)
-    for r in range(n):
-        out[r] = rows[r * PITCH : r * PITCH + PITCH, :].astype(BF16)
+    for pair in range(STACK // 2):
+        part = rows[pair * 2 * n : (pair + 1) * 2 * n, :].astype(BF16)
+        out[:, :, pair * LANES : (pair + 1) * LANES] = part.reshape(n, 2, LANES)
     for copy in copies:
         copy.wait()
 
 
-def cell_kernel(tp_pos, arrived, normalizer, stab, ibias, fbias, memory_in, *rest):
-    out, keys, vals, keeps, norm_out, stab_out, memory, sems = rest
+def hold_kernel(memory, after, out, sem):
+    copy = pltpu.make_async_copy(memory, out, sem)
+    copy.start()
+    copy.wait()
+
+
+def cell_kernel(tp_pos, arrived, memory, normalizer, stab, ibias, fbias, out, keys, vals, keeps, norm_out, stab_out):
     tp = tp_pos[0]
     heads = memory.shape[0]
-    loads = [pltpu.make_async_copy(memory_in.at[h], memory.at[h], sems.at[h]) for h in range(heads)]
-    for load in loads:
-        load.start()
     pad = jnp.zeros((1, LANES - 32), F32)
     bias = jnp.concatenate([ibias[...], fbias[...], pad], axis=1)
     old_stab = jnp.concatenate([stab[...], jnp.zeros((1, LANES - 8), F32)], axis=1)
@@ -110,10 +117,14 @@
             acc = acc + arrived[i * 8 + j].astype(F32)
         return acc
 
-    acc = lax.fori_loop(0, count // 8, add, jnp.zeros((PITCH, LANES), F32))
+    acc = lax.fori_loop(0, count // 8, add, jnp.zeros(arrived.shape[1:], F32))
+
+    def stack(first):
+        return jnp.concatenate([acc[:, j * LANES : (j + 1) * LANES] for j in range(first // 2, first // 2 + 4)], axis=0)
+
     lane = lax.broadcasted_iota(jnp.int32, (8, LANES), 1)
     sub = lax.broadcasted_iota(jnp.int32, (8, LANES), 0)
-    extra = jnp.broadcast_to(acc[32:33], (8, LANES))
+    extra = jnp.broadcast_to(acc[0:1, 16 * LANES :], (8, LANES))
     squares = jnp.sum(jnp.where((lane == 64) | (lane == 65), extra, 0.0), axis=1, keepdims=True)
     scale = lax.rsqrt(squares * (1.0 / 4096.0) + NORM_EPS)
     gates = extra * scale + bias
@@ -127,14 +138,13 @@
     keep = jnp.exp(carried - new)
     fresh = jnp.exp(igate - new)
     stab_out[...] = jnp.sum(jnp.where(lane == sub, new, 0.0), axis=0, keepdims=True)[:, :8]
-    q = acc[0:8] * (scale * DQK ** (-0.5))
-    k = acc[8:16] * scale
-    v = jnp.concatenate([acc[16:24], acc[24:32]], axis=1) * scale
+    q = stack(0) * (scale * DQK ** (-0.5))
+    k = stack(8) * scale
+    v = jnp.concatenate([stack(16), stack(24)], axis=1) * scale
     q_both = jnp.concatenate(split(q), axis=0)
     sub2 = lax.broadcasted_iota(jnp.int32, (8, DV), 0)
     recall = jnp.zeros((8, DV), F32)
     for h in range(heads):
-        loads[h].wait()
         part = lax.dot_general(q_both, memory[h].astype(BF16), NT, preferred_element_type=F32)
         recall = jnp.where(sub2 == h, part[:8] + part[8:], recall)
     match = jnp.sum(q * k, axis=1, keepdims=True)
@@ -353,7 +363,7 @@
     sends, state_norm, old_stab, ibias, fbias = call(
         project_kernel,
         [
-            ((rows, PITCH, LANES), BF16),
+            ((rows, 2, STACK // 2 * LANES), BF16),
             (normalizer.shape[1:], F32),
             (stabilizer.shape, F32),
             ((1, igate_bias.shape[0]), F32),
@@ -375,7 +385,7 @@
         far=4,
         fetched=4,
         away=(0,),
-        scratch=[pltpu.VMEM((rows * PITCH, LANES), F32), pltpu.SemaphoreType.DMA((4,))],
+        scratch=[pltpu.VMEM((rows * STACK, LANES), F32), pltpu.SemaphoreType.DMA((4,))],
     )
     arrived = lax.all_to_all(sends, "kv", 0, 0, tiled=True)
     hidden = w_up.shape[1]
@@ -392,11 +402,19 @@
         scalars=1,
         far=1,
         fetched=1,
-        away=(1,),
+        away=(0, 1),
         scratch=[pltpu.VMEM((kv, 2, 2, quarter, hidden), BF16), pltpu.SemaphoreType.DMA],
     )
     other = lax.ppermute(send, "tp", [(0, 1), (1, 0)])
-    arrived, keep, other = lax.optimization_barrier((arrived, keep, other))
+    state = pl.pallas_call(
+        hold_kernel,
+        out_shape=pltpu.VMEM(memory.shape[1:], F32),
+        in_specs=[any_space, any_space],
+        out_specs=any_space,
+        scratch_shapes=[pltpu.SemaphoreType.DMA],
+        compiler_params=pltpu.CompilerParams(vmem_limit_bytes=1024 * 1024),
+    )(pltpu.with_memory_space_constraint(memory[0], pltpu.HBM), other)
+    arrived, keep, other, state = lax.optimization_barrier((arrived, keep, other, state))
     cell, keys, vals, keeps, new_normalizer, new_stabilizer = call(
         cell_kernel,
         [
@@ -409,15 +427,13 @@
         ],
         tp_pos,
         arrived,
+        state,
         state_norm,
         old_stab,
         ibias,
         fbias,
-        memory[0],
         scalars=1,
-        far=1,
         away=(0, 4, 5),
-        scratch=[pltpu.VMEM(memory.shape[1:], F32), pltpu.SemaphoreType.DMA((8,))],
     )
     cells = lax.all_to_all(cell, "kv", 0, 0, tiled=True)
     new_memory = call(

time: 115 us -> 112 us (0.974)
  waiting for transfers between devices: 23.6 us -> 21.2 us
  local copies, waits for them, and re-layouts: 1.57 us -> 0.36 us
    all_to_all x1, waiting for transfers between devices: 10.9 us -> 8.53 us  [on_device(): arrived = lax.all_to_all(sends, 'kv', 0, 0, tiled=True)]
    pallas_call x0 -> x1, Pallas kernels: none -> 1.23 us  [on_device(): pl.pallas_call(hold_kernel, out_shape=pltpu.VMEM(memory.shape[1:], F32),...]
    unnamed x6 -> x8, local copies, waits for them, and re-layouts: 1.23 us -> 0.02 us
  transfers between devices with their start and end apart: 4 -> 4, of which waited for: 4 -> 4; matrix products, arithmetic and copies ran while one was open for 0% -> 0% of each run, Pallas kernels for 5% -> 7%
where the time goes in v5:
time: 112 us; the launch traced here: 110 us
  blocking collectives  49 us (44%)
  starting transfers between devices  24.6 us (22%)
  waiting for transfers between devices  21.2 us (19%)
  Pallas kernels  14.2 us (13%)
    all_to_all x1, blocking collectives, on_device(): lax.all_to_all(middle, 'kv', 0, 0, tiled=True)  17.2 us
    all_to_all x1, blocking collectives, on_device(): lax.all_to_all(downs.reshape(kv, quarter, 2 * rows), 'kv', 0, 0, tiled=True)  17.2 us
    pallas_call x10, Pallas kernels, call(): pl.pallas_call(kernel, out_shape=outs if many else outs[0], in_specs=[sme...  12.9 us
    all_to_all x1, starting transfers between devices, on_device(): arrived = lax.all_to_all(sends, 'kv', 0, 0, tiled=True)  11 us
    all_to_all x1, waiting for transfers between devices, on_device(): cells = lax.all_to_all(cell, 'kv', 0, 0, tiled=True)  9.32 us
    psum x1, blocking collectives, on_device(): packed = lax.psum(padded, 'tp')  9 us
    all_to_all x1, waiting for transfers between devices, on_device(): arrived = lax.all_to_all(sends, 'kv', 0, 0, tiled=True)  8.53 us
    all_to_all x1, starting transfers between devices, on_device(): cells = lax.all_to_all(cell, 'kv', 0, 0, tiled=True)  6.72 us
  transfers between devices with their start and end apart: 4, of which 4 were waited for; matrix products, arithmetic and copies ran while one was open for 0% of the time, Pallas kernels for 7%

profile of v5, /device:TPU:1, one launch (start us, length us, event | category | flops | bytes accessed | tf_op | source)
XLA Modules:
  0.0 110.1 jit_solution(343719204977629641)
XLA Ops:
  0.6 1.2 %shard_map.183 = (bf16[32,128]{1,0:T(8,128)(2,1)S(1)}, bf16[32,64]{1,0:T(8,128)(2,1)S(1)}, f32[32,128]{1,0:T(8,128)S(1)}, bf16[64,1024]{1,0:T(8,128)(2,1)S(1)}, ...) custom-call(s32[1]{0:T(128)} %bitcast.1.kv_pos, ...), custom_call_target="tpu_custom_call" | custom-call | tf_op jit(solution)/shard_map/pallas_call | solution.py:301
  1.8 9.0 %psum.14.packed = bf16[32,128]{1,0:T(8,128)(2,1)S(1)} all-reduce(bf16[32,128]{1,0:T(8,128)(2,1)S(1)} %get-tuple-element.36), channel_id=1, replica_groups=mesh['dp'=4,'kv'=64,'tp'=2] {'tp'}, use_global_device_ids=true, to_apply=%region_0.0 | all-reduce | flops 4096 | bytes 16384 | tf_op jit(solution)/shard_map/psum | solution.py:361
  10.8 2.1 %shard_map.184 = (bf16[64,2,2176]{2,1,0:T(2,128)(2,1)}, f32[8,128]{1,0:T(8,128)S(1)}, f32[1,8]{1,0:T(1,128)S(1)}, f32[1,16]{1,0:T(1,128)S(1)}, f32[1,16]{1,0:T(1,128)S(1)}) custom-call(s32[1]{0:T(128)} %bitcast.1.kv_pos, bf16[32,128]{1,0:T(8,128)(2,1)S(1)} %psum.14.packed, f32[32,128]{1,0:T(8,128)S(1)} %get-tuple-element.37.gain, ...), custom_call_target="tpu_custom_call" | custom-call | tf_op jit(solution)/shard_map/pallas_call | solution.py:301
  12.9 11.0 %all-to-all-start = ((bf16[64,2,2176]{2,1,0:T(2,128)(2,1)}), bf16[64,2,2176]{2,1,0:T(2,128)(2,1)S(1)}, u32[]{:S(2)}, u32[]{:S(2)}) async-start(bf16[64,2,2176]{2,1,0:T(2,128)(2,1)} %get-tuple-element.43), calls=%async_computation | async-start | bytes 1114112 | tf_op jit(solution)/shard_map/all_to_all | solution.py:390
  23.9 0.2 reshape.36
  24.2 0.1 reshape.37.gain
  24.3 3.0 %shard_map.185 = (bf16[2048,256]{1,0:T(8,128)(2,1)}, bf16[2048,256]{1,0:T(8,128)(2,1)}, bf16[64,2048]{1,0:T(8,128)(2,1)S(1)}) custom-call(s32[1]{0:T(128)} %bitcast.tp_pos, bf16[64,2,2,16,128]{4,3,2,1,0:T(8,128)(2,1)S(1)} %bitcast.20, f32[4,1024]{1,0:T(4,128)S(1)} %reshape.37.gain, bf16[128,4096]{1,0:T(8,128)(2,1)S(1)} %copy-done.2, bf16[64,2048]{1,0:T(8,128)(2,1)} %bitcast.27), custom_call_target="tpu_custom_call" | custom-call | tf_op jit(solution)/shard_map/pallas_call | solution.py:301
  27.3 2.5 %collective-permute-start = (bf16[2048,256]{1,0:T(8,128)(2,1)}, bf16[2048,256]{1,0:T(8,128)(2,1)S(1)}, u32[]{:S(2)}, u32[]{:S(2)}) collective-permute-start(bf16[2048,256]{1,0:T(8,128)(2,1)} %get-tuple-element.45), channel_id=1, source_target_pairs={{0,1},{1,0},{2,3},{3,2},{4,5},{5,4},{6,7},{7,6},{8,9},{9,8},{10,11... | collective-permute-start | bytes 3145736 | tf_op jit(solution)/shard_map/ppermute | solution.py:408
  29.8 2.5 %collective-permute-done.after.other = bf16[2048,256]{1,0:T(8,128)(2,1)S(1)} collective-permute-done((bf16[2048,256]{1,0:T(8,128)(2,1)}, bf16[2048,256]{1,0:T(8,128)(2,1)S(1)}, u32[]{:S(2)}, u32[]{:S(2)}) %collective-permute-start) | collective-permute-done | bytes 1048608 | tf_op jit(solution)/shard_map/ppermute | solution.py:408
  32.3 1.2 %shard_map.186.memory = f32[8,256,128]{2,1,0:T(8,128)S(1)} custom-call(f32[8,256,128]{2,1,0:T(8,128)} %bitcast.23, bf16[2048,256]{1,0:T(8,128)(2,1)S(1)} %collective-permute-done.after.other), custom_call_target="tpu_custom_call" | custom-call | tf_op jit(solution)/shard_map/pallas_call | solution.py:409
  33.5 8.5 %all-to-all-done.arrived = bf16[64,2,2176]{2,1,0:T(2,128)(2,1)S(1)} async-done(((bf16[64,2,2176]{2,1,0:T(2,128)(2,1)}), bf16[64,2,2176]{2,1,0:T(2,128)(2,1)S(1)}, u32[]{:S(2)}, u32[]{:S(2)}) %all-to-all-start) | async-done | bytes 557088 | tf_op jit(solution)/shard_map/all_to_all | solution.py:390
  42.1 1.2 %shard_map.187 = (bf16[64,16,128]{2,1,0:T(8,128)(2,1)}, f32[8,128]{1,0:T(8,128)S(1)}, f32[8,256]{1,0:T(8,128)S(1)}, f32[8,128]{1,0:T(8,128)S(1)}, f32[8,128]{1,0:T(8,128)}, /*index=5*/f32[1,8]{1,0:T(1,128)}) custom-call(s32[1]{0:T(128)} %bitcast.tp_pos, bf16[64,2,2176]{2,1,0:T(2,128)(2,1)S(1)} %all-to-all-done.arrived, ...), custom_call_target="tpu_custom_call" | custom-call | tf_op jit(solution)/shard_map/pallas_call | solution.py:301
  43.3 6.7 %all-to-all-start.1 = ((bf16[64,16,128]{2,1,0:T(8,128)(2,1)}), bf16[64,16,128]{2,1,0:T(8,128)(2,1)S(1)}, u32[]{:S(2)}, u32[]{:S(2)}) async-start(bf16[64,16,128]{2,1,0:T(8,128)(2,1)} %get-tuple-element.52), calls=%async_computation.1 | async-start | bytes 524288 | tf_op jit(solution)/shard_map/all_to_all | solution.py:438
  50.0 3.2 %shard_map.188 = f32[8,256,128]{2,1,0:T(8,128)} custom-call(f32[8,128]{1,0:T(8,128)S(1)} %get-tuple-element.53.keys, f32[8,256]{1,0:T(8,128)S(1)} %get-tuple-element.54.vals, f32[8,128]{1,0:T(8,128)S(1)} %get-tuple-element.55.keeps, f32[8,256,128]{2,1,0:T(8,128)} %bitcast.24), custom_call_target="tpu_custom_call" | custom-call | tf_op jit(solution)/shard_map/pallas_call | solution.py:301
  53.2 9.3 %all-to-all-done.1.arrived = bf16[64,16,128]{2,1,0:T(8,128)(2,1)S(1)} async-done(((bf16[64,16,128]{2,1,0:T(8,128)(2,1)}), bf16[64,16,128]{2,1,0:T(8,128)(2,1)S(1)}, u32[]{:S(2)}, u32[]{:S(2)}) %all-to-all-start.1) | async-done | bytes 262176 | tf_op jit(solution)/shard_map/all_to_all | solution.py:438
  62.5 0.4 shard_map.189
  62.9 5.5 %psum.15.both = bf16[32,128]{1,0:T(8,128)(2,1)S(1)} all-reduce(bf16[32,128]{1,0:T(8,128)(2,1)S(1)} %get-tuple-element.59), channel_id=1, replica_groups=mesh['dp'=4,'kv'=64,'tp'=2] {'tp'}, use_global_device_ids=true, to_apply=%region_1.0 | all-reduce | flops 4096 | bytes 16384 | tf_op jit(solution)/shard_map/psum | solution.py:468
  68.5 17.2 %all_to_all.20 = bf16[64,16,128]{2,1,0:T(8,128)(2,1)S(1)} all-to-all(bf16[64,16,128]{2,1,0:T(8,128)(2,1)S(1)} %get-tuple-element.61), channel_id=1, replica_groups=mesh['dp'=4,'kv'=64,'tp'=2] {'kv'}, dimensions={0} | all-to-all | bytes 524288 | tf_op jit(solution)/shard_map/all_to_all | solution.py:472
  85.8 0.6 shard_map.191.near
  86.4 4.4 %collective-permute-start.1 = (f32[136,128]{1,0:T(8,128)S(1)}, f32[136,128]{1,0:T(8,128)S(1)}, u32[]{:S(2)}, u32[]{:S(2)}) collective-permute-start(f32[136,128]{1,0:T(8,128)S(1)} %shard_map.191.near), channel_id=1, source_target_pairs={{0,1},{1,0},{2,3},{3,2},{4,5},{5,4},{6,7},{7,6},{8,9},{9,8},{10,11... | collective-permute-start | bytes 208904 | tf_op jit(solution)/shard_map/ppermute | solution.py:479
  90.7 0.9 collective-permute-done.1.far_sums
  91.6 0.5 shard_map.192
  92.1 17.2 %all_to_all.21.back = bf16[64,16,128]{2,1,0:T(8,128)(2,1)S(1)} all-to-all(bf16[64,16,128]{2,1,0:T(8,128)(2,1)S(1)} %bitcast.21), channel_id=1, replica_groups=mesh['dp'=4,'kv'=64,'tp'=2] {'kv'}, dimensions={0} | all-to-all | bytes 524288 | tf_op jit(solution)/shard_map/all_to_all | solution.py:484
  109.3 0.8 shard_map.193
  (10 shorter events, 0.1 us)
Async XLA Ops:
  1.8 22.1 %copy-start.3 = (f32[4096]{0:T(1024)S(1)}, f32[4096]{0:T(1024)}, u32[]{:S(2)}) copy-start(f32[4096]{0:T(1024)} %param.29) | copy-start | bytes 49156
  10.8 13.5 %copy-start.1 = (bf16[4096,128]{1,0:T(8,128)(2,1)S(1)}, bf16[4096,128]{1,0:T(8,128)(2,1)}, u32[]{:S(2)}) copy-start(bf16[4096,128]{1,0:T(8,128)(2,1)} %param.30) | copy-start | bytes 3145732
  10.8 13.5 %copy-start.2 = (bf16[128,4096]{1,0:T(8,128)(2,1)S(1)}, bf16[128,4096]{1,0:T(8,128)(2,1)}, u32[]{:S(2)}) copy-start(bf16[128,4096]{1,0:T(8,128)(2,1)} %w_down.1) | copy-start | bytes 3145732
  12.9 29.1 %all-to-all-start = ((bf16[64,2,2176]{2,1,0:T(2,128)(2,1)}), bf16[64,2,2176]{2,1,0:T(2,128)(2,1)S(1)}, u32[]{:S(2)}, u32[]{:S(2)}) async-start(bf16[64,2,2176]{2,1,0:T(2,128)(2,1)} %get-tuple-element.43), calls=%async_computation | async-start | bytes 1114112 | tf_op jit(solution)/shard_map/all_to_all | solution.py:390
  27.3 5.0 %collective-permute-start = (bf16[2048,256]{1,0:T(8,128)(2,1)}, bf16[2048,256]{1,0:T(8,128)(2,1)S(1)}, u32[]{:S(2)}, u32[]{:S(2)}) collective-permute-start(bf16[2048,256]{1,0:T(8,128)(2,1)} %get-tuple-element.45), channel_id=1, source_target_pairs={{0,1},{1,0},{2,3},{3,2},{4,5},{5,4},{6,7},{7,6},{8,9},{9,8},{10,11... | collective-permute-start | bytes 3145736 | tf_op jit(solution)/shard_map/ppermute | solution.py:408
  43.3 19.2 %all-to-all-start.1 = ((bf16[64,16,128]{2,1,0:T(8,128)(2,1)}), bf16[64,16,128]{2,1,0:T(8,128)(2,1)S(1)}, u32[]{:S(2)}, u32[]{:S(2)}) async-start(bf16[64,16,128]{2,1,0:T(8,128)(2,1)} %get-tuple-element.52), calls=%async_computation.1 | async-start | bytes 524288 | tf_op jit(solution)/shard_map/all_to_all | solution.py:438
  53.2 32.6 %copy-start = (bf16[2048,256]{1,0:T(8,128)(2,1)S(1)}, bf16[2048,256]{1,0:T(8,128)(2,1)}, u32[]{:S(2)}) copy-start(bf16[2048,256]{1,0:T(8,128)(2,1)} %get-tuple-element.62.keep) | copy-start | bytes 3145732
  86.4 5.3 %collective-permute-start.1 = (f32[136,128]{1,0:T(8,128)S(1)}, f32[136,128]{1,0:T(8,128)S(1)}, u32[]{:S(2)}, u32[]{:S(2)}) collective-permute-start(f32[136,128]{1,0:T(8,128)S(1)} %shard_map.191.near), channel_id=1, source_target_pairs={{0,1},{1,0},{2,3},{3,2},{4,5},{5,4},{6,7},{7,6},{8,9},{9,8},{10,11... | collective-permute-start | bytes 208904 | tf_op jit(solution)/shard_map/ppermute | solution.py:479

commit v6 on v5

--- a/solution.py
+++ b/solution.py
@@ -48,7 +48,7 @@
 
 
 def project_kernel(kv_pos, packed, gain, wq, wk, wv, wig, wfg, *rest):
-    sources, out, held, rows, sems = rest[:4], rest[4], rest[5:9], rest[9], rest[10]
+    sources, held, out, rows, ready, sems = rest[:4], rest[4:8], rest[8], rest[9], rest[10], rest[11]
     copies = [pltpu.make_async_copy(src, dst, sems.at[i]) for i, (src, dst) in enumerate(zip(sources, held))]
     for copy in copies:
         copy.start()
@@ -79,21 +79,35 @@
     for at in range(32, STACK):
         put(at, sums)
 
-    def place(w, first, step):
-        cols = w.shape[1]
-        for c in range(0, cols, 256):
+    def send(first, pairs):
+        for pair in range(first, first + pairs):
+            part = rows[pair * 2 * n : (pair + 1) * 2 * n, :].astype(BF16)
+            ready[:, :, pair * LANES : (pair + 1) * LANES] = part.reshape(n, 2, LANES)
+        lanes = pl.ds(first * LANES, pairs * LANES)
+        copy = pltpu.make_async_copy(ready.at[:, :, lanes], out.at[:, :, lanes], sems.at[len(copies)])
+        copy.start()
+        copies.append(copy)
+
+    def place(w, first, start, stop, step):
+        for c in range(start, stop, 256):
             part = jnp.dot(lhs, w[:, c : c + 256], preferred_element_type=F32)
             for half in range(2):
                 tile = c // LANES + half
                 at = first + (tile if step == 1 else (tile % 2) * 8 + tile // 2)
                 put(at, part[:, half * LANES : (half + 1) * LANES])
 
-    place(wq, 0, 1)
-    place(wk, 8, 1)
-    place(wv, 16, 2)
-    for pair in range(STACK // 2):
-        part = rows[pair * 2 * n : (pair + 1) * 2 * n, :].astype(BF16)
-        out[:, :, pair * LANES : (pair + 1) * LANES] = part.reshape(n, 2, LANES)
+    cols = wq.shape[1]
+    place(wq, 0, 0, cols, 1)
+    send(0, 4)
+    place(wk, 8, 0, cols, 1)
+    send(4, 4)
+    send(16, 1)
+    place(wv, 16, 0, cols, 2)
+    send(8, 2)
+    send(12, 2)
+    place(wv, 16, cols, 2 * cols, 2)
+    send(10, 2)
+    send(14, 2)
     for copy in copies:
         copy.wait()
 
@@ -161,12 +175,9 @@
     keeps[...] = jnp.broadcast_to(keep, keeps.shape)
 
 
-def update_kernel(keys, vals, keeps, memory_in, memory_out, memory, sems):
+def update_kernel(keys, vals, keeps, memory, memory_out, fresh, sems):
     heads = memory.shape[0]
-    loads = [pltpu.make_async_copy(memory_in.at[h], memory.at[h], sems.at[h]) for h in range(heads)]
-    stores = [pltpu.make_async_copy(memory.at[h], memory_out.at[h], sems.at[heads + h]) for h in range(heads)]
-    for load in loads:
-        load.start()
+    stores = [pltpu.make_async_copy(fresh.at[h], memory_out.at[h], sems.at[h]) for h in range(heads)]
     v_high, v_low = split(vals[...])
     k_high, k_low = split(keys[...])
     for h in range(heads):
@@ -174,8 +185,7 @@
         left = jnp.concatenate([v_high[row], v_high[row], v_low[row]], axis=0)
         right = jnp.concatenate([k_high[row], k_low[row], k_high[row]], axis=0)
         outer = lax.dot_general(left, right, TN, preferred_element_type=F32)
-        loads[h].wait()
-        memory[h] = keeps[row, :] * memory[h] + outer
+        fresh[h] = keeps[row, :] * memory[h] + outer
         stores[h].start()
     for store in stores:
         store.wait()
@@ -360,14 +370,14 @@
     )
     packed = lax.psum(padded, "tp")
 
-    sends, state_norm, old_stab, ibias, fbias = call(
+    state_norm, old_stab, ibias, fbias, sends = call(
         project_kernel,
         [
-            ((rows, 2, STACK // 2 * LANES), BF16),
             (normalizer.shape[1:], F32),
             (stabilizer.shape, F32),
             ((1, igate_bias.shape[0]), F32),
             ((1, fgate_bias.shape[0]), F32),
+            ((rows, 2, STACK // 2 * LANES), BF16),
         ],
         kv_pos,
         packed,
@@ -383,9 +393,13 @@
         fgate_bias[None],
         scalars=1,
         far=4,
-        fetched=4,
-        away=(0,),
-        scratch=[pltpu.VMEM((rows * STACK, LANES), F32), pltpu.SemaphoreType.DMA((4,))],
+        fetched=5,
+        away=(4,),
+        scratch=[
+            pltpu.VMEM((rows * STACK, LANES), F32),
+            pltpu.VMEM((rows, 2, STACK // 2 * LANES), BF16),
+            pltpu.SemaphoreType.DMA((11,)),
+        ],
     )
     arrived = lax.all_to_all(sends, "kv", 0, 0, tiled=True)
     hidden = w_up.shape[1]
@@ -433,24 +447,9 @@
         ibias,
         fbias,
         scalars=1,
-        away=(0, 4, 5),
+        away=(4, 5),
     )
     cells = lax.all_to_all(cell, "kv", 0, 0, tiled=True)
-    new_memory = call(
-        update_kernel,
-        [(memory.shape[1:], F32)],
-        keys,
-        vals,
-        keeps,
-        memory[0],
-        far=1,
-        fetched=1,
-        away=(0,),
-        scratch=[pltpu.VMEM(memory.shape[1:], F32), pltpu.SemaphoreType.DMA((16,))],
-    )
-
-    cells, new_memory = lax.optimization_barrier((cells, new_memory))
-
     half, crossing = call(
         output_kernel,
         [((quarter, 2 * rows), BF16), ((thin, 2 * rows), BF16)],
@@ -471,12 +470,24 @@
     )
     middles = lax.all_to_all(middle, "kv", 0, 0, tiled=True).reshape(kv * quarter, 2 * rows)
     sums = call(up_kernel, [((136, 128), F32)], tp_pos, middles, keep, other, scalars=1)
+    far_sums = lax.ppermute(sums, "tp", [(0, 1), (1, 0)])
+    new_memory = call(
+        update_kernel,
+        [(memory.shape[1:], F32)],
+        keys,
+        vals,
+        keeps,
+        state,
+        fetched=1,
+        away=(0,),
+        scratch=[pltpu.VMEM(memory.shape[1:], F32), pltpu.SemaphoreType.DMA((8,))],
+    )
     downs = call(
         down_kernel,
         [((kv * quarter, 2 * rows), BF16)],
         tp_pos,
         sums,
-        lax.ppermute(sums, "tp", [(0, 1), (1, 0)]),
+        far_sums,
         keep,
         other,
         scalars=1,

time: 112 us -> 112 us (level)
  waiting for transfers between devices: 21.2 us -> 24.1 us
  starting transfers between devices: 24.6 us -> 22.5 us
  blocking collectives: 49 us -> 50.9 us
  Pallas kernels: 14.2 us -> 12.4 us
    all_to_all x1, waiting for transfers between devices: 9.32 us -> 12.2 us  [on_device(): lax.all_to_all(downs.reshape(kv, quarter, 2 * rows), 'kv', 0, 0, tiled=True)]
    all_to_all x1, starting transfers between devices: 6.72 us -> 4.61 us  [on_device(): lax.all_to_all(downs.reshape(kv, quarter, 2 * rows), 'kv', 0, 0, tiled=True)]
    all_to_all x1, blocking collectives: 17.2 us -> 19.1 us  [on_device(): cells = lax.all_to_all(cell, 'kv', 0, 0, tiled=True)]
    pallas_call x10, Pallas kernels: 12.9 us -> 11.1 us  [call(): pl.pallas_call(kernel, out_shape=outs if many else outs[0], in_specs=[sme...]
  transfers between devices with their start and end apart: 4 -> 4, of which waited for: 4 -> 4; matrix products, arithmetic and copies ran while one was open for 0% -> 0% of each run, Pallas kernels for 7% -> 5%
where the time goes in v6:
time: 112 us; the launch traced here: 111 us
  blocking collectives  50.9 us (45%)
  waiting for transfers between devices  24.1 us (22%)
  starting transfers between devices  22.5 us (20%)
  Pallas kernels  12.4 us (11%)
    all_to_all x1, blocking collectives, on_device(): cells = lax.all_to_all(cell, 'kv', 0, 0, tiled=True)  19.1 us
    all_to_all x1, blocking collectives, on_device(): lax.all_to_all(middle, 'kv', 0, 0, tiled=True)  17.2 us
    all_to_all x1, waiting for transfers between devices, on_device(): lax.all_to_all(downs.reshape(kv, quarter, 2 * rows), 'kv', 0, 0, tiled=True)  12.2 us
    pallas_call x10, Pallas kernels, call(): pl.pallas_call(kernel, out_shape=outs if many else outs[0], in_specs=[sme...  11.1 us
    all_to_all x1, starting transfers between devices, on_device(): arrived = lax.all_to_all(sends, 'kv', 0, 0, tiled=True)  11 us
    psum x1, blocking collectives, on_device(): packed = lax.psum(padded, 'tp')  9 us
    all_to_all x1, waiting for transfers between devices, on_device(): arrived = lax.all_to_all(sends, 'kv', 0, 0, tiled=True)  8.52 us
    psum x1, blocking collectives, on_device(): lax.psum(crossing, 'tp')  5.54 us
  transfers between devices with their start and end apart: 4, of which 4 were waited for; matrix products, arithmetic and copies ran while one was open for 0% of the time, Pallas kernels for 5%

profile of v6, /device:TPU:1, one launch (start us, length us, event | category | flops | bytes accessed | tf_op | source)
XLA Modules:
  0.0 111.0 jit_solution(13626272890822914456)
XLA Ops:
  0.6 1.2 %shard_map.183 = (bf16[32,128]{1,0:T(8,128)(2,1)S(1)}, bf16[32,64]{1,0:T(8,128)(2,1)S(1)}, f32[32,128]{1,0:T(8,128)S(1)}, bf16[64,1024]{1,0:T(8,128)(2,1)S(1)}, ...) custom-call(s32[1]{0:T(128)} %bitcast.1.kv_pos, ...), custom_call_target="tpu_custom_call" | custom-call | tf_op jit(solution)/shard_map/pallas_call | solution.py:311
  1.8 9.0 %psum.14.packed = bf16[32,128]{1,0:T(8,128)(2,1)S(1)} all-reduce(bf16[32,128]{1,0:T(8,128)(2,1)S(1)} %get-tuple-element.34), channel_id=1, replica_groups=mesh['dp'=4,'kv'=64,'tp'=2] {'tp'}, use_global_device_ids=true, to_apply=%region_0.0 | all-reduce | flops 4096 | bytes 16384 | tf_op jit(solution)/shard_map/psum | solution.py:371
  10.8 1.7 %shard_map.184 = (f32[8,128]{1,0:T(8,128)S(1)}, f32[1,8]{1,0:T(1,128)S(1)}, f32[1,16]{1,0:T(1,128)S(1)}, f32[1,16]{1,0:T(1,128)S(1)}, bf16[64,2,2176]{2,1,0:T(2,128)(2,1)}) custom-call(s32[1]{0:T(128)} %bitcast.1.kv_pos, bf16[32,128]{1,0:T(8,128)(2,1)S(1)} %psum.14.packed, f32[32,128]{1,0:T(8,128)S(1)} %get-tuple-element.35.gain, ...), custom_call_target="tpu_custom_call" | custom-call | tf_op jit(solution)/shard_map/pallas_call | solution.py:311
  12.6 11.0 %all-to-all-start = ((bf16[64,2,2176]{2,1,0:T(2,128)(2,1)}), bf16[64,2,2176]{2,1,0:T(2,128)(2,1)S(1)}, u32[]{:S(2)}, u32[]{:S(2)}) async-start(bf16[64,2,2176]{2,1,0:T(2,128)(2,1)} %get-tuple-element.41), calls=%async_computation | async-start | bytes 1114112 | tf_op jit(solution)/shard_map/all_to_all | solution.py:404
  23.6 0.2 reshape.36
  23.8 0.1 reshape.37.gain
  24.0 3.0 %shard_map.185 = (bf16[2048,256]{1,0:T(8,128)(2,1)}, bf16[2048,256]{1,0:T(8,128)(2,1)}, bf16[64,2048]{1,0:T(8,128)(2,1)S(1)}) custom-call(s32[1]{0:T(128)} %bitcast.tp_pos, bf16[64,2,2,16,128]{4,3,2,1,0:T(8,128)(2,1)S(1)} %bitcast.20, f32[4,1024]{1,0:T(4,128)S(1)} %reshape.37.gain, bf16[128,4096]{1,0:T(8,128)(2,1)S(1)} %copy-done.2, bf16[64,2048]{1,0:T(8,128)(2,1)} %bitcast.25), custom_call_target="tpu_custom_call" | custom-call | tf_op jit(solution)/shard_map/pallas_call | solution.py:311
  26.9 2.5 %collective-permute-start = (bf16[2048,256]{1,0:T(8,128)(2,1)}, bf16[2048,256]{1,0:T(8,128)(2,1)S(1)}, u32[]{:S(2)}, u32[]{:S(2)}) collective-permute-start(bf16[2048,256]{1,0:T(8,128)(2,1)} %get-tuple-element.43), channel_id=1, source_target_pairs={{0,1},{1,0},{2,3},{3,2},{4,5},{5,4},{6,7},{7,6},{8,9},{9,8},{10,11... | collective-permute-start | bytes 3145736 | tf_op jit(solution)/shard_map/ppermute | solution.py:422
  29.5 2.5 %collective-permute-done.after.other = bf16[2048,256]{1,0:T(8,128)(2,1)S(1)} collective-permute-done((bf16[2048,256]{1,0:T(8,128)(2,1)}, bf16[2048,256]{1,0:T(8,128)(2,1)S(1)}, u32[]{:S(2)}, u32[]{:S(2)}) %collective-permute-start) | collective-permute-done | bytes 1048608 | tf_op jit(solution)/shard_map/ppermute | solution.py:422
  32.0 1.2 %shard_map.186.memory = f32[8,256,128]{2,1,0:T(8,128)S(1)} custom-call(f32[8,256,128]{2,1,0:T(8,128)} %bitcast.22, bf16[2048,256]{1,0:T(8,128)(2,1)S(1)} %collective-permute-done.after.other), custom_call_target="tpu_custom_call" | custom-call | tf_op jit(solution)/shard_map/pallas_call | solution.py:423
  33.2 8.5 %all-to-all-done.arrived = bf16[64,2,2176]{2,1,0:T(2,128)(2,1)S(1)} async-done(((bf16[64,2,2176]{2,1,0:T(2,128)(2,1)}), bf16[64,2,2176]{2,1,0:T(2,128)(2,1)S(1)}, u32[]{:S(2)}, u32[]{:S(2)}) %all-to-all-start) | async-done | bytes 557088 | tf_op jit(solution)/shard_map/all_to_all | solution.py:404
  41.7 1.0 shard_map.187
  42.7 19.1 %all_to_all.20.arrived = bf16[64,16,128]{2,1,0:T(8,128)(2,1)S(1)} all-to-all(bf16[64,16,128]{2,1,0:T(8,128)(2,1)S(1)} %get-tuple-element.50), channel_id=1, replica_groups=mesh['dp'=4,'kv'=64,'tp'=2] {'kv'}, dimensions={0} | all-to-all | bytes 524288 | tf_op jit(solution)/shard_map/all_to_all | solution.py:452
  61.8 0.4 shard_map.188
  62.2 5.5 %psum.15.both = bf16[32,128]{1,0:T(8,128)(2,1)S(1)} all-reduce(bf16[32,128]{1,0:T(8,128)(2,1)S(1)} %get-tuple-element.53), channel_id=1, replica_groups=mesh['dp'=4,'kv'=64,'tp'=2] {'tp'}, use_global_device_ids=true, to_apply=%region_1.0 | all-reduce | flops 4096 | bytes 16384 | tf_op jit(solution)/shard_map/psum | solution.py:467
  67.9 17.2 %all_to_all.21 = bf16[64,16,128]{2,1,0:T(8,128)(2,1)S(1)} all-to-all(bf16[64,16,128]{2,1,0:T(8,128)(2,1)S(1)} %get-tuple-element.55), channel_id=1, replica_groups=mesh['dp'=4,'kv'=64,'tp'=2] {'kv'}, dimensions={0} | all-to-all | bytes 524288 | tf_op jit(solution)/shard_map/all_to_all | solution.py:471
  85.1 0.6 shard_map.190.near
  85.7 4.4 %collective-permute-start.1 = (f32[136,128]{1,0:T(8,128)S(1)}, f32[136,128]{1,0:T(8,128)S(1)}, u32[]{:S(2)}, u32[]{:S(2)}) collective-permute-start(f32[136,128]{1,0:T(8,128)S(1)} %shard_map.190.near), channel_id=1, source_target_pairs={{0,1},{1,0},{2,3},{3,2},{4,5},{5,4},{6,7},{7,6},{8,9},{9,8},{10,11... | collective-permute-start | bytes 208904 | tf_op jit(solution)/shard_map/ppermute | solution.py:473
  90.1 0.9 collective-permute-done.1.far_sums
  90.9 1.2 %shard_map.191 = bf16[1024,128]{1,0:T(8,128)(2,1)} custom-call(s32[1]{0:T(128)} %bitcast.tp_pos, f32[136,128]{1,0:T(8,128)S(1)} %shard_map.190.near, f32[136,128]{1,0:T(8,128)S(1)} %collective-permute-done.1.far_sums, bf16[2048,256]{1,0:T(8,128)(2,1)S(1)} %copy-done, bf16[2048,256]{1,0:T(8,128)(2,1)S(1)} %collective-permute-done.after.other), custom_call_target="tpu_custom_call" | custom-call | tf_op jit(solution)/shard_map/pallas_call | solution.py:311
  92.2 4.6 %all-to-all-start.3 = ((bf16[64,16,128]{2,1,0:T(8,128)(2,1)}), bf16[64,16,128]{2,1,0:T(8,128)(2,1)S(1)}, u32[]{:S(2)}, u32[]{:S(2)}) async-start(bf16[64,16,128]{2,1,0:T(8,128)(2,1)} %bitcast.14), calls=%async_computation.3 | async-start | bytes 524288 | tf_op jit(solution)/shard_map/all_to_all | solution.py:495
  96.8 1.2 %shard_map.193 = f32[8,256,128]{2,1,0:T(8,128)} custom-call(f32[8,128]{1,0:T(8,128)S(1)} %get-tuple-element.59.keys, f32[8,256]{1,0:T(8,128)S(1)} %get-tuple-element.60.vals, f32[8,128]{1,0:T(8,128)S(1)} %get-tuple-element.61.keeps, f32[8,256,128]{2,1,0:T(8,128)S(1)} %shard_map.186.memory), custom_call_target="tpu_custom_call" | custom-call | tf_op jit(solution)/shard_map/pallas_call | solution.py:311
  98.0 12.2 %all-to-all-done.3.back = bf16[64,16,128]{2,1,0:T(8,128)(2,1)S(1)} async-done(((bf16[64,16,128]{2,1,0:T(8,128)(2,1)}), bf16[64,16,128]{2,1,0:T(8,128)(2,1)S(1)}, u32[]{:S(2)}, u32[]{:S(2)}) %all-to-all-start.3) | async-done | bytes 262176 | tf_op jit(solution)/shard_map/all_to_all | solution.py:495
  110.3 0.8 shard_map.192
  (10 shorter events, 0.1 us)
Async XLA Ops:
  1.8 21.8 %copy-start.3 = (f32[4096]{0:T(1024)S(1)}, f32[4096]{0:T(1024)}, u32[]{:S(2)}) copy-start(f32[4096]{0:T(1024)} %param.29) | copy-start | bytes 49156
  10.8 13.1 %copy-start.1 = (bf16[4096,128]{1,0:T(8,128)(2,1)S(1)}, bf16[4096,128]{1,0:T(8,128)(2,1)}, u32[]{:S(2)}) copy-start(bf16[4096,128]{1,0:T(8,128)(2,1)} %param.30) | copy-start | bytes 3145732
  10.8 13.1 %copy-start.2 = (bf16[128,4096]{1,0:T(8,128)(2,1)S(1)}, bf16[128,4096]{1,0:T(8,128)(2,1)}, u32[]{:S(2)}) copy-start(bf16[128,4096]{1,0:T(8,128)(2,1)} %w_down.1) | copy-start | bytes 3145732
  12.6 29.1 %all-to-all-start = ((bf16[64,2,2176]{2,1,0:T(2,128)(2,1)}), bf16[64,2,2176]{2,1,0:T(2,128)(2,1)S(1)}, u32[]{:S(2)}, u32[]{:S(2)}) async-start(bf16[64,2,2176]{2,1,0:T(2,128)(2,1)} %get-tuple-element.41), calls=%async_computation | async-start | bytes 1114112 | tf_op jit(solution)/shard_map/all_to_all | solution.py:404
  26.9 5.0 %collective-permute-start = (bf16[2048,256]{1,0:T(8,128)(2,1)}, bf16[2048,256]{1,0:T(8,128)(2,1)S(1)}, u32[]{:S(2)}, u32[]{:S(2)}) collective-permute-start(bf16[2048,256]{1,0:T(8,128)(2,1)} %get-tuple-element.43), channel_id=1, source_target_pairs={{0,1},{1,0},{2,3},{3,2},{4,5},{5,4},{6,7},{7,6},{8,9},{9,8},{10,11... | collective-permute-start | bytes 3145736 | tf_op jit(solution)/shard_map/ppermute | solution.py:422
  42.7 42.4 %copy-start = (bf16[2048,256]{1,0:T(8,128)(2,1)S(1)}, bf16[2048,256]{1,0:T(8,128)(2,1)}, u32[]{:S(2)}) copy-start(bf16[2048,256]{1,0:T(8,128)(2,1)} %get-tuple-element.56.keep) | copy-start | bytes 3145732
  85.7 5.3 %collective-permute-start.1 = (f32[136,128]{1,0:T(8,128)S(1)}, f32[136,128]{1,0:T(8,128)S(1)}, u32[]{:S(2)}, u32[]{:S(2)}) collective-permute-start(f32[136,128]{1,0:T(8,128)S(1)} %shard_map.190.near), channel_id=1, source_target_pairs={{0,1},{1,0},{2,3},{3,2},{4,5},{5,4},{6,7},{7,6},{8,9},{9,8},{10,11... | collective-permute-start | bytes 208904 | tf_op jit(solution)/shard_map/ppermute | solution.py:473
  92.2 18.1 %all-to-all-start.3 = ((bf16[64,16,128]{2,1,0:T(8,128)(2,1)}), bf16[64,16,128]{2,1,0:T(8,128)(2,1)S(1)}, u32[]{:S(2)}, u32[]{:S(2)}) async-start(bf16[64,16,128]{2,1,0:T(8,128)(2,1)} %bitcast.14), calls=%async_computation.3 | async-start | bytes 524288 | tf_op jit(solution)/shard_map/all_to_all | solution.py:495

commit v7 on v6

--- a/solution.py
+++ b/solution.py
@@ -32,31 +32,30 @@
 any_space = pl.BlockSpec(memory_space=pl.ANY)
 
 
-def fetch_kernel(kv_pos, tp_pos, tokens, gain, wq, wk, wv, wig, wfg, padded, *rest):
+def fetch_kernel(kv_pos, tokens, gain, wq, wk, wv, wig, wfg, *rest):
     outs, sems = rest[:-1], rest[-1]
     start = pl.multiple_of(kv_pos[0] // 2 * LANES, LANES)
     sources = (tokens, gain, wq, wk, wv, wig.at[:, pl.ds(start, LANES)], wfg.at[:, pl.ds(start, LANES)])
     copies = [pltpu.make_async_copy(src, dst, sems.at[i]) for i, (src, dst) in enumerate(zip(sources, outs))]
     for copy in copies:
         copy.start()
-    copies[0].wait()
-    x = outs[0][...].astype(F32)
-    twice = jnp.concatenate([x, x], axis=1)
-    padded[...] = jnp.where(halves_of(twice) == tp_pos[0], twice, 0.0).astype(BF16)
-    for copy in copies[1:]:
+    for copy in copies:
         copy.wait()
 
 
-def project_kernel(kv_pos, packed, gain, wq, wk, wv, wig, wfg, *rest):
+def project_kernel(kv_pos, tp_pos, own, other, gain, wq, wk, wv, wig, wfg, *rest):
     sources, held, out, rows, ready, sems = rest[:4], rest[4:8], rest[8], rest[9], rest[10], rest[11]
     copies = [pltpu.make_async_copy(src, dst, sems.at[i]) for i, (src, dst) in enumerate(zip(sources, held))]
     for copy in copies:
         copy.start()
-    n = packed.shape[1] // 2
+    n = own.shape[1]
     block = kv_pos[0] // 2
     odd = kv_pos[0] % 2
-    wide = packed[...].astype(F32)
-    x = jnp.concatenate([wide[:, :n].T, wide[:, n:].T], axis=1)
+    near = own[...].astype(F32)
+    far = other[...].astype(F32)
+    first = jnp.where(tp_pos[0] == 0, near, far)
+    second = jnp.where(tp_pos[0] == 0, far, near)
+    x = jnp.concatenate([first.T, second.T], axis=1)
     twice = jnp.concatenate([x, x], axis=1)
 
     def put(at, tile):
@@ -342,10 +341,10 @@
     rows, thin = tokens.shape
     kv_pos = kv_index.astype(jnp.int32).reshape(1)
     tp_pos = tp_index.astype(jnp.int32).reshape(1)
-    padded, own_tokens, gain_near, wq, wk, wv, ig, fg = call(
+    far_tokens = lax.ppermute(tokens.T, "tp", [(0, 1), (1, 0)])
+    own_tokens, gain_near, wq, wk, wv, ig, fg = call(
         fetch_kernel,
         [
-            ((thin, 2 * rows), BF16),
             ((thin, rows), BF16),
             ((mix_gain.shape[0] // LANES, LANES), F32),
             (w_query.shape, BF16),
@@ -355,7 +354,6 @@
             ((w_fgate.shape[1], LANES), BF16),
         ],
         kv_pos,
-        tp_pos,
         tokens.T,
         mix_gain.reshape(-1, LANES),
         w_query,
@@ -363,12 +361,11 @@
         w_value,
         w_igate.T,
         w_fgate.T,
-        scalars=2,
+        scalars=1,
         far=7,
-        fetched=6,
+        fetched=7,
         scratch=[pltpu.SemaphoreType.DMA((7,))],
     )
-    packed = lax.psum(padded, "tp")
 
     state_norm, old_stab, ibias, fbias, sends = call(
         project_kernel,
@@ -380,7 +377,9 @@
             ((rows, 2, STACK // 2 * LANES), BF16),
         ],
         kv_pos,
-        packed,
+        tp_pos,
+        own_tokens,
+        far_tokens,
         gain_near,
         wq,
         wk,
@@ -391,7 +390,7 @@
         stabilizer,
         igate_bias[None],
         fgate_bias[None],
-        scalars=1,
+        scalars=2,
         far=4,
         fetched=5,
         away=(4,),

time: 112 us -> 112 us (level)
  blocking collectives: 50.9 us -> 41.8 us
  starting transfers between devices: 22.5 us -> 31 us
    psum x1 -> x0, blocking collectives: 9 us -> none  [on_device(): packed = lax.psum(padded, 'tp')]
    ppermute x0 -> x1, starting transfers between devices: none -> 8.75 us  [on_device(): far_tokens = lax.ppermute(tokens.T, 'tp', [(0, 1), (1, 0)])]
  transfers between devices with their start and end apart: 4 -> 5, of which waited for: 4 -> 4; matrix products, arithmetic and copies ran while one was open for 0% -> 0% of each run, Pallas kernels for 5% -> 6%
where the time goes in v7:
time: 112 us; the launch traced here: 111 us
  blocking collectives  41.8 us (37%)
  starting transfers between devices  31 us (28%)
  waiting for transfers between devices  24.6 us (22%)
  Pallas kernels  12.3 us (11%)
    all_to_all x1, blocking collectives, on_device(): cells = lax.all_to_all(cell, 'kv', 0, 0, tiled=True)  18.9 us
    all_to_all x1, blocking collectives, on_device(): lax.all_to_all(middle, 'kv', 0, 0, tiled=True)  17.3 us
    all_to_all x1, waiting for transfers between devices, on_device(): lax.all_to_all(downs.reshape(kv, quarter, 2 * rows), 'kv', 0, 0, tiled=True)  12.2 us
    pallas_call x10, Pallas kernels, call(): pl.pallas_call(kernel, out_shape=outs if many else outs[0], in_specs=[sme...  11 us
    all_to_all x1, starting transfers between devices, on_device(): arrived = lax.all_to_all(sends, 'kv', 0, 0, tiled=True)  11 us
    all_to_all x1, waiting for transfers between devices, on_device(): arrived = lax.all_to_all(sends, 'kv', 0, 0, tiled=True)  9.05 us
    ppermute x1, starting transfers between devices, on_device(): far_tokens = lax.ppermute(tokens.T, 'tp', [(0, 1), (1, 0)])  8.75 us
    psum x1, blocking collectives, on_device(): lax.psum(crossing, 'tp')  5.66 us
  transfers between devices with their start and end apart: 5, of which 4 were waited for; matrix products, arithmetic and copies ran while one was open for 0% of the time, Pallas kernels for 6%

profile of v7, /device:TPU:1, one launch (start us, length us, event | category | flops | bytes accessed | tf_op | source)
XLA Modules:
  0.0 110.9 jit_solution(2558728272278407789)
XLA Ops:
  0.6 8.7 %collective-permute-start = (bf16[32,64]{1,0:T(8,128)(2,1)}, bf16[32,64]{1,0:T(8,128)(2,1)S(1)}, u32[]{:S(2)}, u32[]{:S(2)}) collective-permute-start(bf16[32,64]{1,0:T(8,128)(2,1)} %bitcast.29), channel_id=1, source_target_pairs={{0,1},{1,0},{2,3},{3,2},{4,5},{5,4},{6,7},{7,6},{8,9},{9,8},{10,11... | collective-permute-start | bytes 12296 | tf_op jit(solution)/shard_map/ppermute | solution.py:344
  9.4 1.2 %shard_map.183 = (bf16[32,64]{1,0:T(8,128)(2,1)S(1)}, f32[32,128]{1,0:T(8,128)S(1)}, bf16[64,1024]{1,0:T(8,128)(2,1)S(1)}, bf16[64,1024]{1,0:T(8,128)(2,1)S(1)},...) custom-call(s32[1]{0:T(128)} %bitcast.1.kv_pos, bf16[32,64]{1,0:T(8,128)(2,1)} %bitcast.30, ...), custom_call_target="tpu_custom_call" | custom-call | tf_op jit(solution)/shard_map/pallas_call | solution.py:310
  10.6 1.6 %shard_map.184 = (f32[8,128]{1,0:T(8,128)S(1)}, f32[1,8]{1,0:T(1,128)S(1)}, f32[1,16]{1,0:T(1,128)S(1)}, f32[1,16]{1,0:T(1,128)S(1)}, bf16[64,2,2176]{2,1,0:T(2,128)(2,1)}) custom-call(s32[1]{0:T(128)} %bitcast.1.kv_pos, s32[1]{0:T(128)} %bitcast.tp_pos, bf16[32,64]{1,0:T(8,128)(2,1)S(1)} %get-tuple-element.33.own.tokens, ...), custom_call_target="tpu_custom_call" | custom-call | tf_op jit(solution)/shard_map/pallas_call | solution.py:310
  12.3 11.0 %all-to-all-start = ((bf16[64,2,2176]{2,1,0:T(2,128)(2,1)}), bf16[64,2,2176]{2,1,0:T(2,128)(2,1)S(1)}, u32[]{:S(2)}, u32[]{:S(2)}) async-start(bf16[64,2,2176]{2,1,0:T(2,128)(2,1)} %get-tuple-element.40), calls=%async_computation | async-start | bytes 1114112 | tf_op jit(solution)/shard_map/all_to_all | solution.py:403
  23.3 0.2 reshape.36
  23.5 0.1 reshape.37.gain
  23.6 3.0 %shard_map.185 = (bf16[2048,256]{1,0:T(8,128)(2,1)}, bf16[2048,256]{1,0:T(8,128)(2,1)}, bf16[64,2048]{1,0:T(8,128)(2,1)S(1)}) custom-call(s32[1]{0:T(128)} %bitcast.tp_pos, bf16[64,2,2,16,128]{4,3,2,1,0:T(8,128)(2,1)S(1)} %bitcast.20, f32[4,1024]{1,0:T(4,128)S(1)} %reshape.37.gain, bf16[128,4096]{1,0:T(8,128)(2,1)S(1)} %copy-done.2, bf16[64,2048]{1,0:T(8,128)(2,1)} %bitcast.25), custom_call_target="tpu_custom_call" | custom-call | tf_op jit(solution)/shard_map/pallas_call | solution.py:310
  26.6 2.3 %collective-permute-start.1 = (bf16[2048,256]{1,0:T(8,128)(2,1)}, bf16[2048,256]{1,0:T(8,128)(2,1)S(1)}, u32[]{:S(2)}, u32[]{:S(2)}) collective-permute-start(bf16[2048,256]{1,0:T(8,128)(2,1)} %get-tuple-element.42), channel_id=1, source_target_pairs={{0,1},{1,0},{2,3},{3,2},{4,5},{5,4},{6,7},{7,6},{8,9},{9,8},{10,11... | collective-permute-start | bytes 3145736 | tf_op jit(solution)/shard_map/ppermute | solution.py:421
  28.9 2.5 %collective-permute-done.1.after.other = bf16[2048,256]{1,0:T(8,128)(2,1)S(1)} collective-permute-done((bf16[2048,256]{1,0:T(8,128)(2,1)}, bf16[2048,256]{1,0:T(8,128)(2,1)S(1)}, u32[]{:S(2)}, u32[]{:S(2)}) %collective-permute-start.1) | collective-permute-done | bytes 1048608 | tf_op jit(solution)/shard_map/ppermute | solution.py:421
  31.4 1.2 %shard_map.186.memory = f32[8,256,128]{2,1,0:T(8,128)S(1)} custom-call(f32[8,256,128]{2,1,0:T(8,128)} %bitcast.22, bf16[2048,256]{1,0:T(8,128)(2,1)S(1)} %collective-permute-done.1.after.other), custom_call_target="tpu_custom_call" | custom-call | tf_op jit(solution)/shard_map/pallas_call | solution.py:422
  32.7 9.0 %all-to-all-done.arrived = bf16[64,2,2176]{2,1,0:T(2,128)(2,1)S(1)} async-done(((bf16[64,2,2176]{2,1,0:T(2,128)(2,1)}), bf16[64,2,2176]{2,1,0:T(2,128)(2,1)S(1)}, u32[]{:S(2)}, u32[]{:S(2)}) %all-to-all-start) | async-done | bytes 557088 | tf_op jit(solution)/shard_map/all_to_all | solution.py:403
  41.7 1.0 shard_map.187
  42.7 18.9 %all_to_all.20.arrived = bf16[64,16,128]{2,1,0:T(8,128)(2,1)S(1)} all-to-all(bf16[64,16,128]{2,1,0:T(8,128)(2,1)S(1)} %get-tuple-element.49), channel_id=1, replica_groups=mesh['dp'=4,'kv'=64,'tp'=2] {'kv'}, dimensions={0} | all-to-all | bytes 524288 | tf_op jit(solution)/shard_map/all_to_all | solution.py:451
  61.6 0.4 shard_map.188
  61.9 5.7 %psum.7.both = bf16[32,128]{1,0:T(8,128)(2,1)S(1)} all-reduce(bf16[32,128]{1,0:T(8,128)(2,1)S(1)} %get-tuple-element.52), channel_id=1, replica_groups=mesh['dp'=4,'kv'=64,'tp'=2] {'tp'}, use_global_device_ids=true, to_apply=%region_0.0 | all-reduce | flops 4096 | bytes 16384 | tf_op jit(solution)/shard_map/psum | solution.py:466
  67.7 17.3 %all_to_all.21 = bf16[64,16,128]{2,1,0:T(8,128)(2,1)S(1)} all-to-all(bf16[64,16,128]{2,1,0:T(8,128)(2,1)S(1)} %get-tuple-element.53), channel_id=1, replica_groups=mesh['dp'=4,'kv'=64,'tp'=2] {'kv'}, dimensions={0} | all-to-all | bytes 524288 | tf_op jit(solution)/shard_map/all_to_all | solution.py:470
  85.0 0.6 shard_map.190.near
  85.6 4.3 %collective-permute-start.2 = (f32[136,128]{1,0:T(8,128)S(1)}, f32[136,128]{1,0:T(8,128)S(1)}, u32[]{:S(2)}, u32[]{:S(2)}) collective-permute-start(f32[136,128]{1,0:T(8,128)S(1)} %shard_map.190.near), channel_id=1, source_target_pairs={{0,1},{1,0},{2,3},{3,2},{4,5},{5,4},{6,7},{7,6},{8,9},{9,8},{10,11... | collective-permute-start | bytes 208904 | tf_op jit(solution)/shard_map/ppermute | solution.py:472
  89.9 0.9 collective-permute-done.2.far_sums
  90.8 1.2 %shard_map.191 = bf16[1024,128]{1,0:T(8,128)(2,1)} custom-call(s32[1]{0:T(128)} %bitcast.tp_pos, f32[136,128]{1,0:T(8,128)S(1)} %shard_map.190.near, f32[136,128]{1,0:T(8,128)S(1)} %collective-permute-done.2.far_sums, bf16[2048,256]{1,0:T(8,128)(2,1)S(1)} %copy-done, bf16[2048,256]{1,0:T(8,128)(2,1)S(1)} %collective-permute-done.1.after.other), custom_call_target="tpu_custom_call" | custom-call | tf_op jit(solution)/shard_map/pallas_call | solution.py:310
  92.0 4.6 %all-to-all-start.3 = ((bf16[64,16,128]{2,1,0:T(8,128)(2,1)}), bf16[64,16,128]{2,1,0:T(8,128)(2,1)S(1)}, u32[]{:S(2)}, u32[]{:S(2)}) async-start(bf16[64,16,128]{2,1,0:T(8,128)(2,1)} %bitcast.14), calls=%async_computation.3 | async-start | bytes 524288 | tf_op jit(solution)/shard_map/all_to_all | solution.py:494
  96.6 1.2 %shard_map.193 = f32[8,256,128]{2,1,0:T(8,128)} custom-call(f32[8,128]{1,0:T(8,128)S(1)} %get-tuple-element.57.keys, f32[8,256]{1,0:T(8,128)S(1)} %get-tuple-element.58.vals, f32[8,128]{1,0:T(8,128)S(1)} %get-tuple-element.59.keeps, f32[8,256,128]{2,1,0:T(8,128)S(1)} %shard_map.186.memory), custom_call_target="tpu_custom_call" | custom-call | tf_op jit(solution)/shard_map/pallas_call | solution.py:310
  97.9 12.2 %all-to-all-done.3.back = bf16[64,16,128]{2,1,0:T(8,128)(2,1)S(1)} async-done(((bf16[64,16,128]{2,1,0:T(8,128)(2,1)}), bf16[64,16,128]{2,1,0:T(8,128)(2,1)S(1)}, u32[]{:S(2)}, u32[]{:S(2)}) %all-to-all-start.3) | async-done | bytes 262176 | tf_op jit(solution)/shard_map/all_to_all | solution.py:494
  110.1 0.8 shard_map.192
  (11 shorter events, 0.1 us)
Async XLA Ops:
  0.6 10.0 %collective-permute-start = (bf16[32,64]{1,0:T(8,128)(2,1)}, bf16[32,64]{1,0:T(8,128)(2,1)S(1)}, u32[]{:S(2)}, u32[]{:S(2)}) collective-permute-start(bf16[32,64]{1,0:T(8,128)(2,1)} %bitcast.29), channel_id=1, source_target_pairs={{0,1},{1,0},{2,3},{3,2},{4,5},{5,4},{6,7},{7,6},{8,9},{9,8},{10,11... | collective-permute-start | bytes 12296 | tf_op jit(solution)/shard_map/ppermute | solution.py:344
  9.4 13.9 %copy-start.3 = (f32[4096]{0:T(1024)S(1)}, f32[4096]{0:T(1024)}, u32[]{:S(2)}) copy-start(f32[4096]{0:T(1024)} %param.29) | copy-start | bytes 49156
  10.6 13.0 %copy-start.1 = (bf16[4096,128]{1,0:T(8,128)(2,1)S(1)}, bf16[4096,128]{1,0:T(8,128)(2,1)}, u32[]{:S(2)}) copy-start(bf16[4096,128]{1,0:T(8,128)(2,1)} %param.30) | copy-start | bytes 3145732
  10.6 13.0 %copy-start.2 = (bf16[128,4096]{1,0:T(8,128)(2,1)S(1)}, bf16[128,4096]{1,0:T(8,128)(2,1)}, u32[]{:S(2)}) copy-start(bf16[128,4096]{1,0:T(8,128)(2,1)} %w_down.1) | copy-start | bytes 3145732
  12.3 29.4 %all-to-all-start = ((bf16[64,2,2176]{2,1,0:T(2,128)(2,1)}), bf16[64,2,2176]{2,1,0:T(2,128)(2,1)S(1)}, u32[]{:S(2)}, u32[]{:S(2)}) async-start(bf16[64,2,2176]{2,1,0:T(2,128)(2,1)} %get-tuple-element.40), calls=%async_computation | async-start | bytes 1114112 | tf_op jit(solution)/shard_map/all_to_all | solution.py:403
  26.6 4.8 %collective-permute-start.1 = (bf16[2048,256]{1,0:T(8,128)(2,1)}, bf16[2048,256]{1,0:T(8,128)(2,1)S(1)}, u32[]{:S(2)}, u32[]{:S(2)}) collective-permute-start(bf16[2048,256]{1,0:T(8,128)(2,1)} %get-tuple-element.42), channel_id=1, source_target_pairs={{0,1},{1,0},{2,3},{3,2},{4,5},{5,4},{6,7},{7,6},{8,9},{9,8},{10,11... | collective-permute-start | bytes 3145736 | tf_op jit(solution)/shard_map/ppermute | solution.py:421
  42.7 42.3 %copy-start = (bf16[2048,256]{1,0:T(8,128)(2,1)S(1)}, bf16[2048,256]{1,0:T(8,128)(2,1)}, u32[]{:S(2)}) copy-start(bf16[2048,256]{1,0:T(8,128)(2,1)} %get-tuple-element.54.keep) | copy-start | bytes 3145732
  85.6 5.2 %collective-permute-start.2 = (f32[136,128]{1,0:T(8,128)S(1)}, f32[136,128]{1,0:T(8,128)S(1)}, u32[]{:S(2)}, u32[]{:S(2)}) collective-permute-start(f32[136,128]{1,0:T(8,128)S(1)} %shard_map.190.near), channel_id=1, source_target_pairs={{0,1},{1,0},{2,3},{3,2},{4,5},{5,4},{6,7},{7,6},{8,9},{9,8},{10,11... | collective-permute-start | bytes 208904 | tf_op jit(solution)/shard_map/ppermute | solution.py:472
  92.0 18.1 %all-to-all-start.3 = ((bf16[64,16,128]{2,1,0:T(8,128)(2,1)}), bf16[64,16,128]{2,1,0:T(8,128)(2,1)S(1)}, u32[]{:S(2)}, u32[]{:S(2)}) async-start(bf16[64,16,128]{2,1,0:T(8,128)(2,1)} %bitcast.14), calls=%async_computation.3 | async-start | bytes 524288 | tf_op jit(solution)/shard_map/all_to_all | solution.py:494
